TPU v7x, 32 devices: a whole 2x2x4 slice. The times are simulated.
32 devices in a mesh: gr: 2 (over x), sp: 8 (over z, y), tp: 2 (over core).
Axes of the slice: x: 2, y: 2, z: 4, core: 2. Of those that a mesh axis runs over, the one named last changes fastest.
Arguments:
- context_input_tensor: bfloat16 [4, 8192, 2048], P(('gr', 'tp'), 'sp'), parts along dimension 0, may hold values from -8 to 8
- content_mapping_matrix: bfloat16 [2048, 1024], replicated, may hold values from -0.125 to 0.125
- address_mapping_matrix: bfloat16 [2048, 256], replicated, may hold values from -0.125 to 0.125
- increment_mapping_matrix: bfloat16 [2048, 16], replicated, may hold values from -0.125 to 0.125
- increment_speed_offset: float32 [16], P('sp'), may hold values from -1 to 0.5
- channel_fading_exponent: float32 [16], P('sp'), may hold values from -12 to -2
- extra_damping_spikes: float32 [4, 16, 8192], P(('gr', 'tp'), 'sp'), parts along dimension 0, may hold values from -3 to 0
- content_smoothing_coefficients: float32 [5, 16, 64], P(None, 'sp'), may hold values from -2.5 to 2.5
- address_smoothing_coefficients: float32 [5, 4, 64], replicated, may hold values from -2.5 to 2.5
- newest_lookup_matrix: bfloat16 [4, 4, 64], P(('gr', 'tp')), parts along dimension 0, may hold values from -6 to 6
- newest_output_switch: bfloat16 [4, 16, 64], P(('gr', 'tp'), 'sp'), parts along dimension 0, may hold values from -6 to 6
- cluster_scaling_coefficients: float32 [16, 64], P('sp'), may hold values from 0.1 to 1.9
Outputs:
- address_content_store: bfloat16 [4, 8192, 16, 128], P(('gr', 'tp'), None, 'sp'), parts along dimension 0
- earliest_switched_retrieval: bfloat16 [4, 16, 64], P(('gr', 'tp'), 'sp'), parts along dimension 0
There are 2 independent parts, one for each index of `gr`. A program takes and returns all parts, laid end to end along the dimension named above; an argument that names none is the same for every part. Nothing has to cross between parts.
All inputs are finite; a program needn't handle non-finite values.
Results may differ from a plain program's by a relative error of at most 0.009.
Values may be sent and summed in bfloat16 or wider, within the bound.
No kernel may reach another device: no remote copies, remote signals or barrier semaphores. Data moves between devices by JAX's collectives and lax.ppermute only.
A program may use at most 128 MiB of HBM per device.

v0:
```python
import jax
import jax.numpy as jnp
from jax import lax
from jax.experimental import pallas as pl
from jax.experimental.pallas import tpu as pltpu
from jax.sharding import PartitionSpec as P


HEADS = 16
HEAD = 64
GROUPS = 4
STATE = 64
LANES = 128
EXTRA = 16
VMEM_LIMIT = 24 * 2**20
EPS = 1e-05
F32 = jnp.float32
BF16 = jnp.bfloat16


def silu(x):
    return 0.5 * x * (1.0 + jnp.tanh(0.5 * x))


def rounded(x):
    return x.astype(BF16).astype(F32)


def lane_index(shape):
    return lax.broadcasted_iota(jnp.int32, shape, 1)


def whole(shape):
    return pl.BlockSpec(shape, lambda *_: (0,) * len(shape))


def on_chip(x):
    return pltpu.with_memory_space_constraint(x, pltpu.VMEM)


def off_chip(x):
    return pltpu.with_memory_space_constraint(x, pltpu.HBM)


def flip_permute(value, flip):
    pairs = [(source, source ^ flip) for source in range(lax.axis_size("sp"))]
    return lax.ppermute(value, "sp", pairs)


def key_block_kernel(group_devices, low_ref, high_ref, wk_ref, wr_ref, *rest):
    outs, (packed, rates) = rest[:-2], rest[-2:]
    repeats = HEADS // GROUPS
    step = pl.program_id(0)
    rows = low_ref.shape[0]
    tiles = rows // LANES
    half_tiles = rates.shape[0] // 2
    wk, wr = wk_ref[...], wr_ref[...]
    both = jnp.concatenate([low_ref[...], high_ref[...]], axis=0)
    k_both = rounded(jnp.dot(both, wk, preferred_element_type=F32))
    k_low, k_high = k_both[:rows], k_both[rows:]
    r_both = lax.dot_general(both, wr, (((1,), (1,)), ((), ())), preferred_element_type=F32).astype(BF16)
    left = lane_index((rows, LANES)) < STATE
    for group in range(GROUPS):
        column = slice(group // 2 * LANES, (group // 2 + 1) * LANES)
        a, b = k_low[:, column], k_high[:, column]
        if group % 2 == 0:
            b = pltpu.roll(b, STATE, 1)
        else:
            a = pltpu.roll(a, STATE, 1)
        packed[group, pl.ds(pl.multiple_of(step * rows, rows), rows), :] = jnp.where(left, a, b).astype(BF16)
    eye = (
        lax.broadcasted_iota(jnp.int32, (HEADS, HEADS), 0) == lax.broadcasted_iota(jnp.int32, (HEADS, HEADS), 1)
    ).astype(BF16)
    for part in range(2):
        r = r_both[part * rows : (part + 1) * rows]
        turned = lax.dot_general(eye, r, (((1,), (1,)), ((), ())), preferred_element_type=F32)
        for tile in range(tiles):
            rates[part * half_tiles + step * tiles + tile] = turned[:, tile * LANES : (tile + 1) * LANES]

    @pl.when(step == pl.num_programs(0) - 1)
    def _():
        half = packed.shape[1] - 2 * half_tiles * repeats
        for group in range(GROUPS):
            tail = jnp.concatenate(
                [rates[tile, group * repeats : (group + 1) * repeats, :] for tile in range(2 * half_tiles)], axis=0
            )
            packed[group, half:, :] = tail.astype(BF16)
        own = lax.axis_index("sp") // group_devices
        for offset, out in enumerate(outs):
            out[...] = packed[own ^ offset]


def key_blocks(rows, wk, wr, group_devices):
    span, model = rows.shape
    repeats = HEADS // GROUPS
    half = span // 2
    tile = half // 2
    steps = half // tile
    height = half + repeats * span // LANES
    block = jax.ShapeDtypeStruct((height, LANES), BF16)
    return pl.pallas_call(
        lambda *refs: key_block_kernel(group_devices, *refs),
        grid=(steps,),
        in_specs=[
            pl.BlockSpec((tile, model), lambda i: (i, 0)),
            pl.BlockSpec((tile, model), lambda i: (i + steps, 0)),
            whole(wk.shape),
            whole(wr.shape),
        ],
        out_specs=[whole((height, LANES))] * GROUPS,
        out_shape=[block] * GROUPS,
        scratch_shapes=[
            pltpu.VMEM((GROUPS, height, LANES), BF16),
            pltpu.VMEM((span // LANES, HEADS, LANES), F32),
        ],
        compiler_params=pltpu.CompilerParams(vmem_limit_bytes=VMEM_LIMIT),
        cost_estimate=pl.CostEstimate(
            flops=2 * span * model * (GROUPS * STATE + HEADS), bytes_accessed=2 * span * model, transcendentals=0
        ),
        name="key_blocks",
    )(off_chip(rows), off_chip(rows), off_chip(wk), wr)


def early_values_kernel(x_ref, after_ref, last_ref, w_ref, _, out_ref):
    rows = x_ref.shape[0]
    share = out_ref.shape[2]
    x = jnp.concatenate([x_ref[...], after_ref[...], last_ref[...]], axis=0)
    y = jnp.dot(x, w_ref[...], preferred_element_type=F32)
    extra = jnp.concatenate([y[rows : rows + 8], y[rows + 24 : rows + 32]], axis=0)
    for device in range(out_ref.shape[0]):
        lanes = slice(device * share, (device + 1) * share)
        out_ref[device, :rows, :] = y[:rows, lanes].astype(BF16)
        out_ref[device, rows:, :] = extra[:, lanes].astype(BF16)


def early_values(rows, wv, started, devices, cut):
    span, model = rows.shape
    width = wv.shape[1]
    share = width // devices
    tile = max(2 * LANES, share)
    return pl.pallas_call(
        early_values_kernel,
        grid=(width // tile,),
        in_specs=[
            whole((cut, model)),
            pl.BlockSpec((EXTRA, model), lambda i: (cut // EXTRA, 0)),
            pl.BlockSpec((EXTRA, model), lambda i: (span // EXTRA - 1, 0)),
            pl.BlockSpec((model, tile), lambda i: (0, i)),
            pl.BlockSpec(memory_space=pl.ANY),
        ],
        out_specs=pl.BlockSpec((tile // share, cut + EXTRA, share), lambda i: (i, 0, 0)),
        out_shape=jax.ShapeDtypeStruct((devices, cut + EXTRA, share), BF16),
        compiler_params=pltpu.CompilerParams(vmem_limit_bytes=VMEM_LIMIT),
        cost_estimate=pl.CostEstimate(
            flops=2 * cut * model * width, bytes_accessed=2 * (cut * model + model * width), transcendentals=0
        ),
        name="early_values",
    )(off_chip(rows), off_chip(rows), off_chip(rows), off_chip(wv), started)


def late_values_kernel(x_ref, before_ref, w_ref, _, *rest):
    outs, kept = rest[:-1], rest[-1]
    step = pl.program_id(0)
    share = kept.shape[2]
    devices = w_ref.shape[1] // share
    x = jnp.concatenate([x_ref[...], before_ref[...]], axis=0)
    y = jnp.dot(x, w_ref[...], preferred_element_type=F32)
    for device in range(devices):
        lanes = slice(device * share, (device + 1) * share)
        kept[step * devices + device] = y[:, lanes].astype(BF16)

    @pl.when(step == pl.num_programs(0) - 1)
    def _():
        own = lax.axis_index("sp")
        for offset, out in enumerate(outs):
            out[...] = kept[own ^ offset]


def late_values(rows, wv, started, devices, cut):
    span, model = rows.shape
    width = wv.shape[1]
    share = width // devices
    tile = max(2 * LANES, share)
    late = span - cut
    block = (late + EXTRA, share)
    return pl.pallas_call(
        late_values_kernel,
        grid=(width // tile,),
        in_specs=[
            pl.BlockSpec((late, model), lambda i: (cut // late, 0)),
            pl.BlockSpec((EXTRA, model), lambda i: (cut // EXTRA - 1, 0)),
            pl.BlockSpec((model, tile), lambda i: (0, i)),
            pl.BlockSpec(memory_space=pl.ANY),
        ],
        out_specs=[whole(block)] * devices,
        out_shape=[jax.ShapeDtypeStruct(block, BF16)] * devices,
        scratch_shapes=[pltpu.VMEM((devices,) + block, BF16)],
        compiler_params=pltpu.CompilerParams(vmem_limit_bytes=VMEM_LIMIT),
        cost_estimate=pl.CostEstimate(
            flops=2 * late * model * width, bytes_accessed=2 * (late * model + model * width), transcendentals=0
        ),
        name="late_values",
    )(off_chip(rows), off_chip(rows), off_chip(wv), started)


def key_read_kernel(
    group_devices, own_ref, *refs
):
    flips = GROUPS - 1
    direct, relayed = refs[:flips], refs[flips : flips + group_devices - 1]
    (
        taps_ref,
        query_ref,
        offset_ref,
        decay_ref,
        spikes_ref,
        keys_ref,
        weight_ref,
        blocks,
        line,
        rates,
        scores,
        spikes,
    ) = refs[flips + group_devices - 1 :]
    repeats = HEADS // GROUPS
    sources = blocks.shape[0]
    half = keys_ref.shape[1] // 2
    heads = spikes_ref.shape[1]
    tiles = 2 * half // LANES
    me = lax.axis_index("sp")
    group, rank = me // group_devices, me % group_devices
    for offset in range(GROUPS):
        block = own_ref[...] if offset == 0 else direct[offset - 1][...]
        blocks[(group ^ offset) * group_devices + rank] = block
        for shift in range(1, group_devices):
            blocks[(group ^ offset) * group_devices + (rank ^ shift)] = relayed[shift - 1][offset]
    taps = []
    for k in range(5):
        tap = taps_ref[k, pl.ds(group, 1), :]
        taps.append(jnp.concatenate([tap, tap], axis=1))
    asked = query_ref[0].astype(F32)
    asked = jnp.where(lax.broadcasted_iota(jnp.int32, asked.shape, 0) == group, asked, 0.0)
    asked = jnp.sum(asked, axis=0, keepdims=True)
    asked = jnp.broadcast_to(jnp.concatenate([asked, asked], axis=1), (16, LANES))
    part_row = lax.broadcasted_iota(jnp.int32, (16, LANES), 0)
    query = jnp.where(part_row == lane_index((16, LANES)) // STATE, asked, 0.0).astype(BF16)
    edge_left = lane_index((16, LANES)) < STATE
    left = lane_index((half, LANES)) < STATE
    picked = lax.broadcasted_iota(jnp.int32, (heads * tiles, repeats * tiles), 0)
    column = lax.broadcasted_iota(jnp.int32, (heads * tiles, repeats * tiles), 1)
    select = (column == (picked % tiles) * repeats + rank * heads + picked // tiles).astype(BF16)

    def one_source(source, carry):
        body = blocks[source, :half, :].astype(F32)
        before = blocks[jnp.maximum(source - 1, 0), half - 16 : half, :].astype(F32)
        after = blocks[jnp.minimum(source + 1, sources - 1), :16, :].astype(F32)
        before = jnp.where(source > 0, before, 0.0)
        after = jnp.where(source < sources - 1, after, 0.0)
        top = jnp.where(edge_left, pltpu.roll(before, STATE, 1), pltpu.roll(body[half - 16 :], STATE, 1))
        bottom = jnp.where(edge_left, pltpu.roll(body[:16], STATE, 1), pltpu.roll(after, STATE, 1))
        line[0:16, :] = top
        line[16 : 16 + half, :] = body
        line[16 + half :, :] = bottom
        total = taps[0] * line[14 : 14 + half, :]
        for k in range(1, 5):
            total = total + taps[k] * line[14 + k : 14 + k + half, :]
        y = silu(total).astype(BF16)
        score = lax.dot_general(query, y, (((1,), (1,)), ((), ())), preferred_element_type=F32)
        scores[source] = jnp.concatenate(
            [score[part : part + 1, c * LANES : (c + 1) * LANES] for part in range(2) for c in range(tiles // 2)],
            axis=0,
        )
        z = y.astype(F32)
        turned = pltpu.roll(z, STATE, 1)
        keys_ref[source, :half, :] = jnp.where(left, z, turned).astype(BF16)
        keys_ref[source, half:, :] = jnp.where(left, turned, z).astype(BF16)
        chosen = jnp.dot(select, blocks[source, half:, :], preferred_element_type=F32)
        for h in range(heads):
            rates[h, source] = chosen[h * tiles : (h + 1) * tiles]
        return carry

    lax.fori_loop(0, sources, one_source, 0)
    count = sources * tiles
    lane_row = lax.broadcasted_iota(jnp.int32, (LANES, LANES), 0)
    lane_col = lax.broadcasted_iota(jnp.int32, (LANES, LANES), 1)
    later_lanes = (lane_row > lane_col).astype(F32)
    row = lax.broadcasted_iota(jnp.int32, (count, count), 0)
    col = lax.broadcasted_iota(jnp.int32, (count, count), 1)
    later_rows = (col > row).astype(F32)
    score = scores[...].reshape(count, LANES)
    for h in range(heads):
        for c in range(count):
            spikes[h, c : c + 1, :] = spikes_ref[0, h : h + 1, c * LANES : (c + 1) * LANES]
    exact = dict(preferred_element_type=F32, precision=lax.Precision.HIGHEST)
    for h in range(heads):
        raw = rates[h].reshape(count, LANES) + offset_ref[h]
        rate = jnp.maximum(raw, 0.0) + jnp.log1p(jnp.exp(-jnp.abs(raw)))
        decay = jnp.exp(jnp.full((1, LANES), decay_ref[h], F32))
        step = spikes[h] - decay * rate
        within = jnp.dot(step, later_lanes, **exact)
        totals = jnp.broadcast_to(jnp.sum(step, axis=1, keepdims=True), (count, LANES))
        ahead = within + jnp.dot(later_rows, totals, **exact)
        weight = rate * jnp.exp(ahead) * score
        high = rounded(weight)
        weight_ref[:, h] = high.reshape(sources, tiles, LANES)
        weight_ref[:, heads + h] = (weight - high).reshape(sources, tiles, LANES)


def key_read(own, direct, relayed, taps, query, offset, decay, spikes, group_devices, span):
    sources = group_devices * GROUPS
    heads = offset.shape[0]
    half = span // 2
    tiles = span // LANES
    smem = pl.BlockSpec(memory_space=pltpu.SMEM)
    vmem = pl.BlockSpec(memory_space=pltpu.VMEM)
    count = 1 + len(direct) + len(relayed)
    return pl.pallas_call(
        lambda *refs: key_read_kernel(group_devices, *refs),
        in_specs=[vmem] * (count + 2) + [smem, smem, vmem],
        out_specs=[vmem, vmem],
        out_shape=[
            jax.ShapeDtypeStruct((sources, span, LANES), BF16),
            jax.ShapeDtypeStruct((sources, 2 * heads, tiles, LANES), F32),
        ],
        scratch_shapes=[
            pltpu.VMEM((sources,) + own.shape, BF16),
            pltpu.VMEM((half + 32, LANES), F32),
            pltpu.VMEM((heads, sources, tiles, LANES), F32),
            pltpu.VMEM((sources, tiles, LANES), F32),
            pltpu.VMEM((heads, sources * tiles, LANES), F32),
        ],
        compiler_params=pltpu.CompilerParams(vmem_limit_bytes=VMEM_LIMIT),
        cost_estimate=pl.CostEstimate(flops=10**9, bytes_accessed=4 * 10**6, transcendentals=10**6),
        name="key_read",
    )(*(on_chip(x) for x in [own, *direct, *relayed, taps, query]), offset, decay, on_chip(spikes))


def convolved(line, woven, body, before, after, taps_ref, keys_ref, weight_ref, source, start_row, out_ref, total):
    rows, share = body.shape
    heads = share // HEAD
    line[0:8, :] = before
    line[8 : 8 + rows, :] = body
    line[8 + rows :, :] = after
    taps = [jnp.concatenate([taps_ref[k, h : h + 1, :] for h in range(heads)], axis=1) for k in range(5)]
    left = lane_index((LANES, LANES)) < HEAD
    tiles = weight_ref.shape[2]
    weight = weight_ref[source].reshape(-1, LANES)
    tile_of = lax.broadcasted_iota(jnp.int32, weight.shape, 0) % tiles
    read = jnp.zeros(total.shape, F32)
    for tile in range(rows // LANES):
        start = tile * LANES
        y = taps[0] * line[6 + start : 6 + start + LANES, :]
        for k in range(1, 5):
            y = y + taps[k] * line[6 + k + start : 6 + k + start + LANES, :]
        y = silu(y).astype(BF16)
        keys = keys_ref[0, start : start + LANES, :].astype(F32)
        z = y.astype(F32)
        if share == LANES:
            pieces = [jnp.where(left, z, keys), jnp.where(left, pltpu.roll(z, HEAD, 1), keys)]
        else:
            pieces = [
                jnp.concatenate([z[:, h * HEAD : (h + 1) * HEAD], keys[:, STATE:]], axis=1) for h in range(heads)
            ]
        for h, piece in enumerate(pieces):
            woven[pl.ds(heads * start + h, LANES, heads), :] = piece
        masked = jnp.where(tile_of == start_row // LANES + tile, weight, 0.0).astype(BF16)
        read = read + jnp.dot(masked, y, preferred_element_type=F32)
        part = slice(heads * start, heads * (start + LANES))
        out_ref[0, part, :] = woven[part, :].astype(BF16)
    total[...] += read


def scratch_for(rows, share, reads):
    return [
        pltpu.VMEM((rows + 16, share), F32),
        pltpu.VMEM((share // HEAD * rows, LANES), F32),
        pltpu.VMEM((reads, share), F32),
    ]


def early_kernel(cut, block_ref, keys_ref, weight_ref, taps_ref, out_ref, read_ref, line, woven, total):
    source = pl.program_id(0)

    @pl.when(source == 0)
    def _():
        total[...] = jnp.zeros_like(total)

    block = block_ref[source].astype(F32)
    before = block_ref[jnp.maximum(source - 1, 0), cut : cut + EXTRA, :].astype(F32)[8:]
    before = jnp.where(source > 0, before, 0.0)
    convolved(
        line,
        woven,
        block[:cut],
        before,
        block[cut : cut + 8],
        taps_ref,
        keys_ref,
        weight_ref,
        source,
        0,
        out_ref,
        total,
    )
    read_ref[...] = total[...]


def early_rows(blocks, keys, weight, taps, cut):
    sources, _, share = blocks.shape
    span = keys.shape[1]
    heads = share // HEAD
    reads = weight.shape[1] * weight.shape[2]
    vmem = pl.BlockSpec(memory_space=pltpu.VMEM)
    return pl.pallas_call(
        lambda *refs: early_kernel(cut, *refs),
        grid=(sources,),
        in_specs=[vmem, pl.BlockSpec((1, cut, LANES), lambda s: (s, 0, 0)), vmem, vmem],
        out_specs=[pl.BlockSpec((1, heads * cut, LANES), lambda s: (s, 0, 0)), whole((reads, share))],
        out_shape=[
            jax.ShapeDtypeStruct((sources, heads * span, LANES), BF16),
            jax.ShapeDtypeStruct((reads, share), F32),
        ],
        scratch_shapes=scratch_for(cut, share, reads),
        compiler_params=pltpu.CompilerParams(vmem_limit_bytes=VMEM_LIMIT),
        cost_estimate=pl.CostEstimate(flops=2 * 10**9, bytes_accessed=6 * 10**6, transcendentals=10**6),
        name="early_rows",
    )(on_chip(blocks), keys, on_chip(weight), on_chip(taps))


def late_kernel(cut, last, order_ref, *refs):
    count = pl.num_programs(0)
    others = 13 if last else 11
    blocks, refs = refs[:-others], refs[-others:]
    early_ref, keys_ref, weight_ref, taps_ref, read_ref = refs[:5]
    gate_ref = refs[5] if last else None
    refs = refs[6 if last else 5 :]
    out_ref, read_out = refs[1], refs[2]
    square_ref = refs[3] if last else None
    line, woven, total = refs[-3:]
    step = pl.program_id(0)
    sources = early_ref.shape[0]
    rows, share = line.shape[0] - 16, line.shape[1]
    heads = share // HEAD

    @pl.when(step == 0)
    def _():
        total[...] = read_ref[...]

    for index, block_ref in enumerate(blocks):

        @pl.when(step == index)
        def _(block_ref=block_ref):
            source = order_ref[index]
            block = block_ref[...].astype(F32)
            after = early_ref[jnp.minimum(source + 1, sources - 1), :16, :].astype(F32)[:8]
            after = jnp.where(source < sources - 1, after, 0.0)
            convolved(
                line,
                woven,
                block[:rows],
                block[rows + 8 :],
                after,
                taps_ref,
                keys_ref,
                weight_ref,
                source,
                cut,
                out_ref,
                total,
            )

    @pl.when(step == count - 1)
    def _():
        if not last:
            read_out[...] = total[...]
            return
        tiles = weight_ref.shape[2]
        shape = total.shape
        head = (lax.broadcasted_iota(jnp.int32, shape, 0) // tiles) % heads
        mine = head == lane_index(shape) // HEAD
        read = jnp.sum(jnp.where(mine, total[...], 0.0), axis=0, keepdims=True)
        read = jnp.concatenate([read[:, h * HEAD : (h + 1) * HEAD] for h in range(heads)], axis=0)
        gated = read * silu(gate_ref[0].astype(F32))
        read_out[...] = gated
        square = jnp.sum(jnp.sum(gated * gated, axis=1, keepdims=True), axis=0, keepdims=True)
        square_ref[...] = jnp.broadcast_to(square, square_ref.shape)


def late_rows(offsets, late, early, keys, weight, taps, read, gate, out, cut, last):
    height, share = late[0].shape
    rows = height - EXTRA
    heads = share // HEAD
    place = cut // rows
    vmem = pl.BlockSpec(memory_space=pltpu.VMEM)
    near = [on_chip(x) for x in [late[k] for k in offsets] + [early]]
    far = [on_chip(x) for x in [weight, taps, read] + ([gate] if last else [])]
    inputs = near + [keys] + far
    order = lax.axis_index("sp") ^ jnp.array(offsets, jnp.int32)
    if last:
        small = [jax.ShapeDtypeStruct((heads, HEAD), F32), jax.ShapeDtypeStruct((1, LANES), F32)]
    else:
        small = [jax.ShapeDtypeStruct(read.shape, F32)]
    return pl.pallas_call(
        lambda *refs: late_kernel(cut, last, *refs),
        grid_spec=pltpu.PrefetchScalarGridSpec(
            num_scalar_prefetch=1,
            grid=(len(offsets),),
            in_specs=[vmem] * len(near)
            + [pl.BlockSpec((1, rows, LANES), lambda i, order: (order[i], place, 0))]
            + [vmem] * len(far)
            + [pl.BlockSpec(memory_space=pl.ANY)],
            out_specs=[pl.BlockSpec((1, heads * rows, LANES), lambda i, order: (order[i], place, 0))]
            + [whole(x.shape) for x in small],
            scratch_shapes=scratch_for(rows, share, read.shape[0]),
        ),
        out_shape=[jax.ShapeDtypeStruct(out.shape, BF16)] + small,
        input_output_aliases={len(inputs) + 1: 0},
        compiler_params=pltpu.CompilerParams(vmem_limit_bytes=VMEM_LIMIT),
        cost_estimate=pl.CostEstimate(flops=10**9, bytes_accessed=2 * 10**6, transcendentals=10**6),
        name="late_rows",
    )(order, *inputs, out)


def on_device(
    context_input_tensor,
    content_mapping_matrix,
    address_mapping_matrix,
    increment_mapping_matrix,
    increment_speed_offset,
    channel_fading_exponent,
    extra_damping_spikes,
    content_smoothing_coefficients,
    address_smoothing_coefficients,
    newest_lookup_matrix,
    newest_output_switch,
    cluster_scaling_coefficients,
):
    rows = context_input_tensor[0]
    span = rows.shape[0]
    repeats = HEADS // GROUPS
    heads = increment_speed_offset.shape[0]
    group_devices = repeats // heads
    devices = lax.axis_size("sp")
    cut = span // 2

    blocks = key_blocks(rows, address_mapping_matrix, increment_mapping_matrix.T, group_devices)
    direct = [None] * (GROUPS - 1)
    for offset in range(1, GROUPS):
        direct[offset - 1] = flip_permute(blocks[offset], offset * group_devices)
    early = early_values(rows, content_mapping_matrix, blocks[0], devices, cut)
    early_blocks = lax.all_to_all(early, "sp", 0, 0, tiled=True)
    late = late_values(rows, content_mapping_matrix, early, devices, cut)
    held = jnp.stack([blocks[0]] + direct)
    relayed = []
    for shift in range(1, group_devices):
        relayed.append(flip_permute(held, shift))
    late_blocks = [None] * devices
    late_blocks[0] = late[0]
    for offset in range(1, devices):
        late_blocks[offset] = flip_permute(late[offset], offset)

    keys, weight = key_read(
        blocks[0],
        direct,
        relayed,
        address_smoothing_coefficients,
        newest_lookup_matrix,
        increment_speed_offset,
        channel_fading_exponent,
        extra_damping_spikes,
        group_devices,
        span,
    )
    taps = content_smoothing_coefficients
    out, read = early_rows(early_blocks, keys, weight, taps, cut)
    half, quarter = devices // 2, devices // 4
    waves = (range(half), range(half + quarter, devices), range(half, half + quarter))
    for index, offsets in enumerate(waves):
        last = index == len(waves) - 1
        out, read, *square = late_rows(
            list(offsets), late_blocks, early_blocks, keys, weight, taps, read, newest_output_switch, out, cut, last
        )
    group_sq = square[0]
    for level in range(group_devices.bit_length() - 1):
        group_sq = group_sq + flip_permute(group_sq, 2**level)
    scaled = read * lax.rsqrt(group_sq[0, 0] / (repeats * HEAD) + EPS) * cluster_scaling_coefficients
    store = out.reshape(1, devices * span, heads, HEAD + STATE)
    return store, scaled.astype(BF16).reshape(1, heads, HEAD)


def solution(mesh):
    placed = (
        P(("gr", "tp"), "sp", None),
        P(),
        P(),
        P(),
        P("sp"),
        P("sp"),
        P(("gr", "tp"), "sp", None),
        P(None, "sp", None),
        P(),
        P(("gr", "tp"), None, None),
        P(("gr", "tp"), "sp", None),
        P("sp", None),
    )

    return jax.shard_map(
        on_device,
        mesh=mesh,
        in_specs=placed,
        out_specs=(P(("gr", "tp"), None, "sp", None), P(("gr", "tp"), "sp", None)),
        check_vma=False,
    )
```

profile of v0, /device:TPU:0, one launch (start us, length us, event | category | flops | bytes accessed | tf_op | source)
XLA Modules:
  0.0 104.2 jit_solution(4024749818585285274)
XLA Ops:
  0.6 0.8 copy-done.8
  1.5 4.6 %key_blocks.1 = (bf16[544,128]{1,0:T(8,128)(2,1)S(1)}, bf16[544,128]{1,0:T(8,128)(2,1)S(1)}, bf16[544,128]{1,0:T(8,128)(2,1)S(1)}, bf16[544,128]{1,0:T(8,128)(2,1)S(1)}) custom-call(bf16[1024,2048]{1,0:T(8,128)(2,1)} %bitcast.16, bf16[1024,2048]{1,0:T(8,128)(2,1)} %bitcast.17, bf16[2048,256]{1,0:T(8,128)(2,1)} %refs_2_.1, bf16[16,2048]{1,0:T(8,128)(2,1)S(1)} %bitcast.15), custom_call_target="tpu_custom_call" | custom-call | flops 1140850688 | bytes 4194304 | tf_op jit(solution)/shard_map/key_blocks/pallas_call | solution.py:101
  6.1 6.4 %early_values.1._ = bf16[8,528,128]{2,1,0:T(8,128)(2,1)} custom-call(bf16[1024,2048]{1,0:T(8,128)(2,1)} %bitcast.18, bf16[1024,2048]{1,0:T(8,128)(2,1)} %bitcast.19, bf16[1024,2048]{1,0:T(8,128)(2,1)} %bitcast.20, bf16[2048,1024]{1,0:T(8,128)(2,1)} %w_ref.3, bf16[544,128]{1,0:T(8,128)(2,1)S(1)} %get-tuple-element.25._.refs_0_), custom_call_target="tpu_custom_call" | custom-call | flops 2147483648 | bytes 6291456 | tf_op jit(solution)/shard_map/early_values/pallas_call | solution.py:141
  12.4 7.3 %all-to-all-start = ((bf16[8,528,128]{2,1,0:T(8,128)(2,1)}), bf16[8,528,128]{2,1,0:T(8,128)(2,1)S(1)}, u32[]{:S(2)}, u32[]{:S(2)}) async-start(bf16[8,528,128]{2,1,0:T(8,128)(2,1)} %early_values.1._), calls=%async_computation | async-start | bytes 2162688 | tf_op jit(solution)/shard_map/all_to_all | solution.py:551
  19.8 2.0 %collective-permute-start.2 = (bf16[544,128]{1,0:T(8,128)(2,1)S(1)}, bf16[544,128]{1,0:T(8,128)(2,1)S(1)}, u32[]{:S(2)}, u32[]{:S(2)}) collective-permute-start(bf16[544,128]{1,0:T(8,128)(2,1)S(1)} %get-tuple-element.28), channel_id=1, source_target_pairs={{0,4},{2,6},{4,0},{6,2},{8,12},{10,14},{12,8},{14,10},{1,5},{3,7},... | collective-permute-start | bytes 417800 | tf_op jit(solution)/shard_map/ppermute | solution.py:47
  21.8 2.4 %collective-permute-start.3 = (bf16[544,128]{1,0:T(8,128)(2,1)S(1)}, bf16[544,128]{1,0:T(8,128)(2,1)S(1)}, u32[]{:S(2)}, u32[]{:S(2)}) collective-permute-start(bf16[544,128]{1,0:T(8,128)(2,1)S(1)} %get-tuple-element.29), channel_id=1, source_target_pairs={{0,8},{2,10},{4,12},{6,14},{8,0},{10,2},{12,4},{14,6},{1,9},{3,11}... | collective-permute-start | bytes 417800 | tf_op jit(solution)/shard_map/ppermute | solution.py:47
  24.3 6.4 %late_values.1 = (bf16[528,128]{1,0:T(8,128)(2,1)S(1)}, bf16[528,128]{1,0:T(8,128)(2,1)}, bf16[528,128]{1,0:T(8,128)(2,1)}, bf16[528,128]{1,0:T(8,128)(2,1)}, bf...) custom-call(bf16[1024,2048]{1,0:T(8,128)(2,1)} %bitcast.21, ...), custom_call_target="tpu_custom_call" | custom-call | flops 2147483648 | bytes 6291456 | tf_op jit(solution)/shard_map/late_values/pallas_call | solution.py:186
  30.7 0.6 copy-done.6
  31.4 0.7 copy-done.11
  32.0 0.7 copy-done.13
  32.7 2.0 %collective-permute-start.10 = (bf16[528,128]{1,0:T(8,128)(2,1)}, bf16[528,128]{1,0:T(8,128)(2,1)}, u32[]{:S(2)}, u32[]{:S(2)}) collective-permute-start(bf16[528,128]{1,0:T(8,128)(2,1)} %get-tuple-element.38), channel_id=1, source_target_pairs={{0,6},{2,4},{4,2},{6,0},{8,14},{10,12},{12,10},{14,8},{1,7},{3,5},... | collective-permute-start | bytes 405512 | tf_op jit(solution)/shard_map/ppermute | solution.py:47
  35.2 6.4 %collective-permute-done.2.refs_1_ = bf16[544,128]{1,0:T(8,128)(2,1)S(1)} collective-permute-done((bf16[544,128]{1,0:T(8,128)(2,1)S(1)}, bf16[544,128]{1,0:T(8,128)(2,1)S(1)}, u32[]{:S(2)}, u32[]{:S(2)}) %collective-permute-start.2) | collective-permute-done | bytes 139296 | tf_op jit(solution)/shard_map/ppermute | solution.py:47
  41.6 2.5 %collective-permute-start.9 = (bf16[528,128]{1,0:T(8,128)(2,1)}, bf16[528,128]{1,0:T(8,128)(2,1)}, u32[]{:S(2)}, u32[]{:S(2)}) collective-permute-start(bf16[528,128]{1,0:T(8,128)(2,1)} %get-tuple-element.37), channel_id=1, source_target_pairs={{0,4},{2,6},{4,0},{6,2},{8,12},{10,14},{12,8},{14,10},{1,5},{3,7},... | collective-permute-start | bytes 405512 | tf_op jit(solution)/shard_map/ppermute | solution.py:47
  44.1 12.4 %collective-permute-done.3.refs_2_ = bf16[544,128]{1,0:T(8,128)(2,1)S(1)} collective-permute-done((bf16[544,128]{1,0:T(8,128)(2,1)S(1)}, bf16[544,128]{1,0:T(8,128)(2,1)S(1)}, u32[]{:S(2)}, u32[]{:S(2)}) %collective-permute-start.3) | collective-permute-done | bytes 139296 | tf_op jit(solution)/shard_map/ppermute | solution.py:47
  56.7 1.7 %collective-permute-start.5 = (bf16[4,544,128]{2,1,0:T(8,128)(2,1)S(1)}, bf16[4,544,128]{2,1,0:T(8,128)(2,1)S(1)}, u32[]{:S(2)}, u32[]{:S(2)}) collective-permute-start(bf16[4,544,128]{2,1,0:T(8,128)(2,1)S(1)} %pad_maximum_fusion), channel_id=1, source_target_pairs={{0,2},{2,0},{4,6},{6,4},{8,10},{10,8},{12,14},{14,12},{1,3},{3,1},... | collective-permute-start | bytes 1671176 | tf_op jit(solution)/shard_map/ppermute | solution.py:47
  58.4 12.5 %collective-permute-done.5.refs_4_ = bf16[4,544,128]{2,1,0:T(8,128)(2,1)S(1)} collective-permute-done((bf16[4,544,128]{2,1,0:T(8,128)(2,1)S(1)}, bf16[4,544,128]{2,1,0:T(8,128)(2,1)S(1)}, u32[]{:S(2)}, u32[]{:S(2)}) %collective-permute-start.5) | collective-permute-done | bytes 557088 | tf_op jit(solution)/shard_map/ppermute | solution.py:47
  70.9 2.6 %collective-permute-start.7 = (bf16[528,128]{1,0:T(8,128)(2,1)}, bf16[528,128]{1,0:T(8,128)(2,1)}, u32[]{:S(2)}, u32[]{:S(2)}) collective-permute-start(bf16[528,128]{1,0:T(8,128)(2,1)} %get-tuple-element.34), channel_id=1, source_target_pairs={{0,14},{2,12},{4,10},{6,8},{8,6},{10,4},{12,2},{14,0},{1,15},{3,13... | collective-permute-start | bytes 405512 | tf_op jit(solution)/shard_map/ppermute | solution.py:47
  73.5 0.9 copy-done.1
  74.4 0.9 copy-done.3
  75.3 0.9 copy-done.5
  76.2 0.7 copy-done.19
  76.9 3.6 %key_read.1 = (bf16[8,1024,128]{2,1,0:T(8,128)(2,1)S(1)}, f32[8,4,8,128]{3,2,1,0:T(8,128)S(1)}) custom-call(bf16[544,128]{1,0:T(8,128)(2,1)S(1)} %get-tuple-element.25._.refs_0_, bf16[544,128]{1,0:T(8,128)(2,1)S(1)} %copy-done.1, bf16[544,128]{1,0:T(8,128)(2,1)S(1)} %copy-done.3, bf16[544,128]{1,0:T(8,128)(2,1)S(1)} %copy-done.5, ...), custom_call_target="tpu_custom_call" | custom-call | flops 1000000000 | bytes 4000000 | tf_op jit(solution)/shard_map/key_read/pallas_call | solution.py:317
  80.5 4.6 %early_rows.1 = (bf16[8,2048,128]{2,1,0:T(8,128)(2,1)}, f32[32,128]{1,0:T(8,128)S(1)}) custom-call(bf16[8,528,128]{2,1,0:T(8,128)(2,1)S(1)} %all-to-all-done.refs_0_.refs_5_.refs_3_, bf16[8,1024,128]{2,1,0:T(8,128)(2,1)S(1)} %get-tuple-element.31.refs_1_.refs_6_.refs_4_, f32[8,4,8,128]{3,2,1,0:T(8,128)S(1)} %get-tuple-element.32.refs_2_.refs_7_.refs_5_, ...), custom_call_target="tpu_custom_call" | custom-call | flops 2000000000 | bytes 6000000 | tf_op jit(solution)/shard_map/early_rows/pallas_call | solution.py:414
  85.2 1.5 %collective-permute-start = (bf16[528,128]{1,0:T(8,128)(2,1)S(1)}, bf16[528,128]{1,0:T(8,128)(2,1)S(1)}, u32[]{:S(2)}, u32[]{:S(2)}) collective-permute-start(bf16[528,128]{1,0:T(8,128)(2,1)S(1)} %copy-done.14), channel_id=1, source_target_pairs={{0,8},{2,10},{4,12},{6,14},{8,0},{10,2},{12,4},{14,6},{1,9},{3,11}... | collective-permute-start | bytes 405512 | tf_op jit(solution)/shard_map/ppermute | solution.py:47
  86.7 1.2 %collective-permute-start.1 = (bf16[528,128]{1,0:T(8,128)(2,1)S(1)}, bf16[528,128]{1,0:T(8,128)(2,1)S(1)}, u32[]{:S(2)}, u32[]{:S(2)}) collective-permute-start(bf16[528,128]{1,0:T(8,128)(2,1)S(1)} %copy-done.12), channel_id=1, source_target_pairs={{0,10},{2,8},{4,14},{6,12},{8,2},{10,0},{12,6},{14,4},{1,11},{3,9}... | collective-permute-start | bytes 405512 | tf_op jit(solution)/shard_map/ppermute | solution.py:47
  87.8 4.2 %late_rows.3 = (bf16[8,2048,128]{2,1,0:T(8,128)(2,1)}, f32[32,128]{1,0:T(8,128)S(1)}) custom-call(s32[4]{0:T(128)S(1)} %iota_xor_fusion.refs_0_, bf16[528,128]{1,0:T(8,128)(2,1)S(1)} %copy-done.7, bf16[528,128]{1,0:T(8,128)(2,1)} %collective-permute-done.8.refs_2_, ...), custom_call_target="tpu_custom_call", output_to_operand_aliasing={{0}: (10, {})} | custom-call | flops 1000000000 | bytes 2000000 | tf_op jit(solution)/shard_map/late_rows/pallas_call | solution.py:503
  92.0 3.0 %late_rows.4 = (bf16[8,2048,128]{2,1,0:T(8,128)(2,1)}, f32[32,128]{1,0:T(8,128)S(1)}) custom-call(s32[2]{0:T(128)S(1)} %broadcast_xor_fusion.refs_0_, bf16[528,128]{1,0:T(8,128)(2,1)} %collective-permute-done.6.refs_1_, bf16[528,128]{1,0:T(8,128)(2,1)} %collective-permute-done.7.refs_2_, ...), custom_call_target="tpu_custom_call", output_to_operand_aliasing={{0}: (8, {})} | custom-call | flops 1000000000 | bytes 2000000 | tf_op jit(solution)/shard_map/late_rows/pallas_call | solution.py:503
  95.1 1.8 %collective-permute-done.refs_1_ = bf16[528,128]{1,0:T(8,128)(2,1)S(1)} collective-permute-done((bf16[528,128]{1,0:T(8,128)(2,1)S(1)}, bf16[528,128]{1,0:T(8,128)(2,1)S(1)}, u32[]{:S(2)}, u32[]{:S(2)}) %collective-permute-start) | collective-permute-done | bytes 135200 | tf_op jit(solution)/shard_map/ppermute | solution.py:47
  96.9 0.8 collective-permute-done.1.refs_2_
  97.7 2.2 %late_rows.5 = (bf16[8,2048,128]{2,1,0:T(8,128)(2,1)}, f32[2,64]{1,0:T(2,128)S(1)}, f32[1,128]{1,0:T(1,128)S(1)}) custom-call(s32[2]{0:T(128)S(1)} %broadcast_xor_fusion.1.refs_0_, bf16[528,128]{1,0:T(8,128)(2,1)S(1)} %collective-permute-done.refs_1_, bf16[528,128]{1,0:T(8,128)(2,1)S(1)} %collective-permute-done.1.refs_2_, ...), custom_call_target="tpu_custom_call", output_to_operand_aliasing={{0}: (9, {})} | custom-call | flops 1000000000 | bytes 2000000 | tf_op jit(solution)/shard_map/late_rows/pallas_call | solution.py:503
  99.9 2.1 %collective-permute-start.11 = (f32[1,128]{1,0:T(1,128)S(1)}, f32[1,128]{1,0:T(1,128)S(1)}, u32[]{:S(2)}, u32[]{:S(2)}) collective-permute-start(f32[1,128]{1,0:T(1,128)S(1)} %get-tuple-element.47), channel_id=1, source_target_pairs={{0,2},{2,0},{4,6},{6,4},{8,10},{10,8},{12,14},{14,12},{1,3},{3,1},... | collective-permute-start | bytes 1544 | tf_op jit(solution)/shard_map/ppermute | solution.py:47
  102.0 1.5 %collective-permute-done.11 = f32[1,128]{1,0:T(1,128)S(1)} collective-permute-done((f32[1,128]{1,0:T(1,128)S(1)}, f32[1,128]{1,0:T(1,128)S(1)}, u32[]{:S(2)}, u32[]{:S(2)}) %collective-permute-start.11) | collective-permute-done | bytes 544 | tf_op jit(solution)/shard_map/ppermute | solution.py:47
  (54 shorter events, 1.4 us)
Async XLA Ops:
  0.6 0.8 copy-start.8
  12.4 68.1 %all-to-all-start = ((bf16[8,528,128]{2,1,0:T(8,128)(2,1)}), bf16[8,528,128]{2,1,0:T(8,128)(2,1)S(1)}, u32[]{:S(2)}, u32[]{:S(2)}) async-start(bf16[8,528,128]{2,1,0:T(8,128)(2,1)} %early_values.1._), calls=%async_computation | async-start | bytes 2162688 | tf_op jit(solution)/shard_map/all_to_all | solution.py:551
  19.8 21.9 %collective-permute-start.2 = (bf16[544,128]{1,0:T(8,128)(2,1)S(1)}, bf16[544,128]{1,0:T(8,128)(2,1)S(1)}, u32[]{:S(2)}, u32[]{:S(2)}) collective-permute-start(bf16[544,128]{1,0:T(8,128)(2,1)S(1)} %get-tuple-element.28), channel_id=1, source_target_pairs={{0,4},{2,6},{4,0},{6,2},{8,12},{10,14},{12,8},{14,10},{1,5},{3,7},... | collective-permute-start | bytes 417800 | tf_op jit(solution)/shard_map/ppermute | solution.py:47
  21.8 34.8 %collective-permute-start.3 = (bf16[544,128]{1,0:T(8,128)(2,1)S(1)}, bf16[544,128]{1,0:T(8,128)(2,1)S(1)}, u32[]{:S(2)}, u32[]{:S(2)}) collective-permute-start(bf16[544,128]{1,0:T(8,128)(2,1)S(1)} %get-tuple-element.29), channel_id=1, source_target_pairs={{0,8},{2,10},{4,12},{6,14},{8,0},{10,2},{12,4},{14,6},{1,9},{3,11}... | collective-permute-start | bytes 417800 | tf_op jit(solution)/shard_map/ppermute | solution.py:47
  24.1 34.3 %copy-start.22 = (s32[2]{0:T(128)S(1)}, s32[2]{0:T(128)}, u32[]{:S(2)}) copy-start(s32[2]{0:T(128)} %constant.19.clone) | copy-start | bytes 28
  24.1 34.3 %copy-start.21 = (s32[2]{0:T(128)S(1)}, s32[2]{0:T(128)}, u32[]{:S(2)}) copy-start(s32[2]{0:T(128)} %constant.20.clone) | copy-start | bytes 28
  24.2 49.4 %copy-start.15 = (f32[1,2,8192]{2,1,0:T(2,128)S(1)}, f32[1,2,8192]{2,1,0:T(2,128)}, u32[]{:S(2)}) copy-start(f32[1,2,8192]{2,1,0:T(2,128)} %refs_9_.1) | copy-start | bytes 196612
  24.2 49.4 %copy-start.16 = (f32[5,4,64]{2,1,0:T(4,128)S(1)}, f32[5,4,64]{2,1,0:T(4,128)}, u32[]{:S(2)}) copy-start(f32[5,4,64]{2,1,0:T(4,128)} %refs_5_.1) | copy-start | bytes 15364
  24.2 49.3 %copy-start.17 = (bf16[1,4,64]{2,1,0:T(4,128)(2,1)S(1)}, bf16[1,4,64]{2,1,0:T(4,128)(2,1)}, u32[]{:S(2)}) copy-start(bf16[1,4,64]{2,1,0:T(4,128)(2,1)} %refs_6_.3) | copy-start | bytes 1540
  24.2 49.3 %copy-start.18 = (f32[2]{0:T(128)S(1)}, f32[2]{0:T(128)}, u32[]{:S(2)}) copy-start(f32[2]{0:T(128)} %refs_7_.1) | copy-start | bytes 28
  24.2 32.4 %collective-permute-start.4 = (bf16[544,128]{1,0:T(8,128)(2,1)S(1)}, bf16[544,128]{1,0:T(8,128)(2,1)S(1)}, u32[]{:S(2)}, u32[]{:S(2)}) collective-permute-start(bf16[544,128]{1,0:T(8,128)(2,1)S(1)} %get-tuple-element.30), channel_id=1, source_target_pairs={{0,12},{2,14},{4,8},{6,10},{8,4},{10,6},{12,0},{14,2},{1,13},{3,15... | collective-permute-start | bytes 417800 | tf_op jit(solution)/shard_map/ppermute | solution.py:47
  32.7 47.9 %copy-start.9 = (f32[5,2,64]{2,1,0:T(2,128)S(1)}, f32[5,2,64]{2,1,0:T(2,128)}, u32[]{:S(2)}) copy-start(f32[5,2,64]{2,1,0:T(2,128)} %refs_6_.5) | copy-start | bytes 7684
  32.7 52.5 %collective-permute-start.10 = (bf16[528,128]{1,0:T(8,128)(2,1)}, bf16[528,128]{1,0:T(8,128)(2,1)}, u32[]{:S(2)}, u32[]{:S(2)}) collective-permute-start(bf16[528,128]{1,0:T(8,128)(2,1)} %get-tuple-element.38), channel_id=1, source_target_pairs={{0,6},{2,4},{4,2},{6,0},{8,14},{10,12},{12,10},{14,8},{1,7},{3,5},... | collective-permute-start | bytes 405512 | tf_op jit(solution)/shard_map/ppermute | solution.py:47
  34.7 52.0 %collective-permute-start.8 = (bf16[528,128]{1,0:T(8,128)(2,1)}, bf16[528,128]{1,0:T(8,128)(2,1)}, u32[]{:S(2)}, u32[]{:S(2)}) collective-permute-start(bf16[528,128]{1,0:T(8,128)(2,1)} %get-tuple-element.36), channel_id=1, source_target_pairs={{0,2},{2,0},{4,6},{6,4},{8,10},{10,8},{12,14},{14,12},{1,3},{3,1},... | collective-permute-start | bytes 405512 | tf_op jit(solution)/shard_map/ppermute | solution.py:47
  41.6 29.3 %copy-start = (bf16[544,128]{1,0:T(8,128)(2,1)}, bf16[544,128]{1,0:T(8,128)(2,1)S(1)}, u32[]{:S(2)}) copy-start(bf16[544,128]{1,0:T(8,128)(2,1)S(1)} %collective-permute-done.2.refs_1_) | copy-start | bytes 417796
  41.6 46.2 %collective-permute-start.9 = (bf16[528,128]{1,0:T(8,128)(2,1)}, bf16[528,128]{1,0:T(8,128)(2,1)}, u32[]{:S(2)}, u32[]{:S(2)}) collective-permute-start(bf16[528,128]{1,0:T(8,128)(2,1)} %get-tuple-element.37), channel_id=1, source_target_pairs={{0,4},{2,6},{4,0},{6,2},{8,12},{10,14},{12,8},{14,10},{1,5},{3,7},... | collective-permute-start | bytes 405512 | tf_op jit(solution)/shard_map/ppermute | solution.py:47
  56.6 14.4 %copy-start.2 = (bf16[544,128]{1,0:T(8,128)(2,1)}, bf16[544,128]{1,0:T(8,128)(2,1)S(1)}, u32[]{:S(2)}) copy-start(bf16[544,128]{1,0:T(8,128)(2,1)S(1)} %collective-permute-done.3.refs_2_) | copy-start | bytes 417796
  56.6 35.5 %collective-permute-start.6 = (bf16[528,128]{1,0:T(8,128)(2,1)}, bf16[528,128]{1,0:T(8,128)(2,1)}, u32[]{:S(2)}, u32[]{:S(2)}) collective-permute-start(bf16[528,128]{1,0:T(8,128)(2,1)} %get-tuple-element.33), channel_id=1, source_target_pairs={{0,12},{2,14},{4,8},{6,10},{8,4},{10,6},{12,0},{14,2},{1,13},{3,15... | collective-permute-start | bytes 405512 | tf_op jit(solution)/shard_map/ppermute | solution.py:47
  56.6 14.3 %copy-start.4 = (bf16[544,128]{1,0:T(8,128)(2,1)}, bf16[544,128]{1,0:T(8,128)(2,1)S(1)}, u32[]{:S(2)}) copy-start(bf16[544,128]{1,0:T(8,128)(2,1)S(1)} %collective-permute-done.4.refs_3_) | copy-start | bytes 417796
  56.7 14.2 %collective-permute-start.5 = (bf16[4,544,128]{2,1,0:T(8,128)(2,1)S(1)}, bf16[4,544,128]{2,1,0:T(8,128)(2,1)S(1)}, u32[]{:S(2)}, u32[]{:S(2)}) collective-permute-start(bf16[4,544,128]{2,1,0:T(8,128)(2,1)S(1)} %pad_maximum_fusion), channel_id=1, source_target_pairs={{0,2},{2,0},{4,6},{6,4},{8,10},{10,8},{12,14},{14,12},{1,3},{3,1},... | collective-permute-start | bytes 1671176 | tf_op jit(solution)/shard_map/ppermute | solution.py:47
  70.9 21.1 %collective-permute-start.7 = (bf16[528,128]{1,0:T(8,128)(2,1)}, bf16[528,128]{1,0:T(8,128)(2,1)}, u32[]{:S(2)}, u32[]{:S(2)}) collective-permute-start(bf16[528,128]{1,0:T(8,128)(2,1)} %get-tuple-element.34), channel_id=1, source_target_pairs={{0,14},{2,12},{4,10},{6,8},{8,6},{10,4},{12,2},{14,0},{1,15},{3,13... | collective-permute-start | bytes 405512 | tf_op jit(solution)/shard_map/ppermute | solution.py:47
  73.5 0.9 copy-start.1
  74.4 0.9 copy-start.3
  75.3 0.9 copy-start.5
  80.5 7.4 %copy-start.7 = (bf16[528,128]{1,0:T(8,128)(2,1)S(1)}, bf16[528,128]{1,0:T(8,128)(2,1)}, u32[]{:S(2)}) copy-start(bf16[528,128]{1,0:T(8,128)(2,1)} %copy-done.6) | copy-start | bytes 405508
  80.5 4.7 %copy-start.14 = (bf16[528,128]{1,0:T(8,128)(2,1)S(1)}, bf16[528,128]{1,0:T(8,128)(2,1)}, u32[]{:S(2)}) copy-start(bf16[528,128]{1,0:T(8,128)(2,1)} %copy-done.13) | copy-start | bytes 405508
  80.5 6.1 %copy-start.12 = (bf16[528,128]{1,0:T(8,128)(2,1)S(1)}, bf16[528,128]{1,0:T(8,128)(2,1)}, u32[]{:S(2)}) copy-start(bf16[528,128]{1,0:T(8,128)(2,1)} %copy-done.11) | copy-start | bytes 405508
  85.2 11.7 %collective-permute-start = (bf16[528,128]{1,0:T(8,128)(2,1)S(1)}, bf16[528,128]{1,0:T(8,128)(2,1)S(1)}, u32[]{:S(2)}, u32[]{:S(2)}) collective-permute-start(bf16[528,128]{1,0:T(8,128)(2,1)S(1)} %copy-done.14), channel_id=1, source_target_pairs={{0,8},{2,10},{4,12},{6,14},{8,0},{10,2},{12,4},{14,6},{1,9},{3,11}... | collective-permute-start | bytes 405512 | tf_op jit(solution)/shard_map/ppermute | solution.py:47
  86.7 11.0 %collective-permute-start.1 = (bf16[528,128]{1,0:T(8,128)(2,1)S(1)}, bf16[528,128]{1,0:T(8,128)(2,1)S(1)}, u32[]{:S(2)}, u32[]{:S(2)}) collective-permute-start(bf16[528,128]{1,0:T(8,128)(2,1)S(1)} %copy-done.12), channel_id=1, source_target_pairs={{0,10},{2,8},{4,14},{6,12},{8,2},{10,0},{12,6},{14,4},{1,11},{3,9}... | collective-permute-start | bytes 405512 | tf_op jit(solution)/shard_map/ppermute | solution.py:47
  92.0 5.7 %copy-start.10 = (bf16[1,2,64]{2,1,0:T(2,128)(2,1)S(1)}, bf16[1,2,64]{2,1,0:T(2,128)(2,1)}, u32[]{:S(2)}) copy-start(bf16[1,2,64]{2,1,0:T(2,128)(2,1)} %refs_8_.5) | copy-start | bytes 772
  95.0 8.6 %copy-start.20 = (f32[2,64]{1,0:T(2,128)S(1)}, f32[2,64]{1,0:T(2,128)}, u32[]{:S(2)}) copy-start(f32[2,64]{1,0:T(2,128)} %param.26) | copy-start | bytes 1540
  99.9 3.7 %collective-permute-start.11 = (f32[1,128]{1,0:T(1,128)S(1)}, f32[1,128]{1,0:T(1,128)S(1)}, u32[]{:S(2)}, u32[]{:S(2)}) collective-permute-start(f32[1,128]{1,0:T(1,128)S(1)} %get-tuple-element.47), channel_id=1, source_target_pairs={{0,2},{2,0},{4,6},{6,4},{8,10},{10,8},{12,14},{14,12},{1,3},{3,1},... | collective-permute-start | bytes 1544 | tf_op jit(solution)/shard_map/ppermute | solution.py:47
  (4 other events, 2.6 us)
where the time goes:
time: 105 us; the launch traced here: 104 us
  waiting for transfers between devices  35.5 us (34%)
  Pallas kernels  35 us (33%)
  starting transfers between devices  25.9 us (25%)
  local copies, waits for them, and re-layouts  6.24 us (6%)
    ppermute x12, waiting for transfers between devices, flip_permute(): return lax.ppermute(value, 'sp', pairs)  35.5 us
    ppermute x12, starting transfers between devices, flip_permute(): return lax.ppermute(value, 'sp', pairs)  18.6 us
    pallas_call x3, Pallas kernels, late_rows(): pl.pallas_call(lambda *refs: late_kernel(cut, last, *refs), grid_spec=plt...  9.38 us
    all_to_all x1, starting transfers between devices, on_device(): early_blocks = lax.all_to_all(early, 'sp', 0, 0, tiled=True)  7.31 us
    pallas_call x1, Pallas kernels, late_values(): pl.pallas_call(late_values_kernel, grid=(width // tile,), in_specs=[pl.Bl...  6.44 us
    pallas_call x1, Pallas kernels, early_values(): pl.pallas_call(early_values_kernel, grid=(width // tile,), in_specs=[whol...  6.37 us
    unnamed x46, local copies, waits for them, and re-layouts  6.24 us
    pallas_call x1, Pallas kernels, early_rows(): pl.pallas_call(lambda *refs: early_kernel(cut, *refs), grid=(sources,), i...  4.64 us
  transfers between devices with their start and end apart: 13, of which 6 were waited for; matrix products, arithmetic and copies ran while one was open for 0% of the time, Pallas kernels for 21%

commit v1 on v0

v1 whole, which is shorter than its diff:
```python
import jax
import jax.numpy as jnp
from jax import lax
from jax.experimental import pallas as pl
from jax.experimental.pallas import tpu as pltpu
from jax.sharding import PartitionSpec as P


HEADS = 16
HEAD = 64
GROUPS = 4
STATE = 64
LANES = 128
EXTRA = 8
TILE_ROWS = 16
VMEM_LIMIT = 24 * 2**20
EPS = 1e-05
F32 = jnp.float32
BF16 = jnp.bfloat16


def silu(x):
    return 0.5 * x * (1.0 + jnp.tanh(0.5 * x))


def rounded(x):
    return x.astype(BF16).astype(F32)


def lane_index(shape):
    return lax.broadcasted_iota(jnp.int32, shape, 1)


def whole(shape):
    return pl.BlockSpec(shape, lambda *_: (0,) * len(shape))


def on_chip(x):
    return pltpu.with_memory_space_constraint(x, pltpu.VMEM)


def off_chip(x):
    return pltpu.with_memory_space_constraint(x, pltpu.HBM)


def flip_permute(value, flip):
    pairs = [(source, source ^ flip) for source in range(lax.axis_size("sp"))]
    return lax.ppermute(value, "sp", pairs)


def key_block_kernel(group_devices, low_ref, high_ref, wk_ref, wr_ref, *rest):
    outs, (packed, rates) = rest[:-2], rest[-2:]
    repeats = HEADS // GROUPS
    step = pl.program_id(0)
    rows = low_ref.shape[0]
    tiles = rows // LANES
    half_tiles = rates.shape[0] // 2
    wk, wr = wk_ref[...], wr_ref[...]
    both = jnp.concatenate([low_ref[...], high_ref[...]], axis=0)
    k_both = rounded(jnp.dot(both, wk, preferred_element_type=F32))
    k_low, k_high = k_both[:rows], k_both[rows:]
    r_both = lax.dot_general(both, wr, (((1,), (1,)), ((), ())), preferred_element_type=F32).astype(BF16)
    left = lane_index((rows, LANES)) < STATE
    for group in range(GROUPS):
        column = slice(group // 2 * LANES, (group // 2 + 1) * LANES)
        a, b = k_low[:, column], k_high[:, column]
        if group % 2 == 0:
            b = pltpu.roll(b, STATE, 1)
        else:
            a = pltpu.roll(a, STATE, 1)
        packed[group, pl.ds(pl.multiple_of(step * rows, rows), rows), :] = jnp.where(left, a, b).astype(BF16)
    eye = (
        lax.broadcasted_iota(jnp.int32, (HEADS, HEADS), 0) == lax.broadcasted_iota(jnp.int32, (HEADS, HEADS), 1)
    ).astype(BF16)
    for part in range(2):
        r = r_both[part * rows : (part + 1) * rows]
        turned = lax.dot_general(eye, r, (((1,), (1,)), ((), ())), preferred_element_type=F32)
        for tile in range(tiles):
            rates[part * half_tiles + step * tiles + tile] = turned[:, tile * LANES : (tile + 1) * LANES]

    @pl.when(step == pl.num_programs(0) - 1)
    def _():
        half = packed.shape[1] - 2 * half_tiles * repeats
        for group in range(GROUPS):
            tail = jnp.concatenate(
                [rates[tile, group * repeats : (group + 1) * repeats, :] for tile in range(2 * half_tiles)], axis=0
            )
            packed[group, half:, :] = tail.astype(BF16)
        own = lax.axis_index("sp") // group_devices
        for offset, out in enumerate(outs):
            out[...] = packed[own ^ offset]


def key_blocks(rows, wk, wr, group_devices):
    span, model = rows.shape
    repeats = HEADS // GROUPS
    half = span // 2
    tile = half // 2
    steps = half // tile
    height = half + repeats * span // LANES
    block = jax.ShapeDtypeStruct((height, LANES), BF16)
    return pl.pallas_call(
        lambda *refs: key_block_kernel(group_devices, *refs),
        grid=(steps,),
        in_specs=[
            pl.BlockSpec((tile, model), lambda i: (i, 0)),
            pl.BlockSpec((tile, model), lambda i: (i + steps, 0)),
            whole(wk.shape),
            whole(wr.shape),
        ],
        out_specs=[whole((height, LANES))] * GROUPS,
        out_shape=[block] * GROUPS,
        scratch_shapes=[
            pltpu.VMEM((GROUPS, height, LANES), BF16),
            pltpu.VMEM((span // LANES, HEADS, LANES), F32),
        ],
        compiler_params=pltpu.CompilerParams(vmem_limit_bytes=VMEM_LIMIT),
        cost_estimate=pl.CostEstimate(
            flops=2 * span * model * (GROUPS * STATE + HEADS), bytes_accessed=2 * span * model, transcendentals=0
        ),
        name="key_blocks",
    )(off_chip(rows), off_chip(rows), off_chip(wk), off_chip(wr))


def value_kernel(x_refs, w_ref, outs, kept):
    step = pl.program_id(0)
    share = kept.shape[2]
    devices = w_ref.shape[1] // share
    rows = x_refs[0].shape[0]
    x = jnp.concatenate([ref[...] for ref in x_refs], axis=0) if len(x_refs) > 1 else x_refs[0][...]
    y = jnp.dot(x, w_ref[...], preferred_element_type=F32)
    for device in range(devices):
        lanes = slice(device * share, (device + 1) * share)
        index = step * devices + device
        kept[index, :rows, :] = y[:rows, lanes].astype(BF16)
        if len(x_refs) > 1:
            half = EXTRA // 2
            last = y.shape[0]
            extra = jnp.concatenate([y[rows : rows + half, lanes], y[last - half :, lanes]], axis=0)
            kept[index, rows:, :] = extra.astype(BF16)

    @pl.when(step == pl.num_programs(0) - 1)
    def _():
        own = lax.axis_index("sp")
        for offset, out in enumerate(outs):
            out[...] = kept[own ^ offset]


def value_blocks(rows, wv, started, devices, cut, early):
    span, model = rows.shape
    width = wv.shape[1]
    share = width // devices
    tile = max(2 * LANES, share)
    if early:
        specs = [
            whole((cut, model)),
            pl.BlockSpec((TILE_ROWS, model), lambda i: (cut // TILE_ROWS, 0)),
            pl.BlockSpec((TILE_ROWS, model), lambda i: (span // TILE_ROWS - 1, 0)),
        ]
        block = (cut + EXTRA, share)
    else:
        specs = [pl.BlockSpec((span - cut, model), lambda i: (cut // (span - cut), 0))]
        block = (span - cut, share)
    count = len(specs)

    def kernel(*refs):
        value_kernel(refs[:count], refs[count], refs[count + 2 : -1], refs[-1])

    return pl.pallas_call(
        kernel,
        grid=(width // tile,),
        in_specs=specs + [pl.BlockSpec((model, tile), lambda i: (0, i)), pl.BlockSpec(memory_space=pl.ANY)],
        out_specs=[whole(block)] * devices,
        out_shape=[jax.ShapeDtypeStruct(block, BF16)] * devices,
        scratch_shapes=[pltpu.VMEM((devices,) + block, BF16)],
        compiler_params=pltpu.CompilerParams(vmem_limit_bytes=VMEM_LIMIT),
        cost_estimate=pl.CostEstimate(
            flops=2 * block[0] * model * width,
            bytes_accessed=2 * (block[0] * model + model * width),
            transcendentals=0,
        ),
        name="early_values" if early else "late_values",
    )(*[off_chip(rows)] * count, off_chip(wv), started)


def key_read_kernel(
    group_devices, held_ref, *refs
):
    relayed = refs[: group_devices - 1]
    (
        taps_ref,
        query_ref,
        offset_ref,
        decay_ref,
        spikes_ref,
        keys_ref,
        weight_ref,
        blocks,
        line,
        rates,
        scores,
        spikes,
    ) = refs[group_devices - 1 :]
    repeats = HEADS // GROUPS
    sources = blocks.shape[0]
    half = keys_ref.shape[1] // 2
    heads = spikes_ref.shape[1]
    tiles = 2 * half // LANES
    me = lax.axis_index("sp")
    group, rank = me // group_devices, me % group_devices
    for offset in range(GROUPS):
        blocks[(group ^ offset) * group_devices + rank] = held_ref[offset]
        for shift in range(1, group_devices):
            blocks[(group ^ offset) * group_devices + (rank ^ shift)] = relayed[shift - 1][offset]
    taps = []
    for k in range(5):
        tap = taps_ref[k, pl.ds(group, 1), :]
        taps.append(jnp.concatenate([tap, tap], axis=1))
    asked = query_ref[0].astype(F32)
    asked = jnp.where(lax.broadcasted_iota(jnp.int32, asked.shape, 0) == group, asked, 0.0)
    asked = jnp.sum(asked, axis=0, keepdims=True)
    asked = jnp.broadcast_to(jnp.concatenate([asked, asked], axis=1), (16, LANES))
    part_row = lax.broadcasted_iota(jnp.int32, (16, LANES), 0)
    query = jnp.where(part_row == lane_index((16, LANES)) // STATE, asked, 0.0).astype(BF16)
    edge_left = lane_index((16, LANES)) < STATE
    left = lane_index((half, LANES)) < STATE
    picked = lax.broadcasted_iota(jnp.int32, (heads * tiles, repeats * tiles), 0)
    column = lax.broadcasted_iota(jnp.int32, (heads * tiles, repeats * tiles), 1)
    select = (column == (picked % tiles) * repeats + rank * heads + picked // tiles).astype(BF16)

    def one_source(source, carry):
        body = blocks[source, :half, :].astype(F32)
        before = blocks[jnp.maximum(source - 1, 0), half - 16 : half, :].astype(F32)
        after = blocks[jnp.minimum(source + 1, sources - 1), :16, :].astype(F32)
        before = jnp.where(source > 0, before, 0.0)
        after = jnp.where(source < sources - 1, after, 0.0)
        top = jnp.where(edge_left, pltpu.roll(before, STATE, 1), pltpu.roll(body[half - 16 :], STATE, 1))
        bottom = jnp.where(edge_left, pltpu.roll(body[:16], STATE, 1), pltpu.roll(after, STATE, 1))
        line[0:16, :] = top
        line[16 : 16 + half, :] = body
        line[16 + half :, :] = bottom
        total = taps[0] * line[14 : 14 + half, :]
        for k in range(1, 5):
            total = total + taps[k] * line[14 + k : 14 + k + half, :]
        y = silu(total).astype(BF16)
        score = lax.dot_general(query, y, (((1,), (1,)), ((), ())), preferred_element_type=F32)
        scores[source] = jnp.concatenate(
            [score[part : part + 1, c * LANES : (c + 1) * LANES] for part in range(2) for c in range(tiles // 2)],
            axis=0,
        )
        z = y.astype(F32)
        turned = pltpu.roll(z, STATE, 1)
        keys_ref[source, :half, :] = jnp.where(left, z, turned).astype(BF16)
        keys_ref[source, half:, :] = jnp.where(left, turned, z).astype(BF16)
        chosen = jnp.dot(select, blocks[source, half:, :], preferred_element_type=F32)
        for h in range(heads):
            rates[h, source] = chosen[h * tiles : (h + 1) * tiles]
        return carry

    lax.fori_loop(0, sources, one_source, 0)
    count = sources * tiles
    lane_row = lax.broadcasted_iota(jnp.int32, (LANES, LANES), 0)
    lane_col = lax.broadcasted_iota(jnp.int32, (LANES, LANES), 1)
    later_lanes = (lane_row > lane_col).astype(F32)
    row = lax.broadcasted_iota(jnp.int32, (count, count), 0)
    col = lax.broadcasted_iota(jnp.int32, (count, count), 1)
    later_rows = (col > row).astype(F32)
    score = scores[...].reshape(count, LANES)
    for h in range(heads):
        for c in range(count):
            spikes[h, c : c + 1, :] = spikes_ref[0, h : h + 1, c * LANES : (c + 1) * LANES]
    exact = dict(preferred_element_type=F32, precision=lax.Precision.HIGHEST)
    for h in range(heads):
        raw = rates[h].reshape(count, LANES) + offset_ref[h]
        rate = jnp.maximum(raw, 0.0) + jnp.log1p(jnp.exp(-jnp.abs(raw)))
        decay = jnp.exp(jnp.full((1, LANES), decay_ref[h], F32))
        step = spikes[h] - decay * rate
        within = jnp.dot(step, later_lanes, **exact)
        totals = jnp.broadcast_to(jnp.sum(step, axis=1, keepdims=True), (count, LANES))
        ahead = within + jnp.dot(later_rows, totals, **exact)
        weight = rate * jnp.exp(ahead) * score
        high = rounded(weight)
        weight_ref[:, h] = high.reshape(sources, tiles, LANES)
        weight_ref[:, heads + h] = (weight - high).reshape(sources, tiles, LANES)


def key_read(held, relayed, taps, query, offset, decay, spikes, group_devices, span):
    sources = group_devices * GROUPS
    heads = offset.shape[0]
    half = span // 2
    tiles = span // LANES
    smem = pl.BlockSpec(memory_space=pltpu.SMEM)
    vmem = pl.BlockSpec(memory_space=pltpu.VMEM)
    count = 1 + len(relayed)
    return pl.pallas_call(
        lambda *refs: key_read_kernel(group_devices, *refs),
        in_specs=[vmem] * (count + 2) + [smem, smem, vmem],
        out_specs=[vmem, vmem],
        out_shape=[
            jax.ShapeDtypeStruct((sources, span, LANES), BF16),
            jax.ShapeDtypeStruct((sources, 2 * heads, tiles, LANES), F32),
        ],
        scratch_shapes=[
            pltpu.VMEM((sources,) + held.shape[1:], BF16),
            pltpu.VMEM((half + 32, LANES), F32),
            pltpu.VMEM((heads, sources, tiles, LANES), F32),
            pltpu.VMEM((sources, tiles, LANES), F32),
            pltpu.VMEM((heads, sources * tiles, LANES), F32),
        ],
        compiler_params=pltpu.CompilerParams(vmem_limit_bytes=VMEM_LIMIT),
        cost_estimate=pl.CostEstimate(flops=10**9, bytes_accessed=4 * 10**6, transcendentals=10**6),
        name="key_read",
    )(*(on_chip(x) for x in [held, *relayed, taps, query]), offset, decay, on_chip(spikes))


def convolved(line, body, before, after, taps_ref, weight_ref, source, start_row, total):
    rows, share = body.shape
    heads = share // HEAD
    line[0:8, :] = before
    line[8 : 8 + rows, :] = body
    line[8 + rows :, :] = after
    taps = [jnp.concatenate([taps_ref[k, h : h + 1, :] for h in range(heads)], axis=1) for k in range(5)]
    tiles = weight_ref.shape[2]
    weight = weight_ref[source].reshape(-1, LANES)
    tile_of = lax.broadcasted_iota(jnp.int32, weight.shape, 0) % tiles
    read = jnp.zeros(total.shape, F32)
    values = []
    for tile in range(rows // LANES):
        start = tile * LANES
        y = taps[0] * line[6 + start : 6 + start + LANES, :]
        for k in range(1, 5):
            y = y + taps[k] * line[6 + k + start : 6 + k + start + LANES, :]
        y = silu(y).astype(BF16)
        masked = jnp.where(tile_of == start_row // LANES + tile, weight, 0.0).astype(BF16)
        read = read + jnp.dot(masked, y, preferred_element_type=F32)
        values.append(y)
    total[...] += read
    return values


def wove(woven, values, keys_ref, source, start_row, out_ref):
    share = values[0].shape[1]
    heads = share // HEAD
    left = lane_index((LANES, LANES)) < HEAD
    for tile, y in enumerate(values):
        start = tile * LANES
        keys = keys_ref[source, start_row + start : start_row + start + LANES, :].astype(F32)
        z = y.astype(F32)
        if share == LANES:
            pieces = [jnp.where(left, z, keys), jnp.where(left, pltpu.roll(z, HEAD, 1), keys)]
        else:
            pieces = [
                jnp.concatenate([z[:, h * HEAD : (h + 1) * HEAD], keys[:, STATE:]], axis=1) for h in range(heads)
            ]
        for h, piece in enumerate(pieces):
            woven[pl.ds(heads * start + h, LANES, heads), :] = piece
        part = slice(heads * start, heads * (start + LANES))
        out_ref[0, part, :] = woven[part, :].astype(BF16)


def line_scratch(rows, share):
    return pltpu.VMEM((rows + 16, share), F32)


def woven_scratch(rows, share):
    return pltpu.VMEM((share // HEAD * rows, LANES), F32)


def early_kernel(cut, *refs):
    blocks = refs[:-10]
    keys_ref, weight_ref, taps_ref, out_ref, read_ref, edges_ref, kept, line, woven, total = refs[-10:]
    source = pl.program_id(0)
    own = lax.axis_index("sp")

    @pl.when(source == 0)
    def _():
        total[...] = jnp.zeros_like(total)
        for offset, block_ref in enumerate(blocks):
            kept[own ^ offset] = block_ref[...]
            edges_ref[own ^ offset, :TILE_ROWS, :] = block_ref[:TILE_ROWS, :]
            edges_ref[own ^ offset, TILE_ROWS:, :] = block_ref[cut - TILE_ROWS : cut, :]

    block = kept[source].astype(F32)
    before = kept[jnp.maximum(source - 1, 0), cut:, :].astype(F32)
    before = jnp.where(source > 0, before, 0.0)
    values = convolved(line, block[:cut], before, block[cut:], taps_ref, weight_ref, source, 0, total)
    wove(woven, values, keys_ref, source, 0, out_ref)
    read_ref[...] = total[...]


def early_rows(blocks, keys, weight, taps, cut):
    sources, span = keys.shape[:2]
    height, share = blocks[0].shape
    heads = share // HEAD
    reads = weight.shape[1] * weight.shape[2]
    edges = (sources, 2 * TILE_ROWS, share)
    vmem = pl.BlockSpec(memory_space=pltpu.VMEM)
    inputs = [*blocks, keys, weight, taps]
    return pl.pallas_call(
        lambda *refs: early_kernel(cut, *refs),
        grid=(sources,),
        in_specs=[vmem] * len(inputs),
        out_specs=[
            pl.BlockSpec((1, heads * cut, LANES), lambda s: (s, 0, 0)),
            whole((reads, share)),
            whole(edges),
        ],
        out_shape=[
            jax.ShapeDtypeStruct((sources, heads * span, LANES), BF16),
            jax.ShapeDtypeStruct((reads, share), F32),
            jax.ShapeDtypeStruct(edges, BF16),
        ],
        scratch_shapes=[
            pltpu.VMEM((sources, height, share), BF16),
            line_scratch(cut, share),
            woven_scratch(cut, share),
            pltpu.VMEM((reads, share), F32),
        ],
        compiler_params=pltpu.CompilerParams(vmem_limit_bytes=VMEM_LIMIT),
        cost_estimate=pl.CostEstimate(flops=2 * 10**9, bytes_accessed=6 * 10**6, transcendentals=10**6),
        name="early_rows",
    )(*(on_chip(x) for x in inputs))


def late_values_of(offset, block_ref, edges_ref, taps_ref, weight_ref, line, total, cut):
    source = lax.axis_index("sp") ^ offset
    sources = edges_ref.shape[0]
    before = edges_ref[source, TILE_ROWS:, :].astype(F32)[TILE_ROWS - 8 :]
    after = edges_ref[jnp.minimum(source + 1, sources - 1), :TILE_ROWS, :].astype(F32)[:8]
    after = jnp.where(source < sources - 1, after, 0.0)
    body = block_ref[...].astype(F32)
    return convolved(line, body, before, after, taps_ref, weight_ref, source, cut, total)


def late_kernel(cut, offsets, *refs):
    count = len(offsets)
    blocks = refs[:count]
    edges_ref, keys_ref, weight_ref, taps_ref, read_ref, _, out_ref, total, line, woven = refs[count:]
    step = pl.program_id(0)

    @pl.when(step == 0)
    def _():
        total[...] = read_ref[...]

    for index, offset in enumerate(offsets):

        @pl.when(step == index)
        def _(index=index, offset=offset):
            values = late_values_of(offset, blocks[index], edges_ref, taps_ref, weight_ref, line, total, cut)
            wove(woven, values, keys_ref, lax.axis_index("sp") ^ offset, cut, out_ref)


def wave_offset(step, offsets):
    offset = step + offsets[0]
    for index in range(1, len(offsets)):
        gap = offsets[index] - offsets[index - 1] - 1
        if gap:
            offset = offset + gap * (step >= index).astype(jnp.int32)
    return offset


def late_out_spec(offsets, shape):
    rows = shape[1] // 2
    return pl.BlockSpec((1, rows, LANES), lambda i: (lax.axis_index("sp") ^ wave_offset(i, offsets), 1, 0))


def late_rows(offsets, late, edges, keys, weight, taps, read, out, cut):
    rows, share = late[0].shape
    vmem = pl.BlockSpec(memory_space=pltpu.VMEM)
    inputs = [late[k] for k in offsets] + [edges, keys, weight, taps, read]
    return pl.pallas_call(
        lambda *refs: late_kernel(cut, offsets, *refs),
        grid=(len(offsets),),
        in_specs=[vmem] * len(inputs) + [pl.BlockSpec(memory_space=pl.ANY)],
        out_specs=[late_out_spec(offsets, out.shape), whole(read.shape)],
        out_shape=[jax.ShapeDtypeStruct(out.shape, BF16), jax.ShapeDtypeStruct(read.shape, F32)],
        scratch_shapes=[line_scratch(rows, share), woven_scratch(rows, share)],
        input_output_aliases={len(inputs): 0},
        compiler_params=pltpu.CompilerParams(vmem_limit_bytes=VMEM_LIMIT),
        cost_estimate=pl.CostEstimate(flops=10**9, bytes_accessed=2 * 10**6, transcendentals=10**6),
        name="late_rows",
    )(*(on_chip(x) for x in inputs), out)


def last_read_kernel(cut, offsets, *refs):
    count = len(offsets)
    blocks = refs[:count]
    edges_ref, weight_ref, taps_ref, read_ref, gate_ref, values_ref, gated_ref, square_ref, line, total = refs[count:]
    total[...] = read_ref[...]
    for index, offset in enumerate(offsets):
        part = line.at[index]
        values = late_values_of(offset, blocks[index], edges_ref, taps_ref, weight_ref, part, total, cut)
        for tile, y in enumerate(values):
            values_ref[index, tile * LANES : (tile + 1) * LANES, :] = y
    tiles = weight_ref.shape[2]
    shape = total.shape
    heads = shape[1] // HEAD
    head = (lax.broadcasted_iota(jnp.int32, shape, 0) // tiles) % heads
    mine = head == lane_index(shape) // HEAD
    read = jnp.sum(jnp.where(mine, total[...], 0.0), axis=0, keepdims=True)
    read = jnp.concatenate([read[:, h * HEAD : (h + 1) * HEAD] for h in range(heads)], axis=0)
    gated = read * silu(gate_ref[0].astype(F32))
    gated_ref[...] = gated
    square = jnp.sum(jnp.sum(gated * gated, axis=1, keepdims=True), axis=0, keepdims=True)
    square_ref[...] = jnp.broadcast_to(square, square_ref.shape)


def last_read(offsets, late, edges, weight, taps, read, gate, cut):
    rows, share = late[0].shape
    vmem = pl.BlockSpec(memory_space=pltpu.VMEM)
    inputs = [late[k] for k in offsets] + [edges, weight, taps, read, gate]
    return pl.pallas_call(
        lambda *refs: last_read_kernel(cut, offsets, *refs),
        in_specs=[vmem] * len(inputs),
        out_specs=[vmem] * 3,
        out_shape=[
            jax.ShapeDtypeStruct((len(offsets), rows, share), BF16),
            jax.ShapeDtypeStruct((share // HEAD, HEAD), F32),
            jax.ShapeDtypeStruct((1, LANES), F32),
        ],
        scratch_shapes=[pltpu.VMEM((len(offsets), rows + 16, share), F32), pltpu.VMEM(read.shape, F32)],
        compiler_params=pltpu.CompilerParams(vmem_limit_bytes=VMEM_LIMIT),
        cost_estimate=pl.CostEstimate(flops=10**9, bytes_accessed=10**6, transcendentals=10**6),
        name="last_read",
    )(*(on_chip(x) for x in inputs))


def last_rows_kernel(cut, offsets, values_ref, keys_ref, _, out_ref, woven):
    step = pl.program_id(0)
    rows = values_ref.shape[1]
    values = [values_ref[step, start : start + LANES, :] for start in range(0, rows, LANES)]
    wove(woven, values, keys_ref, lax.axis_index("sp") ^ wave_offset(step, offsets), cut, out_ref)


def last_rows(offsets, values, keys, out, cut):
    rows, share = values.shape[1:]
    vmem = pl.BlockSpec(memory_space=pltpu.VMEM)
    return pl.pallas_call(
        lambda *refs: last_rows_kernel(cut, offsets, *refs),
        grid=(len(offsets),),
        in_specs=[vmem, vmem, pl.BlockSpec(memory_space=pl.ANY)],
        out_specs=late_out_spec(offsets, out.shape),
        out_shape=jax.ShapeDtypeStruct(out.shape, BF16),
        scratch_shapes=[woven_scratch(rows, share)],
        input_output_aliases={2: 0},
        compiler_params=pltpu.CompilerParams(vmem_limit_bytes=VMEM_LIMIT),
        cost_estimate=pl.CostEstimate(flops=10**9, bytes_accessed=2 * 10**6, transcendentals=0),
        name="last_rows",
    )(on_chip(values), on_chip(keys), out)


def on_device(
    context_input_tensor,
    content_mapping_matrix,
    address_mapping_matrix,
    increment_mapping_matrix,
    increment_speed_offset,
    channel_fading_exponent,
    extra_damping_spikes,
    content_smoothing_coefficients,
    address_smoothing_coefficients,
    newest_lookup_matrix,
    newest_output_switch,
    cluster_scaling_coefficients,
):
    rows = context_input_tensor[0]
    span = rows.shape[0]
    repeats = HEADS // GROUPS
    heads = increment_speed_offset.shape[0]
    group_devices = repeats // heads
    devices = lax.axis_size("sp")
    cut = span // 2

    blocks = key_blocks(rows, address_mapping_matrix, increment_mapping_matrix.T, group_devices)
    direct = [None] * (GROUPS - 1)
    for offset in range(1, GROUPS):
        direct[offset - 1] = flip_permute(blocks[offset], offset * group_devices)
    early = value_blocks(rows, content_mapping_matrix, blocks[0], devices, cut, True)
    late = value_blocks(rows, content_mapping_matrix, early[0], devices, cut, False)
    held = jnp.stack([blocks[0]] + direct)
    relayed = []
    for shift in range(1, group_devices):
        relayed.append(flip_permute(held, shift))
    early_blocks, late_blocks = [early[0]], [late[0]]
    for offset in range(1, devices):
        early_blocks.append(flip_permute(early[offset], offset))
        late_blocks.append(flip_permute(late[offset], offset))

    keys, weight = key_read(
        held,
        relayed,
        address_smoothing_coefficients,
        newest_lookup_matrix,
        increment_speed_offset,
        channel_fading_exponent,
        extra_damping_spikes,
        group_devices,
        span,
    )
    taps = content_smoothing_coefficients
    out, read, edges = early_rows(early_blocks, keys, weight, taps, cut)
    across = [offset for offset in range(devices) if offset % group_devices]
    along = [offset for offset in range(devices) if offset % group_devices == 0]
    near = [offset for offset in across if offset < devices // 2]
    final = [offset for offset in across if offset >= devices // 2]
    for wave in (along, near):
        out, read = late_rows(wave, late_blocks, edges, keys, weight, taps, read, out, cut)
    values, gated, group_sq = last_read(final, late_blocks, edges, weight, taps, read, newest_output_switch, cut)
    for level in range(group_devices.bit_length() - 1):
        group_sq = group_sq + flip_permute(group_sq, 2**level)
    out = last_rows(final, values, keys, out, cut)
    scaled = gated * lax.rsqrt(group_sq[0, 0] / (repeats * HEAD) + EPS) * cluster_scaling_coefficients
    store = out.reshape(1, devices * span, heads, HEAD + STATE)
    return store, scaled.astype(BF16).reshape(1, heads, HEAD)


def solution(mesh):
    placed = (
        P(("gr", "tp"), "sp", None),
        P(),
        P(),
        P(),
        P("sp"),
        P("sp"),
        P(("gr", "tp"), "sp", None),
        P(None, "sp", None),
        P(),
        P(("gr", "tp"), None, None),
        P(("gr", "tp"), "sp", None),
        P("sp", None),
    )

    return jax.shard_map(
        on_device,
        mesh=mesh,
        in_specs=placed,
        out_specs=(P(("gr", "tp"), None, "sp", None), P(("gr", "tp"), "sp", None)),
        check_vma=False,
    )
```

time: 105 us -> 88.8 us (0.85)
  waiting for transfers between devices: 35.5 us -> 19.6 us
  starting transfers between devices: 25.9 us -> 37.6 us
  local copies, waits for them, and re-layouts: 6.24 us -> 0.03 us
  Pallas kernels: 35 us -> 29.9 us
    ppermute x12 -> x19, starting transfers between devices: 18.6 us -> 37.6 us  [flip_permute(): return lax.ppermute(value, 'sp', pairs)]
    ppermute x12 -> x19, waiting for transfers between devices: 35.5 us -> 19.6 us  [flip_permute(): return lax.ppermute(value, 'sp', pairs)]
    all_to_all x1 -> x0, starting transfers between devices: 7.31 us -> none  [on_device(): early_blocks = lax.all_to_all(early, 'sp', 0, 0, tiled=True)]
    unnamed x46 -> x16, local copies, waits for them, and re-layouts: 6.24 us -> 0.03 us
    pallas_call x5 -> x6, Pallas kernels: 22.2 us -> 17 us  [the longest x2 11.2 us: value_blocks(): pl.pallas_call(kernel, grid=(width // tile,), in_specs=specs + [pl.BlockS...]
  transfers between devices with their start and end apart: 13 -> 19, of which waited for: 6 -> 6; matrix products, arithmetic and copies ran while one was open for 0% -> 0% of each run, Pallas kernels for 21% -> 28%
where the time goes in v1:
time: 88.8 us; the launch traced here: 88.6 us
  starting transfers between devices  37.6 us (42%)
  Pallas kernels  29.9 us (34%)
  waiting for transfers between devices  19.6 us (22%)
    ppermute x19, starting transfers between devices, flip_permute(): return lax.ppermute(value, 'sp', pairs)  37.6 us
    ppermute x19, waiting for transfers between devices, flip_permute(): return lax.ppermute(value, 'sp', pairs)  19.6 us
    pallas_call x2, Pallas kernels, value_blocks(): pl.pallas_call(kernel, grid=(width // tile,), in_specs=specs + [pl.BlockS...  11.2 us
    pallas_call x1, Pallas kernels, early_rows(): pl.pallas_call(lambda *refs: early_kernel(cut, *refs), grid=(sources,), i...  4.72 us
    pallas_call x1, Pallas kernels, key_blocks(): pl.pallas_call(lambda *refs: key_block_kernel(group_devices, *refs), grid...  4.63 us
    pallas_call x2, Pallas kernels, late_rows(): pl.pallas_call(lambda *refs: late_kernel(cut, offsets, *refs), grid=(len(...  4.13 us
    pallas_call x1, Pallas kernels, key_read(): pl.pallas_call(lambda *refs: key_read_kernel(group_devices, *refs), in_sp...  3.59 us
  transfers between devices with their start and end apart: 19, of which 6 were waited for; matrix products, arithmetic and copies ran while one was open for 0% of the time, Pallas kernels for 28%

profile of v1, /device:TPU:0, one launch (start us, length us, event | category | flops | bytes accessed | tf_op | source)
XLA Modules:
  0.0 88.6 jit_solution(6211223730852656251)
XLA Ops:
  0.6 4.6 %key_blocks.1 = (bf16[544,128]{1,0:T(8,128)(2,1)S(1)}, bf16[544,128]{1,0:T(8,128)(2,1)S(1)}, bf16[544,128]{1,0:T(8,128)(2,1)S(1)}, bf16[544,128]{1,0:T(8,128)(2,1)S(1)}) custom-call(bf16[1024,2048]{1,0:T(8,128)(2,1)} %bitcast.12, bf16[1024,2048]{1,0:T(8,128)(2,1)} %bitcast.13, bf16[2048,256]{1,0:T(8,128)(2,1)} %refs_2_.2, bf16[16,2048]{1,0:T(8,128)(2,1)} %bitcast.22), custom_call_target="tpu_custom_call" | custom-call | flops 1140850688 | bytes 4194304 | tf_op jit(solution)/shard_map/key_blocks/pallas_call | solution.py:102
  5.3 3.1 %collective-permute-start.9 = (bf16[544,128]{1,0:T(8,128)(2,1)S(1)}, bf16[544,128]{1,0:T(8,128)(2,1)S(1)}, u32[]{:S(2)}, u32[]{:S(2)}) collective-permute-start(bf16[544,128]{1,0:T(8,128)(2,1)S(1)} %get-tuple-element.45), channel_id=1, source_target_pairs={{0,4},{2,6},{4,0},{6,2},{8,12},{10,14},{12,8},{14,10},{1,5},{3,7},... | collective-permute-start | bytes 417800 | tf_op jit(solution)/shard_map/ppermute | solution.py:48
  8.4 2.6 %collective-permute-start.10 = (bf16[544,128]{1,0:T(8,128)(2,1)S(1)}, bf16[544,128]{1,0:T(8,128)(2,1)S(1)}, u32[]{:S(2)}, u32[]{:S(2)}) collective-permute-start(bf16[544,128]{1,0:T(8,128)(2,1)S(1)} %get-tuple-element.46), channel_id=1, source_target_pairs={{0,8},{2,10},{4,12},{6,14},{8,0},{10,2},{12,4},{14,6},{1,9},{3,11}... | collective-permute-start | bytes 417800 | tf_op jit(solution)/shard_map/ppermute | solution.py:48
  11.0 2.9 %collective-permute-done.9 = bf16[544,128]{1,0:T(8,128)(2,1)S(1)} collective-permute-done((bf16[544,128]{1,0:T(8,128)(2,1)S(1)}, bf16[544,128]{1,0:T(8,128)(2,1)S(1)}, u32[]{:S(2)}, u32[]{:S(2)}) %collective-permute-start.9) | collective-permute-done | bytes 139296 | tf_op jit(solution)/shard_map/ppermute | solution.py:48
  13.9 7.9 %collective-permute-done.10 = bf16[544,128]{1,0:T(8,128)(2,1)S(1)} collective-permute-done((bf16[544,128]{1,0:T(8,128)(2,1)S(1)}, bf16[544,128]{1,0:T(8,128)(2,1)S(1)}, u32[]{:S(2)}, u32[]{:S(2)}) %collective-permute-start.10) | collective-permute-done | bytes 139296 | tf_op jit(solution)/shard_map/ppermute | solution.py:48
  21.9 1.6 %collective-permute-start.12 = (bf16[4,544,128]{2,1,0:T(8,128)(2,1)S(1)}, bf16[4,544,128]{2,1,0:T(8,128)(2,1)S(1)}, u32[]{:S(2)}, u32[]{:S(2)}) collective-permute-start(bf16[4,544,128]{2,1,0:T(8,128)(2,1)S(1)} %pad_maximum_fusion.refs_0_), channel_id=1, source_target_pairs={{0,2},{2,0},{4,6},{6,4},{8,10},{10,8},{12,14},{14,12},{1,3},{3,1},... | collective-permute-start | bytes 1671176 | tf_op jit(solution)/shard_map/ppermute | solution.py:48
  23.5 5.6 %early_values.1 = (bf16[520,128]{1,0:T(8,128)(2,1)S(1)}, bf16[520,128]{1,0:T(8,128)(2,1)S(1)}, bf16[520,128]{1,0:T(8,128)(2,1)S(1)}, bf16[520,128]{1,0:T(8,128)(...) custom-call(bf16[1024,2048]{1,0:T(8,128)(2,1)} %bitcast.14, ...), custom_call_target="tpu_custom_call" | custom-call | flops 2181038080 | bytes 6324224 | tf_op jit(solution)/shard_map/early_values/pallas_call | solution.py:169
  29.1 0.6 collective-permute-start.2
  29.7 2.2 %collective-permute-start.3 = (bf16[520,128]{1,0:T(8,128)(2,1)S(1)}, bf16[520,128]{1,0:T(8,128)(2,1)S(1)}, u32[]{:S(2)}, u32[]{:S(2)}) collective-permute-start(bf16[520,128]{1,0:T(8,128)(2,1)S(1)} %get-tuple-element.39), channel_id=1, source_target_pairs={{0,4},{2,6},{4,0},{6,2},{8,12},{10,14},{12,8},{14,10},{1,5},{3,7},... | collective-permute-start | bytes 399368 | tf_op jit(solution)/shard_map/ppermute | solution.py:48
  31.9 1.0 %collective-permute-start.4 = (bf16[520,128]{1,0:T(8,128)(2,1)S(1)}, bf16[520,128]{1,0:T(8,128)(2,1)S(1)}, u32[]{:S(2)}, u32[]{:S(2)}) collective-permute-start(bf16[520,128]{1,0:T(8,128)(2,1)S(1)} %get-tuple-element.40), channel_id=1, source_target_pairs={{0,6},{2,4},{4,2},{6,0},{8,14},{10,12},{12,10},{14,8},{1,7},{3,5},... | collective-permute-start | bytes 399368 | tf_op jit(solution)/shard_map/ppermute | solution.py:48
  32.8 3.0 %collective-permute-start.5 = (bf16[520,128]{1,0:T(8,128)(2,1)S(1)}, bf16[520,128]{1,0:T(8,128)(2,1)S(1)}, u32[]{:S(2)}, u32[]{:S(2)}) collective-permute-start(bf16[520,128]{1,0:T(8,128)(2,1)S(1)} %get-tuple-element.41), channel_id=1, source_target_pairs={{0,8},{2,10},{4,12},{6,14},{8,0},{10,2},{12,4},{14,6},{1,9},{3,11}... | collective-permute-start | bytes 399368 | tf_op jit(solution)/shard_map/ppermute | solution.py:48
  35.9 2.6 %collective-permute-done.2.refs_1_ = bf16[520,128]{1,0:T(8,128)(2,1)S(1)} collective-permute-done((bf16[520,128]{1,0:T(8,128)(2,1)S(1)}, bf16[520,128]{1,0:T(8,128)(2,1)S(1)}, u32[]{:S(2)}, u32[]{:S(2)}) %collective-permute-start.2) | collective-permute-done | bytes 133152 | tf_op jit(solution)/shard_map/ppermute | solution.py:48
  38.4 6.8 %collective-permute-start.6 = (bf16[520,128]{1,0:T(8,128)(2,1)S(1)}, bf16[520,128]{1,0:T(8,128)(2,1)S(1)}, u32[]{:S(2)}, u32[]{:S(2)}) collective-permute-start(bf16[520,128]{1,0:T(8,128)(2,1)S(1)} %get-tuple-element.42), channel_id=1, source_target_pairs={{0,10},{2,8},{4,14},{6,12},{8,2},{10,0},{12,6},{14,4},{1,11},{3,9}... | collective-permute-start | bytes 399368 | tf_op jit(solution)/shard_map/ppermute | solution.py:48
  45.3 1.2 %collective-permute-start.7 = (bf16[520,128]{1,0:T(8,128)(2,1)S(1)}, bf16[520,128]{1,0:T(8,128)(2,1)S(1)}, u32[]{:S(2)}, u32[]{:S(2)}) collective-permute-start(bf16[520,128]{1,0:T(8,128)(2,1)S(1)} %get-tuple-element.43), channel_id=1, source_target_pairs={{0,12},{2,14},{4,8},{6,10},{8,4},{10,6},{12,0},{14,2},{1,13},{3,15... | collective-permute-start | bytes 399368 | tf_op jit(solution)/shard_map/ppermute | solution.py:48
  46.4 2.6 %collective-permute-start.8 = (bf16[520,128]{1,0:T(8,128)(2,1)S(1)}, bf16[520,128]{1,0:T(8,128)(2,1)S(1)}, u32[]{:S(2)}, u32[]{:S(2)}) collective-permute-start(bf16[520,128]{1,0:T(8,128)(2,1)S(1)} %get-tuple-element.44), channel_id=1, source_target_pairs={{0,14},{2,12},{4,10},{6,8},{8,6},{10,4},{12,2},{14,0},{1,15},{3,13... | collective-permute-start | bytes 399368 | tf_op jit(solution)/shard_map/ppermute | solution.py:48
  49.1 5.6 %late_values.1 = (bf16[512,128]{1,0:T(8,128)(2,1)S(1)}, bf16[512,128]{1,0:T(8,128)(2,1)S(1)}, bf16[512,128]{1,0:T(8,128)(2,1)S(1)}, bf16[512,128]{1,0:T(8,128)(2...) custom-call(bf16[1024,2048]{1,0:T(8,128)(2,1)} %bitcast.17, ...), custom_call_target="tpu_custom_call" | custom-call | flops 2147483648 | bytes 6291456 | tf_op jit(solution)/shard_map/late_values/pallas_call | solution.py:169
  54.7 3.6 %key_read.1 = (bf16[8,1024,128]{2,1,0:T(8,128)(2,1)S(1)}, f32[8,4,8,128]{3,2,1,0:T(8,128)S(1)}) custom-call(bf16[4,544,128]{2,1,0:T(8,128)(2,1)S(1)} %pad_maximum_fusion.refs_0_, bf16[4,544,128]{2,1,0:T(8,128)(2,1)S(1)} %collective-permute-done.12.refs_1_, f32[5,4,64]{2,1,0:T(4,128)S(1)} %copy-done.2, bf16[1,4,64]{2,1,0:T(4,128)(2,1)S(1)} %copy-done.3, ...), custom_call_target="tpu_custom_call" | custom-call | flops 1000000000 | bytes 4000000 | tf_op jit(solution)/shard_map/key_read/pallas_call | solution.py:295
  58.3 1.6 %collective-permute-start.13 = (bf16[512,128]{1,0:T(8,128)(2,1)S(1)}, bf16[512,128]{1,0:T(8,128)(2,1)S(1)}, u32[]{:S(2)}, u32[]{:S(2)}) collective-permute-start(bf16[512,128]{1,0:T(8,128)(2,1)S(1)} %get-tuple-element.51), channel_id=1, source_target_pairs={{0,2},{2,0},{4,6},{6,4},{8,10},{10,8},{12,14},{14,12},{1,3},{3,1},... | collective-permute-start | bytes 393224 | tf_op jit(solution)/shard_map/ppermute | solution.py:48
  59.9 2.0 %collective-permute-start.15 = (bf16[512,128]{1,0:T(8,128)(2,1)S(1)}, bf16[512,128]{1,0:T(8,128)(2,1)S(1)}, u32[]{:S(2)}, u32[]{:S(2)}) collective-permute-start(bf16[512,128]{1,0:T(8,128)(2,1)S(1)} %get-tuple-element.54), channel_id=1, source_target_pairs={{0,4},{2,6},{4,0},{6,2},{8,12},{10,14},{12,8},{14,10},{1,5},{3,7},... | collective-permute-start | bytes 393224 | tf_op jit(solution)/shard_map/ppermute | solution.py:48
  61.9 2.5 %collective-permute-start.17 = (bf16[512,128]{1,0:T(8,128)(2,1)S(1)}, bf16[512,128]{1,0:T(8,128)(2,1)S(1)}, u32[]{:S(2)}, u32[]{:S(2)}) collective-permute-start(bf16[512,128]{1,0:T(8,128)(2,1)S(1)} %get-tuple-element.56), channel_id=1, source_target_pairs={{0,12},{2,14},{4,8},{6,10},{8,4},{10,6},{12,0},{14,2},{1,13},{3,15... | collective-permute-start | bytes 393224 | tf_op jit(solution)/shard_map/ppermute | solution.py:48
  64.4 4.7 %early_rows.1 = (bf16[8,2048,128]{2,1,0:T(8,128)(2,1)}, f32[32,128]{1,0:T(8,128)S(1)}, bf16[8,32,128]{2,1,0:T(8,128)(2,1)S(1)}) custom-call(bf16[520,128]{1,0:T(8,128)(2,1)S(1)} %get-tuple-element.35.refs_2_.refs_0_, bf16[520,128]{1,0:T(8,128)(2,1)S(1)} %collective-permute-done.2.refs_1_, bf16[520,128]{1,0:T(8,128)(2,1)S(1)} %collective-permute-done.3.refs_2_, ...), custom_call_target="tpu_custom_call" | custom-call | flops 2000000000 | bytes 6000000 | tf_op jit(solution)/shard_map/early_rows/pallas_call | solution.py:399
  69.1 1.6 %collective-permute-start = (bf16[512,128]{1,0:T(8,128)(2,1)S(1)}, bf16[512,128]{1,0:T(8,128)(2,1)S(1)}, u32[]{:S(2)}, u32[]{:S(2)}) collective-permute-start(bf16[512,128]{1,0:T(8,128)(2,1)S(1)} %get-tuple-element.36), channel_id=1, source_target_pairs={{0,10},{2,8},{4,14},{6,12},{8,2},{10,0},{12,6},{14,4},{1,11},{3,9}... | collective-permute-start | bytes 393224 | tf_op jit(solution)/shard_map/ppermute | solution.py:48
  70.8 4.3 %collective-permute-done.16.refs_2_ = bf16[512,128]{1,0:T(8,128)(2,1)S(1)} collective-permute-done((bf16[512,128]{1,0:T(8,128)(2,1)S(1)}, bf16[512,128]{1,0:T(8,128)(2,1)S(1)}, u32[]{:S(2)}, u32[]{:S(2)}) %collective-permute-start.16) | collective-permute-done | bytes 131104 | tf_op jit(solution)/shard_map/ppermute | solution.py:48
  75.1 3.1 %collective-permute-start.1 = (bf16[512,128]{1,0:T(8,128)(2,1)S(1)}, bf16[512,128]{1,0:T(8,128)(2,1)S(1)}, u32[]{:S(2)}, u32[]{:S(2)}) collective-permute-start(bf16[512,128]{1,0:T(8,128)(2,1)S(1)} %get-tuple-element.37), channel_id=1, source_target_pairs={{0,14},{2,12},{4,10},{6,8},{8,6},{10,4},{12,2},{14,0},{1,15},{3,13... | collective-permute-start | bytes 393224 | tf_op jit(solution)/shard_map/ppermute | solution.py:48
  78.2 2.6 %late_rows.2 = (bf16[8,2048,128]{2,1,0:T(8,128)(2,1)}, f32[32,128]{1,0:T(8,128)S(1)}) custom-call(bf16[512,128]{1,0:T(8,128)(2,1)S(1)} %get-tuple-element.53.refs_0_, bf16[512,128]{1,0:T(8,128)(2,1)S(1)} %collective-permute-done.15.refs_1_, bf16[512,128]{1,0:T(8,128)(2,1)S(1)} %collective-permute-done.16.refs_2_, ...), custom_call_target="tpu_custom_call", output_to_operand_aliasing={{0}: (9, {})} | custom-call | flops 1000000000 | bytes 2000000 | tf_op jit(solution)/shard_map/late_rows/pallas_call | solution.py:471
  80.8 1.5 %late_rows.3 = (bf16[8,2048,128]{2,1,0:T(8,128)(2,1)}, f32[32,128]{1,0:T(8,128)S(1)}) custom-call(bf16[512,128]{1,0:T(8,128)(2,1)S(1)} %collective-permute-done.13.refs_0_, bf16[512,128]{1,0:T(8,128)(2,1)S(1)} %collective-permute-done.14.refs_1_, bf16[8,32,128]{2,1,0:T(8,128)(2,1)S(1)} %get-tuple-element.50.refs_4_.refs_2_, ...), custom_call_target="tpu_custom_call", output_to_operand_aliasing={{0}: (7, {})} | custom-call | flops 1000000000 | bytes 2000000 | tf_op jit(solution)/shard_map/late_rows/pallas_call | solution.py:471
  82.4 1.3 %collective-permute-done.refs_0_ = bf16[512,128]{1,0:T(8,128)(2,1)S(1)} collective-permute-done((bf16[512,128]{1,0:T(8,128)(2,1)S(1)}, bf16[512,128]{1,0:T(8,128)(2,1)S(1)}, u32[]{:S(2)}, u32[]{:S(2)}) %collective-permute-start) | collective-permute-done | bytes 131104 | tf_op jit(solution)/shard_map/ppermute | solution.py:48
  83.7 0.7 last_read.1
  84.4 2.1 %collective-permute-start.18 = (f32[1,128]{1,0:T(1,128)S(1)}, f32[1,128]{1,0:T(1,128)S(1)}, u32[]{:S(2)}, u32[]{:S(2)}) collective-permute-start(f32[1,128]{1,0:T(1,128)S(1)} %get-tuple-element.65), channel_id=1, source_target_pairs={{0,2},{2,0},{4,6},{6,4},{8,10},{10,8},{12,14},{14,12},{1,3},{3,1},... | collective-permute-start | bytes 1544 | tf_op jit(solution)/shard_map/ppermute | solution.py:48
  86.4 1.0 %last_rows.1 = bf16[8,2048,128]{2,1,0:T(8,128)(2,1)} custom-call(bf16[2,512,128]{2,1,0:T(8,128)(2,1)S(1)} %get-tuple-element.62.refs_0_, bf16[8,1024,128]{2,1,0:T(8,128)(2,1)S(1)} %get-tuple-element.48.refs_8_.refs_5_.refs_3_.refs_1_, bf16[8,2048,128]{2,1,0:T(8,128)(2,1)} %get-tuple-element.63.refs_2_), custom_call_target="tpu_custom_call", output_to_operand_aliasing={{}: (2, {})} | custom-call | flops 1000000000 | bytes 2000000 | tf_op jit(solution)/shard_map/last_rows/pallas_call | solution.py:538
  87.4 0.6 collective-permute-done.18
  88.1 0.5 fusion
  (34 shorter events, 0.2 us)
Async XLA Ops:
  5.3 8.6 %collective-permute-start.9 = (bf16[544,128]{1,0:T(8,128)(2,1)S(1)}, bf16[544,128]{1,0:T(8,128)(2,1)S(1)}, u32[]{:S(2)}, u32[]{:S(2)}) collective-permute-start(bf16[544,128]{1,0:T(8,128)(2,1)S(1)} %get-tuple-element.45), channel_id=1, source_target_pairs={{0,4},{2,6},{4,0},{6,2},{8,12},{10,14},{12,8},{14,10},{1,5},{3,7},... | collective-permute-start | bytes 417800 | tf_op jit(solution)/shard_map/ppermute | solution.py:48
  8.4 13.4 %collective-permute-start.10 = (bf16[544,128]{1,0:T(8,128)(2,1)S(1)}, bf16[544,128]{1,0:T(8,128)(2,1)S(1)}, u32[]{:S(2)}, u32[]{:S(2)}) collective-permute-start(bf16[544,128]{1,0:T(8,128)(2,1)S(1)} %get-tuple-element.46), channel_id=1, source_target_pairs={{0,8},{2,10},{4,12},{6,14},{8,0},{10,2},{12,4},{14,6},{1,9},{3,11}... | collective-permute-start | bytes 417800 | tf_op jit(solution)/shard_map/ppermute | solution.py:48
  11.0 10.8 %collective-permute-start.11 = (bf16[544,128]{1,0:T(8,128)(2,1)S(1)}, bf16[544,128]{1,0:T(8,128)(2,1)S(1)}, u32[]{:S(2)}, u32[]{:S(2)}) collective-permute-start(bf16[544,128]{1,0:T(8,128)(2,1)S(1)} %get-tuple-element.47), channel_id=1, source_target_pairs={{0,12},{2,14},{4,8},{6,10},{8,4},{10,6},{12,0},{14,2},{1,13},{3,15... | collective-permute-start | bytes 417800 | tf_op jit(solution)/shard_map/ppermute | solution.py:48
  21.9 24.5 %collective-permute-start.12 = (bf16[4,544,128]{2,1,0:T(8,128)(2,1)S(1)}, bf16[4,544,128]{2,1,0:T(8,128)(2,1)S(1)}, u32[]{:S(2)}, u32[]{:S(2)}) collective-permute-start(bf16[4,544,128]{2,1,0:T(8,128)(2,1)S(1)} %pad_maximum_fusion.refs_0_), channel_id=1, source_target_pairs={{0,2},{2,0},{4,6},{6,4},{8,10},{10,8},{12,14},{14,12},{1,3},{3,1},... | collective-permute-start | bytes 1671176 | tf_op jit(solution)/shard_map/ppermute | solution.py:48
  29.1 9.3 %collective-permute-start.2 = (bf16[520,128]{1,0:T(8,128)(2,1)S(1)}, bf16[520,128]{1,0:T(8,128)(2,1)S(1)}, u32[]{:S(2)}, u32[]{:S(2)}) collective-permute-start(bf16[520,128]{1,0:T(8,128)(2,1)S(1)} %get-tuple-element.38), channel_id=1, source_target_pairs={{0,2},{2,0},{4,6},{6,4},{8,10},{10,8},{12,14},{14,12},{1,3},{3,1},... | collective-permute-start | bytes 399368 | tf_op jit(solution)/shard_map/ppermute | solution.py:48
  29.7 15.6 %collective-permute-start.3 = (bf16[520,128]{1,0:T(8,128)(2,1)S(1)}, bf16[520,128]{1,0:T(8,128)(2,1)S(1)}, u32[]{:S(2)}, u32[]{:S(2)}) collective-permute-start(bf16[520,128]{1,0:T(8,128)(2,1)S(1)} %get-tuple-element.39), channel_id=1, source_target_pairs={{0,4},{2,6},{4,0},{6,2},{8,12},{10,14},{12,8},{14,10},{1,5},{3,7},... | collective-permute-start | bytes 399368 | tf_op jit(solution)/shard_map/ppermute | solution.py:48
  31.9 26.5 %collective-permute-start.4 = (bf16[520,128]{1,0:T(8,128)(2,1)S(1)}, bf16[520,128]{1,0:T(8,128)(2,1)S(1)}, u32[]{:S(2)}, u32[]{:S(2)}) collective-permute-start(bf16[520,128]{1,0:T(8,128)(2,1)S(1)} %get-tuple-element.40), channel_id=1, source_target_pairs={{0,6},{2,4},{4,2},{6,0},{8,14},{10,12},{12,10},{14,8},{1,7},{3,5},... | collective-permute-start | bytes 399368 | tf_op jit(solution)/shard_map/ppermute | solution.py:48
  32.8 27.1 %collective-permute-start.5 = (bf16[520,128]{1,0:T(8,128)(2,1)S(1)}, bf16[520,128]{1,0:T(8,128)(2,1)S(1)}, u32[]{:S(2)}, u32[]{:S(2)}) collective-permute-start(bf16[520,128]{1,0:T(8,128)(2,1)S(1)} %get-tuple-element.41), channel_id=1, source_target_pairs={{0,8},{2,10},{4,12},{6,14},{8,0},{10,2},{12,4},{14,6},{1,9},{3,11}... | collective-permute-start | bytes 399368 | tf_op jit(solution)/shard_map/ppermute | solution.py:48
  38.4 21.5 %collective-permute-start.6 = (bf16[520,128]{1,0:T(8,128)(2,1)S(1)}, bf16[520,128]{1,0:T(8,128)(2,1)S(1)}, u32[]{:S(2)}, u32[]{:S(2)}) collective-permute-start(bf16[520,128]{1,0:T(8,128)(2,1)S(1)} %get-tuple-element.42), channel_id=1, source_target_pairs={{0,10},{2,8},{4,14},{6,12},{8,2},{10,0},{12,6},{14,4},{1,11},{3,9}... | collective-permute-start | bytes 399368 | tf_op jit(solution)/shard_map/ppermute | solution.py:48
  45.3 16.6 %collective-permute-start.7 = (bf16[520,128]{1,0:T(8,128)(2,1)S(1)}, bf16[520,128]{1,0:T(8,128)(2,1)S(1)}, u32[]{:S(2)}, u32[]{:S(2)}) collective-permute-start(bf16[520,128]{1,0:T(8,128)(2,1)S(1)} %get-tuple-element.43), channel_id=1, source_target_pairs={{0,12},{2,14},{4,8},{6,10},{8,4},{10,6},{12,0},{14,2},{1,13},{3,15... | collective-permute-start | bytes 399368 | tf_op jit(solution)/shard_map/ppermute | solution.py:48
  46.4 15.5 %collective-permute-start.8 = (bf16[520,128]{1,0:T(8,128)(2,1)S(1)}, bf16[520,128]{1,0:T(8,128)(2,1)S(1)}, u32[]{:S(2)}, u32[]{:S(2)}) collective-permute-start(bf16[520,128]{1,0:T(8,128)(2,1)S(1)} %get-tuple-element.44), channel_id=1, source_target_pairs={{0,14},{2,12},{4,10},{6,8},{8,6},{10,4},{12,2},{14,0},{1,15},{3,13... | collective-permute-start | bytes 399368 | tf_op jit(solution)/shard_map/ppermute | solution.py:48
  49.0 5.6 %copy-start.1 = (f32[1,2,8192]{2,1,0:T(2,128)S(1)}, f32[1,2,8192]{2,1,0:T(2,128)}, u32[]{:S(2)}) copy-start(f32[1,2,8192]{2,1,0:T(2,128)} %refs_6_.2) | copy-start | bytes 196612
  49.1 5.6 %copy-start.2 = (f32[5,4,64]{2,1,0:T(4,128)S(1)}, f32[5,4,64]{2,1,0:T(4,128)}, u32[]{:S(2)}) copy-start(f32[5,4,64]{2,1,0:T(4,128)} %refs_2_.3) | copy-start | bytes 15364
  49.1 5.6 %copy-start.3 = (bf16[1,4,64]{2,1,0:T(4,128)(2,1)S(1)}, bf16[1,4,64]{2,1,0:T(4,128)(2,1)}, u32[]{:S(2)}) copy-start(bf16[1,4,64]{2,1,0:T(4,128)(2,1)} %refs_3_.3) | copy-start | bytes 1540
  49.1 5.6 %copy-start.4 = (f32[2]{0:T(128)S(1)}, f32[2]{0:T(128)}, u32[]{:S(2)}) copy-start(f32[2]{0:T(128)} %refs_4_.2) | copy-start | bytes 28
  49.1 5.6 %copy-start.5 = (f32[2]{0:T(128)S(1)}, f32[2]{0:T(128)}, u32[]{:S(2)}) copy-start(f32[2]{0:T(128)} %refs_5_.2) | copy-start | bytes 28
  49.1 15.3 %copy-start = (f32[5,2,64]{2,1,0:T(2,128)S(1)}, f32[5,2,64]{2,1,0:T(2,128)}, u32[]{:S(2)}) copy-start(f32[5,2,64]{2,1,0:T(2,128)} %refs_4_.3) | copy-start | bytes 7684
  58.3 22.5 %collective-permute-start.13 = (bf16[512,128]{1,0:T(8,128)(2,1)S(1)}, bf16[512,128]{1,0:T(8,128)(2,1)S(1)}, u32[]{:S(2)}, u32[]{:S(2)}) collective-permute-start(bf16[512,128]{1,0:T(8,128)(2,1)S(1)} %get-tuple-element.51), channel_id=1, source_target_pairs={{0,2},{2,0},{4,6},{6,4},{8,10},{10,8},{12,14},{14,12},{1,3},{3,1},... | collective-permute-start | bytes 393224 | tf_op jit(solution)/shard_map/ppermute | solution.py:48
  59.9 20.9 %collective-permute-start.14 = (bf16[512,128]{1,0:T(8,128)(2,1)S(1)}, bf16[512,128]{1,0:T(8,128)(2,1)S(1)}, u32[]{:S(2)}, u32[]{:S(2)}) collective-permute-start(bf16[512,128]{1,0:T(8,128)(2,1)S(1)} %get-tuple-element.52), channel_id=1, source_target_pairs={{0,6},{2,4},{4,2},{6,0},{8,14},{10,12},{12,10},{14,8},{1,7},{3,5},... | collective-permute-start | bytes 393224 | tf_op jit(solution)/shard_map/ppermute | solution.py:48
  59.9 9.2 %collective-permute-start.15 = (bf16[512,128]{1,0:T(8,128)(2,1)S(1)}, bf16[512,128]{1,0:T(8,128)(2,1)S(1)}, u32[]{:S(2)}, u32[]{:S(2)}) collective-permute-start(bf16[512,128]{1,0:T(8,128)(2,1)S(1)} %get-tuple-element.54), channel_id=1, source_target_pairs={{0,4},{2,6},{4,0},{6,2},{8,12},{10,14},{12,8},{14,10},{1,5},{3,7},... | collective-permute-start | bytes 393224 | tf_op jit(solution)/shard_map/ppermute | solution.py:48
  61.9 13.2 %collective-permute-start.16 = (bf16[512,128]{1,0:T(8,128)(2,1)S(1)}, bf16[512,128]{1,0:T(8,128)(2,1)S(1)}, u32[]{:S(2)}, u32[]{:S(2)}) collective-permute-start(bf16[512,128]{1,0:T(8,128)(2,1)S(1)} %get-tuple-element.55), channel_id=1, source_target_pairs={{0,8},{2,10},{4,12},{6,14},{8,0},{10,2},{12,4},{14,6},{1,9},{3,11}... | collective-permute-start | bytes 393224 | tf_op jit(solution)/shard_map/ppermute | solution.py:48
  61.9 16.3 %collective-permute-start.17 = (bf16[512,128]{1,0:T(8,128)(2,1)S(1)}, bf16[512,128]{1,0:T(8,128)(2,1)S(1)}, u32[]{:S(2)}, u32[]{:S(2)}) collective-permute-start(bf16[512,128]{1,0:T(8,128)(2,1)S(1)} %get-tuple-element.56), channel_id=1, source_target_pairs={{0,12},{2,14},{4,8},{6,10},{8,4},{10,6},{12,0},{14,2},{1,13},{3,15... | collective-permute-start | bytes 393224 | tf_op jit(solution)/shard_map/ppermute | solution.py:48
  69.1 14.6 %collective-permute-start = (bf16[512,128]{1,0:T(8,128)(2,1)S(1)}, bf16[512,128]{1,0:T(8,128)(2,1)S(1)}, u32[]{:S(2)}, u32[]{:S(2)}) collective-permute-start(bf16[512,128]{1,0:T(8,128)(2,1)S(1)} %get-tuple-element.36), channel_id=1, source_target_pairs={{0,10},{2,8},{4,14},{6,12},{8,2},{10,0},{12,6},{14,4},{1,11},{3,9}... | collective-permute-start | bytes 393224 | tf_op jit(solution)/shard_map/ppermute | solution.py:48
  75.1 8.6 %collective-permute-start.1 = (bf16[512,128]{1,0:T(8,128)(2,1)S(1)}, bf16[512,128]{1,0:T(8,128)(2,1)S(1)}, u32[]{:S(2)}, u32[]{:S(2)}) collective-permute-start(bf16[512,128]{1,0:T(8,128)(2,1)S(1)} %get-tuple-element.37), channel_id=1, source_target_pairs={{0,14},{2,12},{4,10},{6,8},{8,6},{10,4},{12,2},{14,0},{1,15},{3,13... | collective-permute-start | bytes 393224 | tf_op jit(solution)/shard_map/ppermute | solution.py:48
  80.8 2.9 %copy-start.6 = (bf16[1,2,64]{2,1,0:T(2,128)(2,1)S(1)}, bf16[1,2,64]{2,1,0:T(2,128)(2,1)}, u32[]{:S(2)}) copy-start(bf16[1,2,64]{2,1,0:T(2,128)(2,1)} %refs_6_.3) | copy-start | bytes 772
  84.4 3.6 %collective-permute-start.18 = (f32[1,128]{1,0:T(1,128)S(1)}, f32[1,128]{1,0:T(1,128)S(1)}, u32[]{:S(2)}, u32[]{:S(2)}) collective-permute-start(f32[1,128]{1,0:T(1,128)S(1)} %get-tuple-element.65), channel_id=1, source_target_pairs={{0,2},{2,0},{4,6},{6,4},{8,10},{10,8},{12,14},{14,12},{1,3},{3,1},... | collective-permute-start | bytes 1544 | tf_op jit(solution)/shard_map/ppermute | solution.py:48
  86.4 1.6 %copy-start.7 = (f32[2,64]{1,0:T(2,128)S(1)}, f32[2,64]{1,0:T(2,128)}, u32[]{:S(2)}) copy-start(f32[2,64]{1,0:T(2,128)} %param.23) | copy-start | bytes 1540

commit v2 on v1

--- a/solution.py
+++ b/solution.py
@@ -184,9 +184,10 @@
 
 
 def key_read_kernel(
-    group_devices, held_ref, *refs
+    group_devices, *refs
 ):
-    relayed = refs[: group_devices - 1]
+    count = GROUPS * group_devices
+    held, refs = refs[:count], refs[count:]
     (
         taps_ref,
         query_ref,
@@ -200,7 +201,7 @@
         rates,
         scores,
         spikes,
-    ) = refs[group_devices - 1 :]
+    ) = refs
     repeats = HEADS // GROUPS
     sources = blocks.shape[0]
     half = keys_ref.shape[1] // 2
@@ -209,9 +210,8 @@
     me = lax.axis_index("sp")
     group, rank = me // group_devices, me % group_devices
     for offset in range(GROUPS):
-        blocks[(group ^ offset) * group_devices + rank] = held_ref[offset]
-        for shift in range(1, group_devices):
-            blocks[(group ^ offset) * group_devices + (rank ^ shift)] = relayed[shift - 1][offset]
+        for shift in range(group_devices):
+            blocks[(group ^ offset) * group_devices + (rank ^ shift)] = held[shift * GROUPS + offset][...]
     taps = []
     for k in range(5):
         tap = taps_ref[k, pl.ds(group, 1), :]
@@ -291,7 +291,7 @@
     tiles = span // LANES
     smem = pl.BlockSpec(memory_space=pltpu.SMEM)
     vmem = pl.BlockSpec(memory_space=pltpu.VMEM)
-    count = 1 + len(relayed)
+    count = len(held) + len(relayed)
     return pl.pallas_call(
         lambda *refs: key_read_kernel(group_devices, *refs),
         in_specs=[vmem] * (count + 2) + [smem, smem, vmem],
@@ -301,7 +301,7 @@
             jax.ShapeDtypeStruct((sources, 2 * heads, tiles, LANES), F32),
         ],
         scratch_shapes=[
-            pltpu.VMEM((sources,) + held.shape[1:], BF16),
+            pltpu.VMEM((sources,) + held[0].shape, BF16),
             pltpu.VMEM((half + 32, LANES), F32),
             pltpu.VMEM((heads, sources, tiles, LANES), F32),
             pltpu.VMEM((sources, tiles, LANES), F32),
@@ -310,7 +310,7 @@
         compiler_params=pltpu.CompilerParams(vmem_limit_bytes=VMEM_LIMIT),
         cost_estimate=pl.CostEstimate(flops=10**9, bytes_accessed=4 * 10**6, transcendentals=10**6),
         name="key_read",
-    )(*(on_chip(x) for x in [held, *relayed, taps, query]), offset, decay, on_chip(spikes))
+    )(*(on_chip(x) for x in [*held, *relayed, taps, query]), offset, decay, on_chip(spikes))
 
 
 def convolved(line, body, before, after, taps_ref, weight_ref, source, start_row, total):
@@ -577,10 +577,11 @@
         direct[offset - 1] = flip_permute(blocks[offset], offset * group_devices)
     early = value_blocks(rows, content_mapping_matrix, blocks[0], devices, cut, True)
     late = value_blocks(rows, content_mapping_matrix, early[0], devices, cut, False)
-    held = jnp.stack([blocks[0]] + direct)
+    held = [blocks[0]] + direct
     relayed = []
     for shift in range(1, group_devices):
-        relayed.append(flip_permute(held, shift))
+        for offset in range(GROUPS):
+            relayed.append(flip_permute(held[offset], shift))
     early_blocks, late_blocks = [early[0]], [late[0]]
     for offset in range(1, devices):
         early_blocks.append(flip_permute(early[offset], offset))
@@ -599,12 +600,9 @@
     )
     taps = content_smoothing_coefficients
     out, read, edges = early_rows(early_blocks, keys, weight, taps, cut)
-    across = [offset for offset in range(devices) if offset % group_devices]
-    along = [offset for offset in range(devices) if offset % group_devices == 0]
-    near = [offset for offset in across if offset < devices // 2]
-    final = [offset for offset in across if offset >= devices // 2]
-    for wave in (along, near):
-        out, read = late_rows(wave, late_blocks, edges, keys, weight, taps, read, out, cut)
+    half = devices // 2
+    first, final = list(range(half)), list(range(half, devices))
+    out, read = late_rows(first, late_blocks, edges, keys, weight, taps, read, out, cut)
     values, gated, group_sq = last_read(final, late_blocks, edges, weight, taps, read, newest_output_switch, cut)
     for level in range(group_devices.bit_length() - 1):
         group_sq = group_sq + flip_permute(group_sq, 2**level)

time: 88.8 us -> 94.4 us (1.063)
  starting transfers between devices: 37.6 us -> 42.2 us
  waiting for transfers between devices: 19.6 us -> 21 us
    ppermute x19 -> x22, starting transfers between devices: 37.6 us -> 42.2 us  [flip_permute(): return lax.ppermute(value, 'sp', pairs)]
    pallas_call x2 -> x1, Pallas kernels: 4.13 us -> 2.59 us  [late_rows(): pl.pallas_call(lambda *refs: late_kernel(cut, offsets, *refs), grid=(len(...]
    ppermute x19 -> x22, waiting for transfers between devices: 19.6 us -> 21 us  [flip_permute(): return lax.ppermute(value, 'sp', pairs)]
  transfers between devices with their start and end apart: 19 -> 22, of which waited for: 6 -> 5; matrix products, arithmetic and copies ran while one was open for 0% -> 0% of each run, Pallas kernels for 28% -> 14%
where the time goes in v2:
time: 94.4 us; the launch traced here: 94.2 us
  starting transfers between devices  42.2 us (45%)
  Pallas kernels  29.6 us (31%)
  waiting for transfers between devices  21 us (22%)
    ppermute x22, starting transfers between devices, flip_permute(): return lax.ppermute(value, 'sp', pairs)  42.2 us
    ppermute x22, waiting for transfers between devices, flip_permute(): return lax.ppermute(value, 'sp', pairs)  21 us
    pallas_call x2, Pallas kernels, value_blocks(): pl.pallas_call(kernel, grid=(width // tile,), in_specs=specs + [pl.BlockS...  11.2 us
    pallas_call x1, Pallas kernels, early_rows(): pl.pallas_call(lambda *refs: early_kernel(cut, *refs), grid=(sources,), i...  4.72 us
    pallas_call x1, Pallas kernels, key_blocks(): pl.pallas_call(lambda *refs: key_block_kernel(group_devices, *refs), grid...  4.63 us
    pallas_call x1, Pallas kernels, key_read(): pl.pallas_call(lambda *refs: key_read_kernel(group_devices, *refs), in_sp...  3.6 us
    pallas_call x1, Pallas kernels, late_rows(): pl.pallas_call(lambda *refs: late_kernel(cut, offsets, *refs), grid=(len(...  2.59 us
  transfers between devices with their start and end apart: 22, of which 5 were waited for; matrix products, arithmetic and copies ran while one was open for 0% of the time, Pallas kernels for 14%

profile of v2, /device:TPU:0, one launch (start us, length us, event | category | flops | bytes accessed | tf_op | source)
XLA Modules:
  0.0 94.2 jit_solution(8595418009408424527)
XLA Ops:
  0.6 4.6 %key_blocks.1 = (bf16[544,128]{1,0:T(8,128)(2,1)S(1)}, bf16[544,128]{1,0:T(8,128)(2,1)S(1)}, bf16[544,128]{1,0:T(8,128)(2,1)S(1)}, bf16[544,128]{1,0:T(8,128)(2,1)S(1)}) custom-call(bf16[1024,2048]{1,0:T(8,128)(2,1)} %bitcast.7, bf16[1024,2048]{1,0:T(8,128)(2,1)} %bitcast.8, bf16[2048,256]{1,0:T(8,128)(2,1)} %refs_2_.1, bf16[16,2048]{1,0:T(8,128)(2,1)} %bitcast.14), custom_call_target="tpu_custom_call" | custom-call | flops 1140850688 | bytes 4194304 | tf_op jit(solution)/shard_map/key_blocks/pallas_call | solution.py:102
  5.3 5.7 %early_values.1 = (bf16[520,128]{1,0:T(8,128)(2,1)S(1)}, bf16[520,128]{1,0:T(8,128)(2,1)S(1)}, bf16[520,128]{1,0:T(8,128)(2,1)S(1)}, bf16[520,128]{1,0:T(8,128)(...) custom-call(bf16[1024,2048]{1,0:T(8,128)(2,1)} %bitcast.9, ...), custom_call_target="tpu_custom_call" | custom-call | flops 2181038080 | bytes 6324224 | tf_op jit(solution)/shard_map/early_values/pallas_call | solution.py:169
  11.0 5.5 %late_values.1 = (bf16[512,128]{1,0:T(8,128)(2,1)S(1)}, bf16[512,128]{1,0:T(8,128)(2,1)S(1)}, bf16[512,128]{1,0:T(8,128)(2,1)S(1)}, bf16[512,128]{1,0:T(8,128)(2...) custom-call(bf16[1024,2048]{1,0:T(8,128)(2,1)} %bitcast.12, ...), custom_call_target="tpu_custom_call" | custom-call | flops 2147483648 | bytes 6291456 | tf_op jit(solution)/shard_map/late_values/pallas_call | solution.py:169
  16.6 3.1 %collective-permute-start.18 = (bf16[512,128]{1,0:T(8,128)(2,1)S(1)}, bf16[512,128]{1,0:T(8,128)(2,1)S(1)}, u32[]{:S(2)}, u32[]{:S(2)}) collective-permute-start(bf16[512,128]{1,0:T(8,128)(2,1)S(1)} %get-tuple-element.52), channel_id=1, source_target_pairs={{0,2},{2,0},{4,6},{6,4},{8,10},{10,8},{12,14},{14,12},{1,3},{3,1},... | collective-permute-start | bytes 393224 | tf_op jit(solution)/shard_map/ppermute | solution.py:48
  19.6 1.6 %collective-permute-start.11 = (bf16[544,128]{1,0:T(8,128)(2,1)S(1)}, bf16[544,128]{1,0:T(8,128)(2,1)S(1)}, u32[]{:S(2)}, u32[]{:S(2)}) collective-permute-start(bf16[544,128]{1,0:T(8,128)(2,1)S(1)} %get-tuple-element.45), channel_id=1, source_target_pairs={{0,4},{2,6},{4,0},{6,2},{8,12},{10,14},{12,8},{14,10},{1,5},{3,7},... | collective-permute-start | bytes 417800 | tf_op jit(solution)/shard_map/ppermute | solution.py:48
  21.2 2.6 %collective-permute-start.12 = (bf16[544,128]{1,0:T(8,128)(2,1)S(1)}, bf16[544,128]{1,0:T(8,128)(2,1)S(1)}, u32[]{:S(2)}, u32[]{:S(2)}) collective-permute-start(bf16[544,128]{1,0:T(8,128)(2,1)S(1)} %get-tuple-element.46), channel_id=1, source_target_pairs={{0,8},{2,10},{4,12},{6,14},{8,0},{10,2},{12,4},{14,6},{1,9},{3,11}... | collective-permute-start | bytes 417800 | tf_op jit(solution)/shard_map/ppermute | solution.py:48
  24.0 0.7 collective-permute-start.19
  24.7 0.5 collective-permute-start.4
  25.2 7.5 %collective-permute-done.19.refs_2_ = bf16[512,128]{1,0:T(8,128)(2,1)S(1)} collective-permute-done((bf16[512,128]{1,0:T(8,128)(2,1)S(1)}, bf16[512,128]{1,0:T(8,128)(2,1)S(1)}, u32[]{:S(2)}, u32[]{:S(2)}) %collective-permute-start.19) | collective-permute-done | bytes 131104 | tf_op jit(solution)/shard_map/ppermute | solution.py:48
  33.1 1.6 %collective-permute-start.15 = (bf16[544,128]{1,0:T(8,128)(2,1)S(1)}, bf16[544,128]{1,0:T(8,128)(2,1)S(1)}, u32[]{:S(2)}, u32[]{:S(2)}) collective-permute-start(bf16[544,128]{1,0:T(8,128)(2,1)S(1)} %collective-permute-done.11.refs_1_), channel_id=1, source_target_pairs={{0,2},{2,0},{4,6},{6,4},{8,10},{10,8},{12,14},{14,12},{1,3},{3,1},... | collective-permute-start | bytes 417800 | tf_op jit(solution)/shard_map/ppermute | solution.py:48
  34.7 0.5 collective-permute-start.16
  35.2 1.6 %collective-permute-start.17 = (bf16[544,128]{1,0:T(8,128)(2,1)S(1)}, bf16[544,128]{1,0:T(8,128)(2,1)S(1)}, u32[]{:S(2)}, u32[]{:S(2)}) collective-permute-start(bf16[544,128]{1,0:T(8,128)(2,1)S(1)} %collective-permute-done.13.refs_3_), channel_id=1, source_target_pairs={{0,2},{2,0},{4,6},{6,4},{8,10},{10,8},{12,14},{14,12},{1,3},{3,1},... | collective-permute-start | bytes 417800 | tf_op jit(solution)/shard_map/ppermute | solution.py:48
  36.7 2.5 %collective-permute-start.5 = (bf16[520,128]{1,0:T(8,128)(2,1)S(1)}, bf16[520,128]{1,0:T(8,128)(2,1)S(1)}, u32[]{:S(2)}, u32[]{:S(2)}) collective-permute-start(bf16[520,128]{1,0:T(8,128)(2,1)S(1)} %get-tuple-element.39), channel_id=1, source_target_pairs={{0,4},{2,6},{4,0},{6,2},{8,12},{10,14},{12,8},{14,10},{1,5},{3,7},... | collective-permute-start | bytes 399368 | tf_op jit(solution)/shard_map/ppermute | solution.py:48
  39.2 3.0 %collective-permute-done.5.refs_2_ = bf16[520,128]{1,0:T(8,128)(2,1)S(1)} collective-permute-done((bf16[520,128]{1,0:T(8,128)(2,1)S(1)}, bf16[520,128]{1,0:T(8,128)(2,1)S(1)}, u32[]{:S(2)}, u32[]{:S(2)}) %collective-permute-start.5) | collective-permute-done | bytes 133152 | tf_op jit(solution)/shard_map/ppermute | solution.py:48
  42.2 1.9 %collective-permute-start.6 = (bf16[520,128]{1,0:T(8,128)(2,1)S(1)}, bf16[520,128]{1,0:T(8,128)(2,1)S(1)}, u32[]{:S(2)}, u32[]{:S(2)}) collective-permute-start(bf16[520,128]{1,0:T(8,128)(2,1)S(1)} %get-tuple-element.40), channel_id=1, source_target_pairs={{0,6},{2,4},{4,2},{6,0},{8,14},{10,12},{12,10},{14,8},{1,7},{3,5},... | collective-permute-start | bytes 399368 | tf_op jit(solution)/shard_map/ppermute | solution.py:48
  44.1 2.9 %collective-permute-start.7 = (bf16[520,128]{1,0:T(8,128)(2,1)S(1)}, bf16[520,128]{1,0:T(8,128)(2,1)S(1)}, u32[]{:S(2)}, u32[]{:S(2)}) collective-permute-start(bf16[520,128]{1,0:T(8,128)(2,1)S(1)} %get-tuple-element.41), channel_id=1, source_target_pairs={{0,8},{2,10},{4,12},{6,14},{8,0},{10,2},{12,4},{14,6},{1,9},{3,11}... | collective-permute-start | bytes 399368 | tf_op jit(solution)/shard_map/ppermute | solution.py:48
  47.0 3.1 %collective-permute-start.8 = (bf16[520,128]{1,0:T(8,128)(2,1)S(1)}, bf16[520,128]{1,0:T(8,128)(2,1)S(1)}, u32[]{:S(2)}, u32[]{:S(2)}) collective-permute-start(bf16[520,128]{1,0:T(8,128)(2,1)S(1)} %get-tuple-element.42), channel_id=1, source_target_pairs={{0,10},{2,8},{4,14},{6,12},{8,2},{10,0},{12,6},{14,4},{1,11},{3,9}... | collective-permute-start | bytes 399368 | tf_op jit(solution)/shard_map/ppermute | solution.py:48
  50.1 1.8 %collective-permute-start.9 = (bf16[520,128]{1,0:T(8,128)(2,1)S(1)}, bf16[520,128]{1,0:T(8,128)(2,1)S(1)}, u32[]{:S(2)}, u32[]{:S(2)}) collective-permute-start(bf16[520,128]{1,0:T(8,128)(2,1)S(1)} %get-tuple-element.43), channel_id=1, source_target_pairs={{0,12},{2,14},{4,8},{6,10},{8,4},{10,6},{12,0},{14,2},{1,13},{3,15... | collective-permute-start | bytes 399368 | tf_op jit(solution)/shard_map/ppermute | solution.py:48
  51.9 2.0 %collective-permute-start.10 = (bf16[520,128]{1,0:T(8,128)(2,1)S(1)}, bf16[520,128]{1,0:T(8,128)(2,1)S(1)}, u32[]{:S(2)}, u32[]{:S(2)}) collective-permute-start(bf16[520,128]{1,0:T(8,128)(2,1)S(1)} %get-tuple-element.44), channel_id=1, source_target_pairs={{0,14},{2,12},{4,10},{6,8},{8,6},{10,4},{12,2},{14,0},{1,15},{3,13... | collective-permute-start | bytes 399368 | tf_op jit(solution)/shard_map/ppermute | solution.py:48
  53.9 3.6 %key_read.1 = (bf16[8,1024,128]{2,1,0:T(8,128)(2,1)S(1)}, f32[8,4,8,128]{3,2,1,0:T(8,128)S(1)}) custom-call(bf16[544,128]{1,0:T(8,128)(2,1)S(1)} %get-tuple-element.32.refs_4_.refs_0_, bf16[544,128]{1,0:T(8,128)(2,1)S(1)} %collective-permute-done.11.refs_1_, bf16[544,128]{1,0:T(8,128)(2,1)S(1)} %collective-permute-done.12.refs_2_, ...), custom_call_target="tpu_custom_call" | custom-call | flops 1000000000 | bytes 4000000 | tf_op jit(solution)/shard_map/key_read/pallas_call | solution.py:295
  57.5 0.6 collective-permute-start
  58.1 6.5 %collective-permute-done.7.refs_4_ = bf16[520,128]{1,0:T(8,128)(2,1)S(1)} collective-permute-done((bf16[520,128]{1,0:T(8,128)(2,1)S(1)}, bf16[520,128]{1,0:T(8,128)(2,1)S(1)}, u32[]{:S(2)}, u32[]{:S(2)}) %collective-permute-start.7) | collective-permute-done | bytes 133152 | tf_op jit(solution)/shard_map/ppermute | solution.py:48
  65.1 3.3 %collective-permute-done.8.refs_5_ = bf16[520,128]{1,0:T(8,128)(2,1)S(1)} collective-permute-done((bf16[520,128]{1,0:T(8,128)(2,1)S(1)}, bf16[520,128]{1,0:T(8,128)(2,1)S(1)}, u32[]{:S(2)}, u32[]{:S(2)}) %collective-permute-start.8) | collective-permute-done | bytes 133152 | tf_op jit(solution)/shard_map/ppermute | solution.py:48
  68.4 5.2 %collective-permute-start.2 = (bf16[512,128]{1,0:T(8,128)(2,1)S(1)}, bf16[512,128]{1,0:T(8,128)(2,1)S(1)}, u32[]{:S(2)}, u32[]{:S(2)}) collective-permute-start(bf16[512,128]{1,0:T(8,128)(2,1)S(1)} %get-tuple-element.36), channel_id=1, source_target_pairs={{0,12},{2,14},{4,8},{6,10},{8,4},{10,6},{12,0},{14,2},{1,13},{3,15... | collective-permute-start | bytes 393224 | tf_op jit(solution)/shard_map/ppermute | solution.py:48
  73.6 8.1 %collective-permute-start.20 = (bf16[512,128]{1,0:T(8,128)(2,1)S(1)}, bf16[512,128]{1,0:T(8,128)(2,1)S(1)}, u32[]{:S(2)}, u32[]{:S(2)}) collective-permute-start(bf16[512,128]{1,0:T(8,128)(2,1)S(1)} %get-tuple-element.54), channel_id=1, source_target_pairs={{0,6},{2,4},{4,2},{6,0},{8,14},{10,12},{12,10},{14,8},{1,7},{3,5},... | collective-permute-start | bytes 393224 | tf_op jit(solution)/shard_map/ppermute | solution.py:48
  81.7 4.7 %early_rows.1 = (bf16[8,2048,128]{2,1,0:T(8,128)(2,1)}, f32[32,128]{1,0:T(8,128)S(1)}, bf16[8,32,128]{2,1,0:T(8,128)(2,1)S(1)}) custom-call(bf16[520,128]{1,0:T(8,128)(2,1)S(1)} %get-tuple-element.33.refs_2_.refs_0_, bf16[520,128]{1,0:T(8,128)(2,1)S(1)} %collective-permute-done.4.refs_1_, bf16[520,128]{1,0:T(8,128)(2,1)S(1)} %collective-permute-done.5.refs_2_, ...), custom_call_target="tpu_custom_call" | custom-call | flops 2000000000 | bytes 6000000 | tf_op jit(solution)/shard_map/early_rows/pallas_call | solution.py:399
  86.4 2.6 %late_rows.1 = (bf16[8,2048,128]{2,1,0:T(8,128)(2,1)}, f32[32,128]{1,0:T(8,128)S(1)}) custom-call(bf16[512,128]{1,0:T(8,128)(2,1)S(1)} %get-tuple-element.51.refs_0_, bf16[512,128]{1,0:T(8,128)(2,1)S(1)} %collective-permute-done.18.refs_1_, bf16[512,128]{1,0:T(8,128)(2,1)S(1)} %collective-permute-done.19.refs_2_, ...), custom_call_target="tpu_custom_call", output_to_operand_aliasing={{0}: (9, {})} | custom-call | flops 1000000000 | bytes 2000000 | tf_op jit(solution)/shard_map/late_rows/pallas_call | solution.py:471
  89.1 1.0 %last_read.1 = (bf16[4,512,128]{2,1,0:T(8,128)(2,1)S(1)}, f32[2,64]{1,0:T(2,128)S(1)}, f32[1,128]{1,0:T(1,128)S(1)}) custom-call(bf16[512,128]{1,0:T(8,128)(2,1)S(1)} %collective-permute-done.refs_0_, bf16[512,128]{1,0:T(8,128)(2,1)S(1)} %collective-permute-done.1.refs_1_, bf16[512,128]{1,0:T(8,128)(2,1)S(1)} %collective-permute-done.2.refs_2_, ...), custom_call_target="tpu_custom_call" | custom-call | flops 1000000000 | bytes 1000000 | tf_op jit(solution)/shard_map/last_read/pallas_call | solution.py:512
  90.1 1.1 %collective-permute-start.21 = (f32[1,128]{1,0:T(1,128)S(1)}, f32[1,128]{1,0:T(1,128)S(1)}, u32[]{:S(2)}, u32[]{:S(2)}) collective-permute-start(f32[1,128]{1,0:T(1,128)S(1)} %get-tuple-element.61), channel_id=1, source_target_pairs={{0,2},{2,0},{4,6},{6,4},{8,10},{10,8},{12,14},{14,12},{1,3},{3,1},... | collective-permute-start | bytes 1544 | tf_op jit(solution)/shard_map/ppermute | solution.py:48
  91.1 1.8 %last_rows.1 = bf16[8,2048,128]{2,1,0:T(8,128)(2,1)} custom-call(bf16[4,512,128]{2,1,0:T(8,128)(2,1)S(1)} %get-tuple-element.58.refs_0_, bf16[8,1024,128]{2,1,0:T(8,128)(2,1)S(1)} %get-tuple-element.48.refs_8_.refs_5_.refs_1_, bf16[8,2048,128]{2,1,0:T(8,128)(2,1)} %get-tuple-element.59.refs_2_), custom_call_target="tpu_custom_call", output_to_operand_aliasing={{}: (2, {})} | custom-call | flops 1000000000 | bytes 2000000 | tf_op jit(solution)/shard_map/last_rows/pallas_call | solution.py:538
  93.0 0.7 collective-permute-done.21
  93.7 0.5 fusion
  (38 shorter events, 1.2 us)
Async XLA Ops:
  10.9 43.0 %copy-start.1 = (f32[1,2,8192]{2,1,0:T(2,128)S(1)}, f32[1,2,8192]{2,1,0:T(2,128)}, u32[]{:S(2)}) copy-start(f32[1,2,8192]{2,1,0:T(2,128)} %refs_12_.1) | copy-start | bytes 196612
  10.9 42.9 %copy-start.2 = (f32[5,4,64]{2,1,0:T(4,128)S(1)}, f32[5,4,64]{2,1,0:T(4,128)}, u32[]{:S(2)}) copy-start(f32[5,4,64]{2,1,0:T(4,128)} %refs_8_.2) | copy-start | bytes 15364
  11.0 42.9 %copy-start.3 = (bf16[1,4,64]{2,1,0:T(4,128)(2,1)S(1)}, bf16[1,4,64]{2,1,0:T(4,128)(2,1)}, u32[]{:S(2)}) copy-start(bf16[1,4,64]{2,1,0:T(4,128)(2,1)} %refs_9_.1) | copy-start | bytes 1540
  11.0 42.9 %copy-start.4 = (f32[2]{0:T(128)S(1)}, f32[2]{0:T(128)}, u32[]{:S(2)}) copy-start(f32[2]{0:T(128)} %refs_10_.2) | copy-start | bytes 28
  11.0 42.9 %copy-start.5 = (f32[2]{0:T(128)S(1)}, f32[2]{0:T(128)}, u32[]{:S(2)}) copy-start(f32[2]{0:T(128)} %refs_11_.1) | copy-start | bytes 28
  11.0 70.7 %copy-start = (f32[5,2,64]{2,1,0:T(2,128)S(1)}, f32[5,2,64]{2,1,0:T(2,128)}, u32[]{:S(2)}) copy-start(f32[5,2,64]{2,1,0:T(2,128)} %refs_6_.1) | copy-start | bytes 7684
  16.6 8.1 %collective-permute-start.18 = (bf16[512,128]{1,0:T(8,128)(2,1)S(1)}, bf16[512,128]{1,0:T(8,128)(2,1)S(1)}, u32[]{:S(2)}, u32[]{:S(2)}) collective-permute-start(bf16[512,128]{1,0:T(8,128)(2,1)S(1)} %get-tuple-element.52), channel_id=1, source_target_pairs={{0,2},{2,0},{4,6},{6,4},{8,10},{10,8},{12,14},{14,12},{1,3},{3,1},... | collective-permute-start | bytes 393224 | tf_op jit(solution)/shard_map/ppermute | solution.py:48
  19.6 13.5 %collective-permute-start.11 = (bf16[544,128]{1,0:T(8,128)(2,1)S(1)}, bf16[544,128]{1,0:T(8,128)(2,1)S(1)}, u32[]{:S(2)}, u32[]{:S(2)}) collective-permute-start(bf16[544,128]{1,0:T(8,128)(2,1)S(1)} %get-tuple-element.45), channel_id=1, source_target_pairs={{0,4},{2,6},{4,0},{6,2},{8,12},{10,14},{12,8},{14,10},{1,5},{3,7},... | collective-permute-start | bytes 417800 | tf_op jit(solution)/shard_map/ppermute | solution.py:48
  21.2 13.5 %collective-permute-start.12 = (bf16[544,128]{1,0:T(8,128)(2,1)S(1)}, bf16[544,128]{1,0:T(8,128)(2,1)S(1)}, u32[]{:S(2)}, u32[]{:S(2)}) collective-permute-start(bf16[544,128]{1,0:T(8,128)(2,1)S(1)} %get-tuple-element.46), channel_id=1, source_target_pairs={{0,8},{2,10},{4,12},{6,14},{8,0},{10,2},{12,4},{14,6},{1,9},{3,11}... | collective-permute-start | bytes 417800 | tf_op jit(solution)/shard_map/ppermute | solution.py:48
  23.8 11.4 %collective-permute-start.13 = (bf16[544,128]{1,0:T(8,128)(2,1)S(1)}, bf16[544,128]{1,0:T(8,128)(2,1)S(1)}, u32[]{:S(2)}, u32[]{:S(2)}) collective-permute-start(bf16[544,128]{1,0:T(8,128)(2,1)S(1)} %get-tuple-element.47), channel_id=1, source_target_pairs={{0,12},{2,14},{4,8},{6,10},{8,4},{10,6},{12,0},{14,2},{1,13},{3,15... | collective-permute-start | bytes 417800 | tf_op jit(solution)/shard_map/ppermute | solution.py:48
  24.0 8.7 %collective-permute-start.19 = (bf16[512,128]{1,0:T(8,128)(2,1)S(1)}, bf16[512,128]{1,0:T(8,128)(2,1)S(1)}, u32[]{:S(2)}, u32[]{:S(2)}) collective-permute-start(bf16[512,128]{1,0:T(8,128)(2,1)S(1)} %get-tuple-element.53), channel_id=1, source_target_pairs={{0,4},{2,6},{4,0},{6,2},{8,12},{10,14},{12,8},{14,10},{1,5},{3,7},... | collective-permute-start | bytes 393224 | tf_op jit(solution)/shard_map/ppermute | solution.py:48
  24.7 12.0 %collective-permute-start.4 = (bf16[520,128]{1,0:T(8,128)(2,1)S(1)}, bf16[520,128]{1,0:T(8,128)(2,1)S(1)}, u32[]{:S(2)}, u32[]{:S(2)}) collective-permute-start(bf16[520,128]{1,0:T(8,128)(2,1)S(1)} %get-tuple-element.38), channel_id=1, source_target_pairs={{0,2},{2,0},{4,6},{6,4},{8,10},{10,8},{12,14},{14,12},{1,3},{3,1},... | collective-permute-start | bytes 399368 | tf_op jit(solution)/shard_map/ppermute | solution.py:48
  32.7 11.4 %collective-permute-start.14 = (bf16[544,128]{1,0:T(8,128)(2,1)S(1)}, bf16[544,128]{1,0:T(8,128)(2,1)S(1)}, u32[]{:S(2)}, u32[]{:S(2)}) collective-permute-start(bf16[544,128]{1,0:T(8,128)(2,1)S(1)} %get-tuple-element.32.refs_4_.refs_0_), channel_id=1, source_target_pairs={{0,2},{2,0},{4,6},{6,4},{8,10},{10,8},{12,14},{14,12},{1,3},{3,1},... | collective-permute-start | bytes 417800 | tf_op jit(solution)/shard_map/ppermute | solution.py:48
  33.1 13.8 %collective-permute-start.15 = (bf16[544,128]{1,0:T(8,128)(2,1)S(1)}, bf16[544,128]{1,0:T(8,128)(2,1)S(1)}, u32[]{:S(2)}, u32[]{:S(2)}) collective-permute-start(bf16[544,128]{1,0:T(8,128)(2,1)S(1)} %collective-permute-done.11.refs_1_), channel_id=1, source_target_pairs={{0,2},{2,0},{4,6},{6,4},{8,10},{10,8},{12,14},{14,12},{1,3},{3,1},... | collective-permute-start | bytes 417800 | tf_op jit(solution)/shard_map/ppermute | solution.py:48
  34.7 15.3 %collective-permute-start.16 = (bf16[544,128]{1,0:T(8,128)(2,1)S(1)}, bf16[544,128]{1,0:T(8,128)(2,1)S(1)}, u32[]{:S(2)}, u32[]{:S(2)}) collective-permute-start(bf16[544,128]{1,0:T(8,128)(2,1)S(1)} %collective-permute-done.12.refs_2_), channel_id=1, source_target_pairs={{0,2},{2,0},{4,6},{6,4},{8,10},{10,8},{12,14},{14,12},{1,3},{3,1},... | collective-permute-start | bytes 417800 | tf_op jit(solution)/shard_map/ppermute | solution.py:48
  35.2 16.7 %collective-permute-start.17 = (bf16[544,128]{1,0:T(8,128)(2,1)S(1)}, bf16[544,128]{1,0:T(8,128)(2,1)S(1)}, u32[]{:S(2)}, u32[]{:S(2)}) collective-permute-start(bf16[544,128]{1,0:T(8,128)(2,1)S(1)} %collective-permute-done.13.refs_3_), channel_id=1, source_target_pairs={{0,2},{2,0},{4,6},{6,4},{8,10},{10,8},{12,14},{14,12},{1,3},{3,1},... | collective-permute-start | bytes 417800 | tf_op jit(solution)/shard_map/ppermute | solution.py:48
  36.7 5.5 %collective-permute-start.5 = (bf16[520,128]{1,0:T(8,128)(2,1)S(1)}, bf16[520,128]{1,0:T(8,128)(2,1)S(1)}, u32[]{:S(2)}, u32[]{:S(2)}) collective-permute-start(bf16[520,128]{1,0:T(8,128)(2,1)S(1)} %get-tuple-element.39), channel_id=1, source_target_pairs={{0,4},{2,6},{4,0},{6,2},{8,12},{10,14},{12,8},{14,10},{1,5},{3,7},... | collective-permute-start | bytes 399368 | tf_op jit(solution)/shard_map/ppermute | solution.py:48
  42.2 15.3 %collective-permute-start.6 = (bf16[520,128]{1,0:T(8,128)(2,1)S(1)}, bf16[520,128]{1,0:T(8,128)(2,1)S(1)}, u32[]{:S(2)}, u32[]{:S(2)}) collective-permute-start(bf16[520,128]{1,0:T(8,128)(2,1)S(1)} %get-tuple-element.40), channel_id=1, source_target_pairs={{0,6},{2,4},{4,2},{6,0},{8,14},{10,12},{12,10},{14,8},{1,7},{3,5},... | collective-permute-start | bytes 399368 | tf_op jit(solution)/shard_map/ppermute | solution.py:48
  44.1 20.5 %collective-permute-start.7 = (bf16[520,128]{1,0:T(8,128)(2,1)S(1)}, bf16[520,128]{1,0:T(8,128)(2,1)S(1)}, u32[]{:S(2)}, u32[]{:S(2)}) collective-permute-start(bf16[520,128]{1,0:T(8,128)(2,1)S(1)} %get-tuple-element.41), channel_id=1, source_target_pairs={{0,8},{2,10},{4,12},{6,14},{8,0},{10,2},{12,4},{14,6},{1,9},{3,11}... | collective-permute-start | bytes 399368 | tf_op jit(solution)/shard_map/ppermute | solution.py:48
  47.0 21.5 %collective-permute-start.8 = (bf16[520,128]{1,0:T(8,128)(2,1)S(1)}, bf16[520,128]{1,0:T(8,128)(2,1)S(1)}, u32[]{:S(2)}, u32[]{:S(2)}) collective-permute-start(bf16[520,128]{1,0:T(8,128)(2,1)S(1)} %get-tuple-element.42), channel_id=1, source_target_pairs={{0,10},{2,8},{4,14},{6,12},{8,2},{10,0},{12,6},{14,4},{1,11},{3,9}... | collective-permute-start | bytes 399368 | tf_op jit(solution)/shard_map/ppermute | solution.py:48
  50.1 23.5 %collective-permute-start.9 = (bf16[520,128]{1,0:T(8,128)(2,1)S(1)}, bf16[520,128]{1,0:T(8,128)(2,1)S(1)}, u32[]{:S(2)}, u32[]{:S(2)}) collective-permute-start(bf16[520,128]{1,0:T(8,128)(2,1)S(1)} %get-tuple-element.43), channel_id=1, source_target_pairs={{0,12},{2,14},{4,8},{6,10},{8,4},{10,6},{12,0},{14,2},{1,13},{3,15... | collective-permute-start | bytes 399368 | tf_op jit(solution)/shard_map/ppermute | solution.py:48
  51.9 21.7 %collective-permute-start.10 = (bf16[520,128]{1,0:T(8,128)(2,1)S(1)}, bf16[520,128]{1,0:T(8,128)(2,1)S(1)}, u32[]{:S(2)}, u32[]{:S(2)}) collective-permute-start(bf16[520,128]{1,0:T(8,128)(2,1)S(1)} %get-tuple-element.44), channel_id=1, source_target_pairs={{0,14},{2,12},{4,10},{6,8},{8,6},{10,4},{12,2},{14,0},{1,15},{3,13... | collective-permute-start | bytes 399368 | tf_op jit(solution)/shard_map/ppermute | solution.py:48
  57.5 31.5 %collective-permute-start = (bf16[512,128]{1,0:T(8,128)(2,1)S(1)}, bf16[512,128]{1,0:T(8,128)(2,1)S(1)}, u32[]{:S(2)}, u32[]{:S(2)}) collective-permute-start(bf16[512,128]{1,0:T(8,128)(2,1)S(1)} %get-tuple-element.34), channel_id=1, source_target_pairs={{0,8},{2,10},{4,12},{6,14},{8,0},{10,2},{12,4},{14,6},{1,9},{3,11}... | collective-permute-start | bytes 393224 | tf_op jit(solution)/shard_map/ppermute | solution.py:48
  64.7 24.4 %collective-permute-start.1 = (bf16[512,128]{1,0:T(8,128)(2,1)S(1)}, bf16[512,128]{1,0:T(8,128)(2,1)S(1)}, u32[]{:S(2)}, u32[]{:S(2)}) collective-permute-start(bf16[512,128]{1,0:T(8,128)(2,1)S(1)} %get-tuple-element.35), channel_id=1, source_target_pairs={{0,10},{2,8},{4,14},{6,12},{8,2},{10,0},{12,6},{14,4},{1,11},{3,9}... | collective-permute-start | bytes 393224 | tf_op jit(solution)/shard_map/ppermute | solution.py:48
  68.4 20.6 %collective-permute-start.2 = (bf16[512,128]{1,0:T(8,128)(2,1)S(1)}, bf16[512,128]{1,0:T(8,128)(2,1)S(1)}, u32[]{:S(2)}, u32[]{:S(2)}) collective-permute-start(bf16[512,128]{1,0:T(8,128)(2,1)S(1)} %get-tuple-element.36), channel_id=1, source_target_pairs={{0,12},{2,14},{4,8},{6,10},{8,4},{10,6},{12,0},{14,2},{1,13},{3,15... | collective-permute-start | bytes 393224 | tf_op jit(solution)/shard_map/ppermute | solution.py:48
  73.6 15.4 %collective-permute-start.3 = (bf16[512,128]{1,0:T(8,128)(2,1)S(1)}, bf16[512,128]{1,0:T(8,128)(2,1)S(1)}, u32[]{:S(2)}, u32[]{:S(2)}) collective-permute-start(bf16[512,128]{1,0:T(8,128)(2,1)S(1)} %get-tuple-element.37), channel_id=1, source_target_pairs={{0,14},{2,12},{4,10},{6,8},{8,6},{10,4},{12,2},{14,0},{1,15},{3,13... | collective-permute-start | bytes 393224 | tf_op jit(solution)/shard_map/ppermute | solution.py:48
  73.6 12.8 %collective-permute-start.20 = (bf16[512,128]{1,0:T(8,128)(2,1)S(1)}, bf16[512,128]{1,0:T(8,128)(2,1)S(1)}, u32[]{:S(2)}, u32[]{:S(2)}) collective-permute-start(bf16[512,128]{1,0:T(8,128)(2,1)S(1)} %get-tuple-element.54), channel_id=1, source_target_pairs={{0,6},{2,4},{4,2},{6,0},{8,14},{10,12},{12,10},{14,8},{1,7},{3,5},... | collective-permute-start | bytes 393224 | tf_op jit(solution)/shard_map/ppermute | solution.py:48
  86.4 2.6 %copy-start.6 = (bf16[1,2,64]{2,1,0:T(2,128)(2,1)S(1)}, bf16[1,2,64]{2,1,0:T(2,128)(2,1)}, u32[]{:S(2)}) copy-start(bf16[1,2,64]{2,1,0:T(2,128)(2,1)} %refs_8_.3) | copy-start | bytes 772
  90.1 3.6 %collective-permute-start.21 = (f32[1,128]{1,0:T(1,128)S(1)}, f32[1,128]{1,0:T(1,128)S(1)}, u32[]{:S(2)}, u32[]{:S(2)}) collective-permute-start(f32[1,128]{1,0:T(1,128)S(1)} %get-tuple-element.61), channel_id=1, source_target_pairs={{0,2},{2,0},{4,6},{6,4},{8,10},{10,8},{12,14},{14,12},{1,3},{3,1},... | collective-permute-start | bytes 1544 | tf_op jit(solution)/shard_map/ppermute | solution.py:48
  91.1 2.6 %copy-start.7 = (f32[2,64]{1,0:T(2,128)S(1)}, f32[2,64]{1,0:T(2,128)}, u32[]{:S(2)}) copy-start(f32[2,64]{1,0:T(2,128)} %param.23) | copy-start | bytes 1540

commit v3 on v2

--- a/solution.py
+++ b/solution.py
@@ -48,18 +48,13 @@
     return lax.ppermute(value, "sp", pairs)
 
 
-def key_block_kernel(group_devices, low_ref, high_ref, wk_ref, wr_ref, *rest):
-    outs, (packed, rates) = rest[:-2], rest[-2:]
-    repeats = HEADS // GROUPS
+def key_block_kernel(group_devices, low_ref, high_ref, wk_ref, *rest):
+    outs, packed = rest[:-1], rest[-1]
     step = pl.program_id(0)
     rows = low_ref.shape[0]
-    tiles = rows // LANES
-    half_tiles = rates.shape[0] // 2
-    wk, wr = wk_ref[...], wr_ref[...]
     both = jnp.concatenate([low_ref[...], high_ref[...]], axis=0)
-    k_both = rounded(jnp.dot(both, wk, preferred_element_type=F32))
+    k_both = rounded(jnp.dot(both, wk_ref[...], preferred_element_type=F32))
     k_low, k_high = k_both[:rows], k_both[rows:]
-    r_both = lax.dot_general(both, wr, (((1,), (1,)), ((), ())), preferred_element_type=F32).astype(BF16)
     left = lane_index((rows, LANES)) < STATE
     for group in range(GROUPS):
         column = slice(group // 2 * LANES, (group // 2 + 1) * LANES)
@@ -69,36 +64,20 @@
         else:
             a = pltpu.roll(a, STATE, 1)
         packed[group, pl.ds(pl.multiple_of(step * rows, rows), rows), :] = jnp.where(left, a, b).astype(BF16)
-    eye = (
-        lax.broadcasted_iota(jnp.int32, (HEADS, HEADS), 0) == lax.broadcasted_iota(jnp.int32, (HEADS, HEADS), 1)
-    ).astype(BF16)
-    for part in range(2):
-        r = r_both[part * rows : (part + 1) * rows]
-        turned = lax.dot_general(eye, r, (((1,), (1,)), ((), ())), preferred_element_type=F32)
-        for tile in range(tiles):
-            rates[part * half_tiles + step * tiles + tile] = turned[:, tile * LANES : (tile + 1) * LANES]
 
     @pl.when(step == pl.num_programs(0) - 1)
     def _():
-        half = packed.shape[1] - 2 * half_tiles * repeats
-        for group in range(GROUPS):
-            tail = jnp.concatenate(
-                [rates[tile, group * repeats : (group + 1) * repeats, :] for tile in range(2 * half_tiles)], axis=0
-            )
-            packed[group, half:, :] = tail.astype(BF16)
         own = lax.axis_index("sp") // group_devices
         for offset, out in enumerate(outs):
             out[...] = packed[own ^ offset]
 
 
-def key_blocks(rows, wk, wr, group_devices):
+def key_blocks(rows, wk, group_devices):
     span, model = rows.shape
-    repeats = HEADS // GROUPS
     half = span // 2
     tile = half // 2
     steps = half // tile
-    height = half + repeats * span // LANES
-    block = jax.ShapeDtypeStruct((height, LANES), BF16)
+    block = jax.ShapeDtypeStruct((half, LANES), BF16)
     return pl.pallas_call(
         lambda *refs: key_block_kernel(group_devices, *refs),
         grid=(steps,),
@@ -106,38 +85,99 @@
             pl.BlockSpec((tile, model), lambda i: (i, 0)),
             pl.BlockSpec((tile, model), lambda i: (i + steps, 0)),
             whole(wk.shape),
-            whole(wr.shape),
-        ],
-        out_specs=[whole((height, LANES))] * GROUPS,
+        ],
+        out_specs=[whole(block.shape)] * GROUPS,
         out_shape=[block] * GROUPS,
-        scratch_shapes=[
-            pltpu.VMEM((GROUPS, height, LANES), BF16),
-            pltpu.VMEM((span // LANES, HEADS, LANES), F32),
-        ],
+        scratch_shapes=[pltpu.VMEM((GROUPS,) + block.shape, BF16)],
         compiler_params=pltpu.CompilerParams(vmem_limit_bytes=VMEM_LIMIT),
         cost_estimate=pl.CostEstimate(
-            flops=2 * span * model * (GROUPS * STATE + HEADS), bytes_accessed=2 * span * model, transcendentals=0
+            flops=2 * span * model * GROUPS * STATE, bytes_accessed=2 * span * model, transcendentals=0
         ),
         name="key_blocks",
-    )(off_chip(rows), off_chip(rows), off_chip(wk), off_chip(wr))
-
-
-def value_kernel(x_refs, w_ref, outs, kept):
+    )(off_chip(rows), off_chip(rows), off_chip(wk))
+
+
+def early_value_kernel(x_ref, after_ref, last_ref, other_ref, w_ref, wr_ref, _, *rest):
+    outs, (kept, rates) = rest[:-2], rest[-2:]
     step = pl.program_id(0)
     share = kept.shape[2]
     devices = w_ref.shape[1] // share
-    rows = x_refs[0].shape[0]
-    x = jnp.concatenate([ref[...] for ref in x_refs], axis=0) if len(x_refs) > 1 else x_refs[0][...]
+    rows = x_ref.shape[0]
+    x = jnp.concatenate([x_ref[...], after_ref[...], last_ref[...]], axis=0)
     y = jnp.dot(x, w_ref[...], preferred_element_type=F32)
+    last = y.shape[0]
+    half = EXTRA // 2
+    extra = jnp.concatenate([y[rows : rows + half], y[last - half :]], axis=0)
     for device in range(devices):
         lanes = slice(device * share, (device + 1) * share)
         index = step * devices + device
         kept[index, :rows, :] = y[:rows, lanes].astype(BF16)
-        if len(x_refs) > 1:
-            half = EXTRA // 2
-            last = y.shape[0]
-            extra = jnp.concatenate([y[rows : rows + half, lanes], y[last - half :, lanes]], axis=0)
-            kept[index, rows:, :] = extra.astype(BF16)
+        kept[index, kept.shape[1] - EXTRA :, :] = extra[:, lanes].astype(BF16)
+    part = other_ref.shape[0]
+    pieces = part // share
+    own_rows = x_ref[pl.ds(pl.multiple_of(step * part, part), part), :]
+    both = jnp.concatenate([own_rows, other_ref[...]], axis=0)
+    r = lax.dot_general(both, wr_ref[...], (((1,), (1,)), ((), ())), preferred_element_type=F32).astype(BF16)
+    eye = (
+        lax.broadcasted_iota(jnp.int32, (HEADS, HEADS), 0) == lax.broadcasted_iota(jnp.int32, (HEADS, HEADS), 1)
+    ).astype(BF16)
+    turned = lax.dot_general(eye, r, (((1,), (1,)), ((), ())), preferred_element_type=F32)
+    count = rates.shape[0]
+    for piece in range(pieces):
+        rates[step * pieces + piece] = turned[:, piece * share : (piece + 1) * share]
+        rates[count // 2 + step * pieces + piece] = turned[:, part + piece * share : part + (piece + 1) * share]
+
+    @pl.when(step == pl.num_programs(0) - 1)
+    def _():
+        heads = share // HEAD
+        for device in range(kept.shape[0]):
+            tile = [rates[t, h : h + 1, :] for h in range(device * heads, (device + 1) * heads) for t in range(count)]
+            kept[device, rows : rows + heads * count, :] = jnp.concatenate(tile, axis=0).astype(BF16)
+        own = lax.axis_index("sp")
+        for offset, out in enumerate(outs):
+            out[...] = kept[own ^ offset]
+
+
+def early_values(rows, wv, wr, started, devices, cut):
+    span, model = rows.shape
+    width = wv.shape[1]
+    share = width // devices
+    tile = max(2 * LANES, share)
+    steps = width // tile
+    part = cut // steps
+    block = (cut + span // HEAD + EXTRA, share)
+    x = off_chip(rows)
+    return pl.pallas_call(
+        early_value_kernel,
+        grid=(steps,),
+        in_specs=[
+            whole((cut, model)),
+            pl.BlockSpec((TILE_ROWS, model), lambda i: (cut // TILE_ROWS, 0)),
+            pl.BlockSpec((TILE_ROWS, model), lambda i: (span // TILE_ROWS - 1, 0)),
+            pl.BlockSpec((part, model), lambda i: (cut // part + i, 0)),
+            pl.BlockSpec((model, tile), lambda i: (0, i)),
+            whole(wr.shape),
+            pl.BlockSpec(memory_space=pl.ANY),
+        ],
+        out_specs=[whole(block)] * devices,
+        out_shape=[jax.ShapeDtypeStruct(block, BF16)] * devices,
+        scratch_shapes=[pltpu.VMEM((devices,) + block, BF16), pltpu.VMEM((span // share, HEADS, share), F32)],
+        compiler_params=pltpu.CompilerParams(vmem_limit_bytes=VMEM_LIMIT),
+        cost_estimate=pl.CostEstimate(
+            flops=2 * cut * model * width, bytes_accessed=2 * (span * model + model * width), transcendentals=0
+        ),
+        name="early_values",
+    )(x, x, x, x, off_chip(wv), off_chip(wr), started)
+
+
+def late_value_kernel(x_ref, w_ref, _, *rest):
+    outs, kept = rest[:-1], rest[-1]
+    step = pl.program_id(0)
+    share = kept.shape[2]
+    devices = w_ref.shape[1] // share
+    y = jnp.dot(x_ref[...], w_ref[...], preferred_element_type=F32)
+    for device in range(devices):
+        kept[step * devices + device] = y[:, device * share : (device + 1) * share].astype(BF16)
 
     @pl.when(step == pl.num_programs(0) - 1)
     def _():
@@ -146,66 +186,38 @@
             out[...] = kept[own ^ offset]
 
 
-def value_blocks(rows, wv, started, devices, cut, early):
+def late_values(rows, wv, started, devices, cut):
     span, model = rows.shape
     width = wv.shape[1]
     share = width // devices
     tile = max(2 * LANES, share)
-    if early:
-        specs = [
-            whole((cut, model)),
-            pl.BlockSpec((TILE_ROWS, model), lambda i: (cut // TILE_ROWS, 0)),
-            pl.BlockSpec((TILE_ROWS, model), lambda i: (span // TILE_ROWS - 1, 0)),
-        ]
-        block = (cut + EXTRA, share)
-    else:
-        specs = [pl.BlockSpec((span - cut, model), lambda i: (cut // (span - cut), 0))]
-        block = (span - cut, share)
-    count = len(specs)
-
-    def kernel(*refs):
-        value_kernel(refs[:count], refs[count], refs[count + 2 : -1], refs[-1])
-
-    return pl.pallas_call(
-        kernel,
+    late = span - cut
+    block = (late, share)
+    return pl.pallas_call(
+        late_value_kernel,
         grid=(width // tile,),
-        in_specs=specs + [pl.BlockSpec((model, tile), lambda i: (0, i)), pl.BlockSpec(memory_space=pl.ANY)],
+        in_specs=[
+            pl.BlockSpec((late, model), lambda i: (cut // late, 0)),
+            pl.BlockSpec((model, tile), lambda i: (0, i)),
+            pl.BlockSpec(memory_space=pl.ANY),
+        ],
         out_specs=[whole(block)] * devices,
         out_shape=[jax.ShapeDtypeStruct(block, BF16)] * devices,
         scratch_shapes=[pltpu.VMEM((devices,) + block, BF16)],
         compiler_params=pltpu.CompilerParams(vmem_limit_bytes=VMEM_LIMIT),
         cost_estimate=pl.CostEstimate(
-            flops=2 * block[0] * model * width,
-            bytes_accessed=2 * (block[0] * model + model * width),
-            transcendentals=0,
+            flops=2 * late * model * width, bytes_accessed=2 * (late * model + model * width), transcendentals=0
         ),
-        name="early_values" if early else "late_values",
-    )(*[off_chip(rows)] * count, off_chip(wv), started)
-
-
-def key_read_kernel(
-    group_devices, *refs
-):
+        name="late_values",
+    )(off_chip(rows), off_chip(wv), started)
+
+
+def key_read_kernel(group_devices, *refs):
     count = GROUPS * group_devices
-    held, refs = refs[:count], refs[count:]
-    (
-        taps_ref,
-        query_ref,
-        offset_ref,
-        decay_ref,
-        spikes_ref,
-        keys_ref,
-        weight_ref,
-        blocks,
-        line,
-        rates,
-        scores,
-        spikes,
-    ) = refs
-    repeats = HEADS // GROUPS
+    held = refs[:count]
+    taps_ref, query_ref, keys_ref, score_ref, blocks, line = refs[count:]
     sources = blocks.shape[0]
-    half = keys_ref.shape[1] // 2
-    heads = spikes_ref.shape[1]
+    half = blocks.shape[1]
     tiles = 2 * half // LANES
     me = lax.axis_index("sp")
     group, rank = me // group_devices, me % group_devices
@@ -224,9 +236,6 @@
     query = jnp.where(part_row == lane_index((16, LANES)) // STATE, asked, 0.0).astype(BF16)
     edge_left = lane_index((16, LANES)) < STATE
     left = lane_index((half, LANES)) < STATE
-    picked = lax.broadcasted_iota(jnp.int32, (heads * tiles, repeats * tiles), 0)
-    column = lax.broadcasted_iota(jnp.int32, (heads * tiles, repeats * tiles), 1)
-    select = (column == (picked % tiles) * repeats + rank * heads + picked // tiles).astype(BF16)
 
     def one_source(source, carry):
         body = blocks[source, :half, :].astype(F32)
@@ -244,7 +253,7 @@
             total = total + taps[k] * line[14 + k : 14 + k + half, :]
         y = silu(total).astype(BF16)
         score = lax.dot_general(query, y, (((1,), (1,)), ((), ())), preferred_element_type=F32)
-        scores[source] = jnp.concatenate(
+        score_ref[source] = jnp.concatenate(
             [score[part : part + 1, c * LANES : (c + 1) * LANES] for part in range(2) for c in range(tiles // 2)],
             axis=0,
         )
@@ -252,12 +261,37 @@
         turned = pltpu.roll(z, STATE, 1)
         keys_ref[source, :half, :] = jnp.where(left, z, turned).astype(BF16)
         keys_ref[source, half:, :] = jnp.where(left, turned, z).astype(BF16)
-        chosen = jnp.dot(select, blocks[source, half:, :], preferred_element_type=F32)
-        for h in range(heads):
-            rates[h, source] = chosen[h * tiles : (h + 1) * tiles]
         return carry
 
     lax.fori_loop(0, sources, one_source, 0)
+
+
+def key_read(held, taps, query, group_devices, span):
+    sources = len(held)
+    vmem = pl.BlockSpec(memory_space=pltpu.VMEM)
+    inputs = [*held, taps, query]
+    return pl.pallas_call(
+        lambda *refs: key_read_kernel(group_devices, *refs),
+        in_specs=[vmem] * len(inputs),
+        out_specs=[vmem, vmem],
+        out_shape=[
+            jax.ShapeDtypeStruct((sources, span, LANES), BF16),
+            jax.ShapeDtypeStruct((sources, span // LANES, LANES), F32),
+        ],
+        scratch_shapes=[
+            pltpu.VMEM((sources,) + held[0].shape, BF16),
+            pltpu.VMEM((span // 2 + 32, LANES), F32),
+        ],
+        compiler_params=pltpu.CompilerParams(vmem_limit_bytes=VMEM_LIMIT),
+        cost_estimate=pl.CostEstimate(flops=10**9, bytes_accessed=4 * 10**6, transcendentals=10**6),
+        name="key_read",
+    )(*(on_chip(x) for x in inputs))
+
+
+def read_weights(blocks, cut, score_ref, offset_ref, decay_ref, spikes_ref, spikes, weight_ref):
+    sources, tiles = score_ref.shape[:2]
+    share = blocks.shape[2]
+    heads = share // HEAD
     count = sources * tiles
     lane_row = lax.broadcasted_iota(jnp.int32, (LANES, LANES), 0)
     lane_col = lax.broadcasted_iota(jnp.int32, (LANES, LANES), 1)
@@ -265,13 +299,27 @@
     row = lax.broadcasted_iota(jnp.int32, (count, count), 0)
     col = lax.broadcasted_iota(jnp.int32, (count, count), 1)
     later_rows = (col > row).astype(F32)
-    score = scores[...].reshape(count, LANES)
+    score = score_ref[...].reshape(count, LANES)
     for h in range(heads):
         for c in range(count):
             spikes[h, c : c + 1, :] = spikes_ref[0, h : h + 1, c * LANES : (c + 1) * LANES]
     exact = dict(preferred_element_type=F32, precision=lax.Precision.HIGHEST)
+    pieces = LANES // share
     for h in range(heads):
-        raw = rates[h].reshape(count, LANES) + offset_ref[h]
+        rates = []
+        for source in range(sources):
+            sent = blocks[source, cut : cut + heads * tiles * pieces, :]
+            if pieces == 1:
+                rates.append(sent.astype(F32)[h * tiles : (h + 1) * tiles])
+            else:
+                picks = []
+                for piece in range(pieces):
+                    wanted = lax.broadcasted_iota(jnp.int32, (tiles, sent.shape[0]), 0)
+                    column = lax.broadcasted_iota(jnp.int32, (tiles, sent.shape[0]), 1)
+                    pick = (column == (h * tiles + wanted) * pieces + piece).astype(BF16)
+                    picks.append(jnp.dot(pick, sent, preferred_element_type=F32))
+                rates.append(jnp.concatenate(picks, axis=1))
+        raw = jnp.concatenate(rates, axis=0) + offset_ref[h]
         rate = jnp.maximum(raw, 0.0) + jnp.log1p(jnp.exp(-jnp.abs(raw)))
         decay = jnp.exp(jnp.full((1, LANES), decay_ref[h], F32))
         step = spikes[h] - decay * rate
@@ -282,35 +330,6 @@
         high = rounded(weight)
         weight_ref[:, h] = high.reshape(sources, tiles, LANES)
         weight_ref[:, heads + h] = (weight - high).reshape(sources, tiles, LANES)
-
-
-def key_read(held, relayed, taps, query, offset, decay, spikes, group_devices, span):
-    sources = group_devices * GROUPS
-    heads = offset.shape[0]
-    half = span // 2
-    tiles = span // LANES
-    smem = pl.BlockSpec(memory_space=pltpu.SMEM)
-    vmem = pl.BlockSpec(memory_space=pltpu.VMEM)
-    count = len(held) + len(relayed)
-    return pl.pallas_call(
-        lambda *refs: key_read_kernel(group_devices, *refs),
-        in_specs=[vmem] * (count + 2) + [smem, smem, vmem],
-        out_specs=[vmem, vmem],
-        out_shape=[
-            jax.ShapeDtypeStruct((sources, span, LANES), BF16),
-            jax.ShapeDtypeStruct((sources, 2 * heads, tiles, LANES), F32),
-        ],
-        scratch_shapes=[
-            pltpu.VMEM((sources,) + held[0].shape, BF16),
-            pltpu.VMEM((half + 32, LANES), F32),
-            pltpu.VMEM((heads, sources, tiles, LANES), F32),
-            pltpu.VMEM((sources, tiles, LANES), F32),
-            pltpu.VMEM((heads, sources * tiles, LANES), F32),
-        ],
-        compiler_params=pltpu.CompilerParams(vmem_limit_bytes=VMEM_LIMIT),
-        cost_estimate=pl.CostEstimate(flops=10**9, bytes_accessed=4 * 10**6, transcendentals=10**6),
-        name="key_read",
-    )(*(on_chip(x) for x in [*held, *relayed, taps, query]), offset, decay, on_chip(spikes))
 
 
 def convolved(line, body, before, after, taps_ref, weight_ref, source, start_row, total):
@@ -367,8 +386,9 @@
 
 
 def early_kernel(cut, *refs):
-    blocks = refs[:-10]
-    keys_ref, weight_ref, taps_ref, out_ref, read_ref, edges_ref, kept, line, woven, total = refs[-10:]
+    blocks, refs = refs[:-15], refs[-15:]
+    keys_ref, score_ref, taps_ref, spikes_ref, offset_ref, decay_ref = refs[:6]
+    out_ref, read_ref, edges_ref, weight_ref, kept, line, woven, total, spikes = refs[6:]
     source = pl.program_id(0)
     own = lax.axis_index("sp")
 
@@ -379,47 +399,55 @@
             kept[own ^ offset] = block_ref[...]
             edges_ref[own ^ offset, :TILE_ROWS, :] = block_ref[:TILE_ROWS, :]
             edges_ref[own ^ offset, TILE_ROWS:, :] = block_ref[cut - TILE_ROWS : cut, :]
+        read_weights(kept, cut, score_ref, offset_ref, decay_ref, spikes_ref, spikes, weight_ref)
 
     block = kept[source].astype(F32)
-    before = kept[jnp.maximum(source - 1, 0), cut:, :].astype(F32)
+    before = kept[jnp.maximum(source - 1, 0), kept.shape[1] - EXTRA :, :].astype(F32)
     before = jnp.where(source > 0, before, 0.0)
-    values = convolved(line, block[:cut], before, block[cut:], taps_ref, weight_ref, source, 0, total)
+    beside = block[block.shape[0] - EXTRA :]
+    values = convolved(line, block[:cut], before, beside, taps_ref, weight_ref, source, 0, total)
     wove(woven, values, keys_ref, source, 0, out_ref)
     read_ref[...] = total[...]
 
 
-def early_rows(blocks, keys, weight, taps, cut):
+def early_rows(blocks, keys, score, taps, spikes, offset, decay, cut):
     sources, span = keys.shape[:2]
     height, share = blocks[0].shape
     heads = share // HEAD
-    reads = weight.shape[1] * weight.shape[2]
+    tiles = span // LANES
+    reads = 2 * heads * tiles
     edges = (sources, 2 * TILE_ROWS, share)
     vmem = pl.BlockSpec(memory_space=pltpu.VMEM)
-    inputs = [*blocks, keys, weight, taps]
+    smem = pl.BlockSpec(memory_space=pltpu.SMEM)
+    inputs = [*blocks, keys, score, taps, spikes]
+    weight = (sources, 2 * heads, tiles, LANES)
     return pl.pallas_call(
         lambda *refs: early_kernel(cut, *refs),
         grid=(sources,),
-        in_specs=[vmem] * len(inputs),
+        in_specs=[vmem] * len(inputs) + [smem, smem],
         out_specs=[
             pl.BlockSpec((1, heads * cut, LANES), lambda s: (s, 0, 0)),
             whole((reads, share)),
             whole(edges),
+            whole(weight),
         ],
         out_shape=[
             jax.ShapeDtypeStruct((sources, heads * span, LANES), BF16),
             jax.ShapeDtypeStruct((reads, share), F32),
             jax.ShapeDtypeStruct(edges, BF16),
+            jax.ShapeDtypeStruct(weight, F32),
         ],
         scratch_shapes=[
             pltpu.VMEM((sources, height, share), BF16),
             line_scratch(cut, share),
             woven_scratch(cut, share),
             pltpu.VMEM((reads, share), F32),
+            pltpu.VMEM((heads, sources * tiles, LANES), F32),
         ],
         compiler_params=pltpu.CompilerParams(vmem_limit_bytes=VMEM_LIMIT),
         cost_estimate=pl.CostEstimate(flops=2 * 10**9, bytes_accessed=6 * 10**6, transcendentals=10**6),
         name="early_rows",
-    )(*(on_chip(x) for x in inputs))
+    )(*(on_chip(x) for x in inputs), offset, decay)
 
 
 def late_values_of(offset, block_ref, edges_ref, taps_ref, weight_ref, line, total, cut):
@@ -571,12 +599,12 @@
     devices = lax.axis_size("sp")
     cut = span // 2
 
-    blocks = key_blocks(rows, address_mapping_matrix, increment_mapping_matrix.T, group_devices)
+    blocks = key_blocks(rows, address_mapping_matrix, group_devices)
     direct = [None] * (GROUPS - 1)
     for offset in range(1, GROUPS):
         direct[offset - 1] = flip_permute(blocks[offset], offset * group_devices)
-    early = value_blocks(rows, content_mapping_matrix, blocks[0], devices, cut, True)
-    late = value_blocks(rows, content_mapping_matrix, early[0], devices, cut, False)
+    early = early_values(rows, content_mapping_matrix, increment_mapping_matrix.T, blocks[0], devices, cut)
+    late = late_values(rows, content_mapping_matrix, early[0], devices, cut)
     held = [blocks[0]] + direct
     relayed = []
     for shift in range(1, group_devices):
@@ -587,19 +615,18 @@
         early_blocks.append(flip_permute(early[offset], offset))
         late_blocks.append(flip_permute(late[offset], offset))
 
-    keys, weight = key_read(
-        held,
-        relayed,
-        address_smoothing_coefficients,
-        newest_lookup_matrix,
+    keys, score = key_read(held + relayed, address_smoothing_coefficients, newest_lookup_matrix, group_devices, span)
+    taps = content_smoothing_coefficients
+    out, read, edges, weight = early_rows(
+        early_blocks,
+        keys,
+        score,
+        taps,
+        extra_damping_spikes,
         increment_speed_offset,
         channel_fading_exponent,
-        extra_damping_spikes,
-        group_devices,
-        span,
+        cut,
     )
-    taps = content_smoothing_coefficients
-    out, read, edges = early_rows(early_blocks, keys, weight, taps, cut)
     half = devices // 2
     first, final = list(range(half)), list(range(half, devices))
     out, read = late_rows(first, late_blocks, edges, keys, weight, taps, read, out, cut)

time: 94.4 us -> 87.6 us (0.928)
  waiting for transfers between devices: 21 us -> 16.9 us
  starting transfers between devices: 42.2 us -> 39 us
    ppermute x22, waiting for transfers between devices: 21 us -> 16.9 us  [flip_permute(): return lax.ppermute(value, 'sp', pairs)]
    ppermute x22, starting transfers between devices: 42.2 us -> 39 us  [flip_permute(): return lax.ppermute(value, 'sp', pairs)]
    pallas_call x2, Pallas kernels: 11.2 us -> 12.7 us  [the longest x1 7.12 us: early_values(): pl.pallas_call(early_value_kernel, grid=(steps,), in_specs=[whole((cut, m...]
    pallas_call x1, Pallas kernels: 4.72 us -> 5.81 us  [early_rows(): pl.pallas_call(lambda *refs: early_kernel(cut, *refs), grid=(sources,), i...]
    pallas_call x1, Pallas kernels: 4.63 us -> 3.56 us  [key_blocks(): pl.pallas_call(lambda *refs: key_block_kernel(group_devices, *refs), grid...]
    pallas_call x1, Pallas kernels: 3.6 us -> 2.59 us  [key_read(): pl.pallas_call(lambda *refs: key_read_kernel(group_devices, *refs), in_sp...]
  transfers between devices with their start and end apart: 22 -> 22, of which waited for: 5 -> 4; matrix products, arithmetic and copies ran while one was open for 0% -> 0% of each run, Pallas kernels for 14% -> 29%
where the time goes in v3:
time: 87.6 us; the launch traced here: 87.4 us
  starting transfers between devices  39 us (45%)
  Pallas kernels  30 us (34%)
  waiting for transfers between devices  16.9 us (19%)
    ppermute x22, starting transfers between devices, flip_permute(): return lax.ppermute(value, 'sp', pairs)  39 us
    ppermute x22, waiting for transfers between devices, flip_permute(): return lax.ppermute(value, 'sp', pairs)  16.9 us
    pallas_call x1, Pallas kernels, early_values(): pl.pallas_call(early_value_kernel, grid=(steps,), in_specs=[whole((cut, m...  7.12 us
    pallas_call x1, Pallas kernels, early_rows(): pl.pallas_call(lambda *refs: early_kernel(cut, *refs), grid=(sources,), i...  5.81 us
    pallas_call x1, Pallas kernels, late_values(): pl.pallas_call(late_value_kernel, grid=(width // tile,), in_specs=[pl.Blo...  5.55 us
    pallas_call x1, Pallas kernels, key_blocks(): pl.pallas_call(lambda *refs: key_block_kernel(group_devices, *refs), grid...  3.56 us
    pallas_call x1, Pallas kernels, late_rows(): pl.pallas_call(lambda *refs: late_kernel(cut, offsets, *refs), grid=(len(...  2.62 us
    pallas_call x1, Pallas kernels, key_read(): pl.pallas_call(lambda *refs: key_read_kernel(group_devices, *refs), in_sp...  2.59 us
  transfers between devices with their start and end apart: 22, of which 4 were waited for; matrix products, arithmetic and copies ran while one was open for 0% of the time, Pallas kernels for 29%

profile of v3, /device:TPU:0, one launch (start us, length us, event | category | flops | bytes accessed | tf_op | source)
XLA Modules:
  0.0 87.4 jit_solution(3847929268881036039)
XLA Ops:
  0.6 3.6 %key_blocks.1 = (bf16[512,128]{1,0:T(8,128)(2,1)S(1)}, bf16[512,128]{1,0:T(8,128)(2,1)S(1)}, bf16[512,128]{1,0:T(8,128)(2,1)S(1)}, bf16[512,128]{1,0:T(8,128)(2,1)S(1)}) custom-call(bf16[1024,2048]{1,0:T(8,128)(2,1)} %bitcast.7, bf16[1024,2048]{1,0:T(8,128)(2,1)} %bitcast.8, bf16[2048,256]{1,0:T(8,128)(2,1)} %refs_2_.1), custom_call_target="tpu_custom_call" | custom-call | flops 1073741824 | bytes 4194304 | tf_op jit(solution)/shard_map/key_blocks/pallas_call | solution.py:81
  4.2 3.1 %collective-permute-start.11 = (bf16[512,128]{1,0:T(8,128)(2,1)S(1)}, bf16[512,128]{1,0:T(8,128)(2,1)S(1)}, u32[]{:S(2)}, u32[]{:S(2)}) collective-permute-start(bf16[512,128]{1,0:T(8,128)(2,1)S(1)} %get-tuple-element.46), channel_id=1, source_target_pairs={{0,4},{2,6},{4,0},{6,2},{8,12},{10,14},{12,8},{14,10},{1,5},{3,7},... | collective-permute-start | bytes 393224 | tf_op jit(solution)/shard_map/ppermute | solution.py:48
  7.3 2.6 %collective-permute-start.12 = (bf16[512,128]{1,0:T(8,128)(2,1)S(1)}, bf16[512,128]{1,0:T(8,128)(2,1)S(1)}, u32[]{:S(2)}, u32[]{:S(2)}) collective-permute-start(bf16[512,128]{1,0:T(8,128)(2,1)S(1)} %get-tuple-element.47), channel_id=1, source_target_pairs={{0,8},{2,10},{4,12},{6,14},{8,0},{10,2},{12,4},{14,6},{1,9},{3,11}... | collective-permute-start | bytes 393224 | tf_op jit(solution)/shard_map/ppermute | solution.py:48
  9.9 1.7 %collective-permute-start.14 = (bf16[512,128]{1,0:T(8,128)(2,1)S(1)}, bf16[512,128]{1,0:T(8,128)(2,1)S(1)}, u32[]{:S(2)}, u32[]{:S(2)}) collective-permute-start(bf16[512,128]{1,0:T(8,128)(2,1)S(1)} %get-tuple-element.33._.refs_0_), channel_id=1, source_target_pairs={{0,2},{2,0},{4,6},{6,4},{8,10},{10,8},{12,14},{14,12},{1,3},{3,1},... | collective-permute-start | bytes 393224 | tf_op jit(solution)/shard_map/ppermute | solution.py:48
  11.6 7.1 %early_values.1 = (bf16[536,128]{1,0:T(8,128)(2,1)S(1)}, bf16[536,128]{1,0:T(8,128)(2,1)S(1)}, bf16[536,128]{1,0:T(8,128)(2,1)S(1)}, bf16[536,128]{1,0:T(8,128)(...) custom-call(bf16[1024,2048]{1,0:T(8,128)(2,1)} %bitcast.9, ...), custom_call_target="tpu_custom_call" | custom-call | flops 2147483648 | bytes 8388608 | tf_op jit(solution)/shard_map/early_values/pallas_call | solution.py:150
  18.8 5.5 %late_values.1 = (bf16[512,128]{1,0:T(8,128)(2,1)S(1)}, bf16[512,128]{1,0:T(8,128)(2,1)S(1)}, bf16[512,128]{1,0:T(8,128)(2,1)S(1)}, bf16[512,128]{1,0:T(8,128)(2...) custom-call(bf16[1024,2048]{1,0:T(8,128)(2,1)} %bitcast.13, ...), custom_call_target="tpu_custom_call" | custom-call | flops 2147483648 | bytes 6291456 | tf_op jit(solution)/shard_map/late_values/pallas_call | solution.py:196
  24.4 0.3 collective-permute-start.18
  24.8 0.9 %collective-permute-start.19 = (bf16[512,128]{1,0:T(8,128)(2,1)S(1)}, bf16[512,128]{1,0:T(8,128)(2,1)S(1)}, u32[]{:S(2)}, u32[]{:S(2)}) collective-permute-start(bf16[512,128]{1,0:T(8,128)(2,1)S(1)} %get-tuple-element.55), channel_id=1, source_target_pairs={{0,4},{2,6},{4,0},{6,2},{8,12},{10,14},{12,8},{14,10},{1,5},{3,7},... | collective-permute-start | bytes 393224 | tf_op jit(solution)/shard_map/ppermute | solution.py:48
  25.7 1.5 %collective-permute-start.4 = (bf16[536,128]{1,0:T(8,128)(2,1)S(1)}, bf16[536,128]{1,0:T(8,128)(2,1)S(1)}, u32[]{:S(2)}, u32[]{:S(2)}) collective-permute-start(bf16[536,128]{1,0:T(8,128)(2,1)S(1)} %get-tuple-element.39), channel_id=1, source_target_pairs={{0,2},{2,0},{4,6},{6,4},{8,10},{10,8},{12,14},{14,12},{1,3},{3,1},... | collective-permute-start | bytes 411656 | tf_op jit(solution)/shard_map/ppermute | solution.py:48
  27.2 1.4 %collective-permute-start.5 = (bf16[536,128]{1,0:T(8,128)(2,1)S(1)}, bf16[536,128]{1,0:T(8,128)(2,1)S(1)}, u32[]{:S(2)}, u32[]{:S(2)}) collective-permute-start(bf16[536,128]{1,0:T(8,128)(2,1)S(1)} %get-tuple-element.40), channel_id=1, source_target_pairs={{0,4},{2,6},{4,0},{6,2},{8,12},{10,14},{12,8},{14,10},{1,5},{3,7},... | collective-permute-start | bytes 411656 | tf_op jit(solution)/shard_map/ppermute | solution.py:48
  28.5 0.3 collective-permute-start.15
  28.8 2.0 %collective-permute-done.18.refs_1_ = bf16[512,128]{1,0:T(8,128)(2,1)S(1)} collective-permute-done((bf16[512,128]{1,0:T(8,128)(2,1)S(1)}, bf16[512,128]{1,0:T(8,128)(2,1)S(1)}, u32[]{:S(2)}, u32[]{:S(2)}) %collective-permute-start.18) | collective-permute-done | bytes 131104 | tf_op jit(solution)/shard_map/ppermute | solution.py:48
  30.8 0.3 collective-permute-start.16
  31.1 1.7 %collective-permute-start.17 = (bf16[512,128]{1,0:T(8,128)(2,1)S(1)}, bf16[512,128]{1,0:T(8,128)(2,1)S(1)}, u32[]{:S(2)}, u32[]{:S(2)}) collective-permute-start(bf16[512,128]{1,0:T(8,128)(2,1)S(1)} %collective-permute-done.13.refs_3_), channel_id=1, source_target_pairs={{0,2},{2,0},{4,6},{6,4},{8,10},{10,8},{12,14},{14,12},{1,3},{3,1},... | collective-permute-start | bytes 393224 | tf_op jit(solution)/shard_map/ppermute | solution.py:48
  32.9 2.4 %collective-permute-done.4.refs_1_ = bf16[536,128]{1,0:T(8,128)(2,1)S(1)} collective-permute-done((bf16[536,128]{1,0:T(8,128)(2,1)S(1)}, bf16[536,128]{1,0:T(8,128)(2,1)S(1)}, u32[]{:S(2)}, u32[]{:S(2)}) %collective-permute-start.4) | collective-permute-done | bytes 137248 | tf_op jit(solution)/shard_map/ppermute | solution.py:48
  35.3 4.1 %collective-permute-start.7 = (bf16[536,128]{1,0:T(8,128)(2,1)S(1)}, bf16[536,128]{1,0:T(8,128)(2,1)S(1)}, u32[]{:S(2)}, u32[]{:S(2)}) collective-permute-start(bf16[536,128]{1,0:T(8,128)(2,1)S(1)} %get-tuple-element.42), channel_id=1, source_target_pairs={{0,8},{2,10},{4,12},{6,14},{8,0},{10,2},{12,4},{14,6},{1,9},{3,11}... | collective-permute-start | bytes 411656 | tf_op jit(solution)/shard_map/ppermute | solution.py:48
  39.4 4.1 %collective-permute-start.8 = (bf16[536,128]{1,0:T(8,128)(2,1)S(1)}, bf16[536,128]{1,0:T(8,128)(2,1)S(1)}, u32[]{:S(2)}, u32[]{:S(2)}) collective-permute-start(bf16[536,128]{1,0:T(8,128)(2,1)S(1)} %get-tuple-element.43), channel_id=1, source_target_pairs={{0,10},{2,8},{4,14},{6,12},{8,2},{10,0},{12,6},{14,4},{1,11},{3,9}... | collective-permute-start | bytes 411656 | tf_op jit(solution)/shard_map/ppermute | solution.py:48
  43.4 1.5 %collective-permute-start.9 = (bf16[536,128]{1,0:T(8,128)(2,1)S(1)}, bf16[536,128]{1,0:T(8,128)(2,1)S(1)}, u32[]{:S(2)}, u32[]{:S(2)}) collective-permute-start(bf16[536,128]{1,0:T(8,128)(2,1)S(1)} %get-tuple-element.44), channel_id=1, source_target_pairs={{0,12},{2,14},{4,8},{6,10},{8,4},{10,6},{12,0},{14,2},{1,13},{3,15... | collective-permute-start | bytes 411656 | tf_op jit(solution)/shard_map/ppermute | solution.py:48
  44.9 3.0 %collective-permute-start.10 = (bf16[536,128]{1,0:T(8,128)(2,1)S(1)}, bf16[536,128]{1,0:T(8,128)(2,1)S(1)}, u32[]{:S(2)}, u32[]{:S(2)}) collective-permute-start(bf16[536,128]{1,0:T(8,128)(2,1)S(1)} %get-tuple-element.45), channel_id=1, source_target_pairs={{0,14},{2,12},{4,10},{6,8},{8,6},{10,4},{12,2},{14,0},{1,15},{3,13... | collective-permute-start | bytes 411656 | tf_op jit(solution)/shard_map/ppermute | solution.py:48
  47.9 2.6 %key_read.1 = (bf16[8,1024,128]{2,1,0:T(8,128)(2,1)S(1)}, f32[8,8,128]{2,1,0:T(8,128)S(1)}) custom-call(bf16[512,128]{1,0:T(8,128)(2,1)S(1)} %get-tuple-element.33._.refs_0_, bf16[512,128]{1,0:T(8,128)(2,1)S(1)} %collective-permute-done.11.refs_1_, bf16[512,128]{1,0:T(8,128)(2,1)S(1)} %collective-permute-done.12.refs_2_, ...), custom_call_target="tpu_custom_call" | custom-call | flops 1000000000 | bytes 4000000 | tf_op jit(solution)/shard_map/key_read/pallas_call | solution.py:273
  50.6 9.1 %collective-permute-done.7.refs_4_ = bf16[536,128]{1,0:T(8,128)(2,1)S(1)} collective-permute-done((bf16[536,128]{1,0:T(8,128)(2,1)S(1)}, bf16[536,128]{1,0:T(8,128)(2,1)S(1)}, u32[]{:S(2)}, u32[]{:S(2)}) %collective-permute-start.7) | collective-permute-done | bytes 137248 | tf_op jit(solution)/shard_map/ppermute | solution.py:48
  59.7 0.3 collective-permute-start.1
  60.0 3.4 %collective-permute-done.8.refs_5_ = bf16[536,128]{1,0:T(8,128)(2,1)S(1)} collective-permute-done((bf16[536,128]{1,0:T(8,128)(2,1)S(1)}, bf16[536,128]{1,0:T(8,128)(2,1)S(1)}, u32[]{:S(2)}, u32[]{:S(2)}) %collective-permute-start.8) | collective-permute-done | bytes 137248 | tf_op jit(solution)/shard_map/ppermute | solution.py:48
  63.4 1.6 %collective-permute-start.2 = (bf16[512,128]{1,0:T(8,128)(2,1)S(1)}, bf16[512,128]{1,0:T(8,128)(2,1)S(1)}, u32[]{:S(2)}, u32[]{:S(2)}) collective-permute-start(bf16[512,128]{1,0:T(8,128)(2,1)S(1)} %get-tuple-element.37), channel_id=1, source_target_pairs={{0,12},{2,14},{4,8},{6,10},{8,4},{10,6},{12,0},{14,2},{1,13},{3,15... | collective-permute-start | bytes 393224 | tf_op jit(solution)/shard_map/ppermute | solution.py:48
  65.0 2.3 %collective-permute-start.3 = (bf16[512,128]{1,0:T(8,128)(2,1)S(1)}, bf16[512,128]{1,0:T(8,128)(2,1)S(1)}, u32[]{:S(2)}, u32[]{:S(2)}) collective-permute-start(bf16[512,128]{1,0:T(8,128)(2,1)S(1)} %get-tuple-element.38), channel_id=1, source_target_pairs={{0,14},{2,12},{4,10},{6,8},{8,6},{10,4},{12,2},{14,0},{1,15},{3,13... | collective-permute-start | bytes 393224 | tf_op jit(solution)/shard_map/ppermute | solution.py:48
  67.3 5.4 %collective-permute-start.20 = (bf16[512,128]{1,0:T(8,128)(2,1)S(1)}, bf16[512,128]{1,0:T(8,128)(2,1)S(1)}, u32[]{:S(2)}, u32[]{:S(2)}) collective-permute-start(bf16[512,128]{1,0:T(8,128)(2,1)S(1)} %get-tuple-element.56), channel_id=1, source_target_pairs={{0,6},{2,4},{4,2},{6,0},{8,14},{10,12},{12,10},{14,8},{1,7},{3,5},... | collective-permute-start | bytes 393224 | tf_op jit(solution)/shard_map/ppermute | solution.py:48
  72.8 5.8 %early_rows.1 = (bf16[8,2048,128]{2,1,0:T(8,128)(2,1)}, f32[32,128]{1,0:T(8,128)S(1)}, bf16[8,32,128]{2,1,0:T(8,128)(2,1)S(1)}, f32[8,4,8,128]{3,2,1,0:T(8,128)S(1)}) custom-call(bf16[536,128]{1,0:T(8,128)(2,1)S(1)} %get-tuple-element.34._.refs_0_, bf16[536,128]{1,0:T(8,128)(2,1)S(1)} %collective-permute-done.4.refs_1_, ...), custom_call_target="tpu_custom_call" | custom-call | flops 2000000000 | bytes 6000000 | tf_op jit(solution)/shard_map/early_rows/pallas_call | solution.py:424
  78.6 2.6 %late_rows.1 = (bf16[8,2048,128]{2,1,0:T(8,128)(2,1)}, f32[32,128]{1,0:T(8,128)S(1)}) custom-call(bf16[512,128]{1,0:T(8,128)(2,1)S(1)} %get-tuple-element.53.refs_0_, bf16[512,128]{1,0:T(8,128)(2,1)S(1)} %collective-permute-done.18.refs_1_, bf16[512,128]{1,0:T(8,128)(2,1)S(1)} %collective-permute-done.19.refs_2_, ...), custom_call_target="tpu_custom_call", output_to_operand_aliasing={{0}: (9, {})} | custom-call | flops 1000000000 | bytes 2000000 | tf_op jit(solution)/shard_map/late_rows/pallas_call | solution.py:499
  81.2 1.0 %last_read.1 = (bf16[4,512,128]{2,1,0:T(8,128)(2,1)S(1)}, f32[2,64]{1,0:T(2,128)S(1)}, f32[1,128]{1,0:T(1,128)S(1)}) custom-call(bf16[512,128]{1,0:T(8,128)(2,1)S(1)} %collective-permute-done.refs_0_, bf16[512,128]{1,0:T(8,128)(2,1)S(1)} %collective-permute-done.1.refs_1_, bf16[512,128]{1,0:T(8,128)(2,1)S(1)} %collective-permute-done.2.refs_2_, ...), custom_call_target="tpu_custom_call" | custom-call | flops 1000000000 | bytes 1000000 | tf_op jit(solution)/shard_map/last_read/pallas_call | solution.py:540
  82.2 2.8 %collective-permute-start.21 = (f32[1,128]{1,0:T(1,128)S(1)}, f32[1,128]{1,0:T(1,128)S(1)}, u32[]{:S(2)}, u32[]{:S(2)}) collective-permute-start(f32[1,128]{1,0:T(1,128)S(1)} %get-tuple-element.63), channel_id=1, source_target_pairs={{0,2},{2,0},{4,6},{6,4},{8,10},{10,8},{12,14},{14,12},{1,3},{3,1},... | collective-permute-start | bytes 1544 | tf_op jit(solution)/shard_map/ppermute | solution.py:48
  85.0 1.8 %last_rows.1 = bf16[8,2048,128]{2,1,0:T(8,128)(2,1)} custom-call(bf16[4,512,128]{2,1,0:T(8,128)(2,1)S(1)} %get-tuple-element.60.refs_0_, bf16[8,1024,128]{2,1,0:T(8,128)(2,1)S(1)} %get-tuple-element.49.refs_8_.refs_5_.refs_1_, bf16[8,2048,128]{2,1,0:T(8,128)(2,1)} %get-tuple-element.61.refs_2_), custom_call_target="tpu_custom_call", output_to_operand_aliasing={{}: (2, {})} | custom-call | flops 1000000000 | bytes 2000000 | tf_op jit(solution)/shard_map/last_rows/pallas_call | solution.py:566
  86.9 0.5 fusion
  (38 shorter events, 0.2 us)
Async XLA Ops:
  4.2 20.6 %collective-permute-start.11 = (bf16[512,128]{1,0:T(8,128)(2,1)S(1)}, bf16[512,128]{1,0:T(8,128)(2,1)S(1)}, u32[]{:S(2)}, u32[]{:S(2)}) collective-permute-start(bf16[512,128]{1,0:T(8,128)(2,1)S(1)} %get-tuple-element.46), channel_id=1, source_target_pairs={{0,4},{2,6},{4,0},{6,2},{8,12},{10,14},{12,8},{14,10},{1,5},{3,7},... | collective-permute-start | bytes 393224 | tf_op jit(solution)/shard_map/ppermute | solution.py:48
  7.3 18.3 %collective-permute-start.12 = (bf16[512,128]{1,0:T(8,128)(2,1)S(1)}, bf16[512,128]{1,0:T(8,128)(2,1)S(1)}, u32[]{:S(2)}, u32[]{:S(2)}) collective-permute-start(bf16[512,128]{1,0:T(8,128)(2,1)S(1)} %get-tuple-element.47), channel_id=1, source_target_pairs={{0,8},{2,10},{4,12},{6,14},{8,0},{10,2},{12,4},{14,6},{1,9},{3,11}... | collective-permute-start | bytes 393224 | tf_op jit(solution)/shard_map/ppermute | solution.py:48
  9.9 17.3 %collective-permute-start.13 = (bf16[512,128]{1,0:T(8,128)(2,1)S(1)}, bf16[512,128]{1,0:T(8,128)(2,1)S(1)}, u32[]{:S(2)}, u32[]{:S(2)}) collective-permute-start(bf16[512,128]{1,0:T(8,128)(2,1)S(1)} %get-tuple-element.48), channel_id=1, source_target_pairs={{0,12},{2,14},{4,8},{6,10},{8,4},{10,6},{12,0},{14,2},{1,13},{3,15... | collective-permute-start | bytes 393224 | tf_op jit(solution)/shard_map/ppermute | solution.py:48
  9.9 18.6 %collective-permute-start.14 = (bf16[512,128]{1,0:T(8,128)(2,1)S(1)}, bf16[512,128]{1,0:T(8,128)(2,1)S(1)}, u32[]{:S(2)}, u32[]{:S(2)}) collective-permute-start(bf16[512,128]{1,0:T(8,128)(2,1)S(1)} %get-tuple-element.33._.refs_0_), channel_id=1, source_target_pairs={{0,2},{2,0},{4,6},{6,4},{8,10},{10,8},{12,14},{14,12},{1,3},{3,1},... | collective-permute-start | bytes 393224 | tf_op jit(solution)/shard_map/ppermute | solution.py:48
  18.8 29.1 %copy-start.2 = (f32[5,4,64]{2,1,0:T(4,128)S(1)}, f32[5,4,64]{2,1,0:T(4,128)}, u32[]{:S(2)}) copy-start(f32[5,4,64]{2,1,0:T(4,128)} %refs_8_.2) | copy-start | bytes 15364
  18.8 29.1 %copy-start.3 = (bf16[1,4,64]{2,1,0:T(4,128)(2,1)S(1)}, bf16[1,4,64]{2,1,0:T(4,128)(2,1)}, u32[]{:S(2)}) copy-start(bf16[1,4,64]{2,1,0:T(4,128)(2,1)} %refs_9_.1) | copy-start | bytes 1540
  18.8 54.0 %copy-start = (f32[5,2,64]{2,1,0:T(2,128)S(1)}, f32[5,2,64]{2,1,0:T(2,128)}, u32[]{:S(2)}) copy-start(f32[5,2,64]{2,1,0:T(2,128)} %refs_6_.1) | copy-start | bytes 7684
  18.8 54.0 %copy-start.1 = (f32[1,2,8192]{2,1,0:T(2,128)S(1)}, f32[1,2,8192]{2,1,0:T(2,128)}, u32[]{:S(2)}) copy-start(f32[1,2,8192]{2,1,0:T(2,128)} %refs_11_.1) | copy-start | bytes 196612
  18.8 54.0 %copy-start.4 = (f32[2]{0:T(128)S(1)}, f32[2]{0:T(128)}, u32[]{:S(2)}) copy-start(f32[2]{0:T(128)} %refs_12_.1) | copy-start | bytes 28
  18.8 53.9 %copy-start.5 = (f32[2]{0:T(128)S(1)}, f32[2]{0:T(128)}, u32[]{:S(2)}) copy-start(f32[2]{0:T(128)} %refs_13_.1) | copy-start | bytes 28
  24.4 6.4 %collective-permute-start.18 = (bf16[512,128]{1,0:T(8,128)(2,1)S(1)}, bf16[512,128]{1,0:T(8,128)(2,1)S(1)}, u32[]{:S(2)}, u32[]{:S(2)}) collective-permute-start(bf16[512,128]{1,0:T(8,128)(2,1)S(1)} %get-tuple-element.54), channel_id=1, source_target_pairs={{0,2},{2,0},{4,6},{6,4},{8,10},{10,8},{12,14},{14,12},{1,3},{3,1},... | collective-permute-start | bytes 393224 | tf_op jit(solution)/shard_map/ppermute | solution.py:48
  24.8 6.4 %collective-permute-start.19 = (bf16[512,128]{1,0:T(8,128)(2,1)S(1)}, bf16[512,128]{1,0:T(8,128)(2,1)S(1)}, u32[]{:S(2)}, u32[]{:S(2)}) collective-permute-start(bf16[512,128]{1,0:T(8,128)(2,1)S(1)} %get-tuple-element.55), channel_id=1, source_target_pairs={{0,4},{2,6},{4,0},{6,2},{8,12},{10,14},{12,8},{14,10},{1,5},{3,7},... | collective-permute-start | bytes 393224 | tf_op jit(solution)/shard_map/ppermute | solution.py:48
  25.7 9.6 %collective-permute-start.4 = (bf16[536,128]{1,0:T(8,128)(2,1)S(1)}, bf16[536,128]{1,0:T(8,128)(2,1)S(1)}, u32[]{:S(2)}, u32[]{:S(2)}) collective-permute-start(bf16[536,128]{1,0:T(8,128)(2,1)S(1)} %get-tuple-element.39), channel_id=1, source_target_pairs={{0,2},{2,0},{4,6},{6,4},{8,10},{10,8},{12,14},{14,12},{1,3},{3,1},... | collective-permute-start | bytes 411656 | tf_op jit(solution)/shard_map/ppermute | solution.py:48
  27.2 8.1 %collective-permute-start.5 = (bf16[536,128]{1,0:T(8,128)(2,1)S(1)}, bf16[536,128]{1,0:T(8,128)(2,1)S(1)}, u32[]{:S(2)}, u32[]{:S(2)}) collective-permute-start(bf16[536,128]{1,0:T(8,128)(2,1)S(1)} %get-tuple-element.40), channel_id=1, source_target_pairs={{0,4},{2,6},{4,0},{6,2},{8,12},{10,14},{12,8},{14,10},{1,5},{3,7},... | collective-permute-start | bytes 411656 | tf_op jit(solution)/shard_map/ppermute | solution.py:48
  28.5 10.8 %collective-permute-start.15 = (bf16[512,128]{1,0:T(8,128)(2,1)S(1)}, bf16[512,128]{1,0:T(8,128)(2,1)S(1)}, u32[]{:S(2)}, u32[]{:S(2)}) collective-permute-start(bf16[512,128]{1,0:T(8,128)(2,1)S(1)} %collective-permute-done.11.refs_1_), channel_id=1, source_target_pairs={{0,2},{2,0},{4,6},{6,4},{8,10},{10,8},{12,14},{14,12},{1,3},{3,1},... | collective-permute-start | bytes 393224 | tf_op jit(solution)/shard_map/ppermute | solution.py:48
  30.8 12.6 %collective-permute-start.16 = (bf16[512,128]{1,0:T(8,128)(2,1)S(1)}, bf16[512,128]{1,0:T(8,128)(2,1)S(1)}, u32[]{:S(2)}, u32[]{:S(2)}) collective-permute-start(bf16[512,128]{1,0:T(8,128)(2,1)S(1)} %collective-permute-done.12.refs_2_), channel_id=1, source_target_pairs={{0,2},{2,0},{4,6},{6,4},{8,10},{10,8},{12,14},{14,12},{1,3},{3,1},... | collective-permute-start | bytes 393224 | tf_op jit(solution)/shard_map/ppermute | solution.py:48
  31.1 13.8 %collective-permute-start.17 = (bf16[512,128]{1,0:T(8,128)(2,1)S(1)}, bf16[512,128]{1,0:T(8,128)(2,1)S(1)}, u32[]{:S(2)}, u32[]{:S(2)}) collective-permute-start(bf16[512,128]{1,0:T(8,128)(2,1)S(1)} %collective-permute-done.13.refs_3_), channel_id=1, source_target_pairs={{0,2},{2,0},{4,6},{6,4},{8,10},{10,8},{12,14},{14,12},{1,3},{3,1},... | collective-permute-start | bytes 393224 | tf_op jit(solution)/shard_map/ppermute | solution.py:48
  35.2 15.3 %collective-permute-start.6 = (bf16[536,128]{1,0:T(8,128)(2,1)S(1)}, bf16[536,128]{1,0:T(8,128)(2,1)S(1)}, u32[]{:S(2)}, u32[]{:S(2)}) collective-permute-start(bf16[536,128]{1,0:T(8,128)(2,1)S(1)} %get-tuple-element.41), channel_id=1, source_target_pairs={{0,6},{2,4},{4,2},{6,0},{8,14},{10,12},{12,10},{14,8},{1,7},{3,5},... | collective-permute-start | bytes 411656 | tf_op jit(solution)/shard_map/ppermute | solution.py:48
  35.3 24.4 %collective-permute-start.7 = (bf16[536,128]{1,0:T(8,128)(2,1)S(1)}, bf16[536,128]{1,0:T(8,128)(2,1)S(1)}, u32[]{:S(2)}, u32[]{:S(2)}) collective-permute-start(bf16[536,128]{1,0:T(8,128)(2,1)S(1)} %get-tuple-element.42), channel_id=1, source_target_pairs={{0,8},{2,10},{4,12},{6,14},{8,0},{10,2},{12,4},{14,6},{1,9},{3,11}... | collective-permute-start | bytes 411656 | tf_op jit(solution)/shard_map/ppermute | solution.py:48
  39.4 24.0 %collective-permute-start.8 = (bf16[536,128]{1,0:T(8,128)(2,1)S(1)}, bf16[536,128]{1,0:T(8,128)(2,1)S(1)}, u32[]{:S(2)}, u32[]{:S(2)}) collective-permute-start(bf16[536,128]{1,0:T(8,128)(2,1)S(1)} %get-tuple-element.43), channel_id=1, source_target_pairs={{0,10},{2,8},{4,14},{6,12},{8,2},{10,0},{12,6},{14,4},{1,11},{3,9}... | collective-permute-start | bytes 411656 | tf_op jit(solution)/shard_map/ppermute | solution.py:48
  43.4 21.6 %collective-permute-start.9 = (bf16[536,128]{1,0:T(8,128)(2,1)S(1)}, bf16[536,128]{1,0:T(8,128)(2,1)S(1)}, u32[]{:S(2)}, u32[]{:S(2)}) collective-permute-start(bf16[536,128]{1,0:T(8,128)(2,1)S(1)} %get-tuple-element.44), channel_id=1, source_target_pairs={{0,12},{2,14},{4,8},{6,10},{8,4},{10,6},{12,0},{14,2},{1,13},{3,15... | collective-permute-start | bytes 411656 | tf_op jit(solution)/shard_map/ppermute | solution.py:48
  44.9 22.4 %collective-permute-start.10 = (bf16[536,128]{1,0:T(8,128)(2,1)S(1)}, bf16[536,128]{1,0:T(8,128)(2,1)S(1)}, u32[]{:S(2)}, u32[]{:S(2)}) collective-permute-start(bf16[536,128]{1,0:T(8,128)(2,1)S(1)} %get-tuple-element.45), channel_id=1, source_target_pairs={{0,14},{2,12},{4,10},{6,8},{8,6},{10,4},{12,2},{14,0},{1,15},{3,13... | collective-permute-start | bytes 411656 | tf_op jit(solution)/shard_map/ppermute | solution.py:48
  50.5 30.7 %collective-permute-start = (bf16[512,128]{1,0:T(8,128)(2,1)S(1)}, bf16[512,128]{1,0:T(8,128)(2,1)S(1)}, u32[]{:S(2)}, u32[]{:S(2)}) collective-permute-start(bf16[512,128]{1,0:T(8,128)(2,1)S(1)} %get-tuple-element.35), channel_id=1, source_target_pairs={{0,8},{2,10},{4,12},{6,14},{8,0},{10,2},{12,4},{14,6},{1,9},{3,11}... | collective-permute-start | bytes 393224 | tf_op jit(solution)/shard_map/ppermute | solution.py:48
  59.7 21.5 %collective-permute-start.1 = (bf16[512,128]{1,0:T(8,128)(2,1)S(1)}, bf16[512,128]{1,0:T(8,128)(2,1)S(1)}, u32[]{:S(2)}, u32[]{:S(2)}) collective-permute-start(bf16[512,128]{1,0:T(8,128)(2,1)S(1)} %get-tuple-element.36), channel_id=1, source_target_pairs={{0,10},{2,8},{4,14},{6,12},{8,2},{10,0},{12,6},{14,4},{1,11},{3,9}... | collective-permute-start | bytes 393224 | tf_op jit(solution)/shard_map/ppermute | solution.py:48
  63.4 17.8 %collective-permute-start.2 = (bf16[512,128]{1,0:T(8,128)(2,1)S(1)}, bf16[512,128]{1,0:T(8,128)(2,1)S(1)}, u32[]{:S(2)}, u32[]{:S(2)}) collective-permute-start(bf16[512,128]{1,0:T(8,128)(2,1)S(1)} %get-tuple-element.37), channel_id=1, source_target_pairs={{0,12},{2,14},{4,8},{6,10},{8,4},{10,6},{12,0},{14,2},{1,13},{3,15... | collective-permute-start | bytes 393224 | tf_op jit(solution)/shard_map/ppermute | solution.py:48
  65.0 16.2 %collective-permute-start.3 = (bf16[512,128]{1,0:T(8,128)(2,1)S(1)}, bf16[512,128]{1,0:T(8,128)(2,1)S(1)}, u32[]{:S(2)}, u32[]{:S(2)}) collective-permute-start(bf16[512,128]{1,0:T(8,128)(2,1)S(1)} %get-tuple-element.38), channel_id=1, source_target_pairs={{0,14},{2,12},{4,10},{6,8},{8,6},{10,4},{12,2},{14,0},{1,15},{3,13... | collective-permute-start | bytes 393224 | tf_op jit(solution)/shard_map/ppermute | solution.py:48
  67.3 11.2 %collective-permute-start.20 = (bf16[512,128]{1,0:T(8,128)(2,1)S(1)}, bf16[512,128]{1,0:T(8,128)(2,1)S(1)}, u32[]{:S(2)}, u32[]{:S(2)}) collective-permute-start(bf16[512,128]{1,0:T(8,128)(2,1)S(1)} %get-tuple-element.56), channel_id=1, source_target_pairs={{0,6},{2,4},{4,2},{6,0},{8,14},{10,12},{12,10},{14,8},{1,7},{3,5},... | collective-permute-start | bytes 393224 | tf_op jit(solution)/shard_map/ppermute | solution.py:48
  78.6 2.6 %copy-start.6 = (bf16[1,2,64]{2,1,0:T(2,128)(2,1)S(1)}, bf16[1,2,64]{2,1,0:T(2,128)(2,1)}, u32[]{:S(2)}) copy-start(bf16[1,2,64]{2,1,0:T(2,128)(2,1)} %refs_8_.3) | copy-start | bytes 772
  82.2 4.6 %collective-permute-start.21 = (f32[1,128]{1,0:T(1,128)S(1)}, f32[1,128]{1,0:T(1,128)S(1)}, u32[]{:S(2)}, u32[]{:S(2)}) collective-permute-start(f32[1,128]{1,0:T(1,128)S(1)} %get-tuple-element.63), channel_id=1, source_target_pairs={{0,2},{2,0},{4,6},{6,4},{8,10},{10,8},{12,14},{14,12},{1,3},{3,1},... | collective-permute-start | bytes 1544 | tf_op jit(solution)/shard_map/ppermute | solution.py:48
  85.0 1.9 %copy-start.7 = (f32[2,64]{1,0:T(2,128)S(1)}, f32[2,64]{1,0:T(2,128)}, u32[]{:S(2)}) copy-start(f32[2,64]{1,0:T(2,128)} %param.23) | copy-start | bytes 1540

commit v4 on v3

--- a/solution.py
+++ b/solution.py
@@ -628,8 +628,11 @@
         cut,
     )
     half = devices // 2
-    first, final = list(range(half)), list(range(half, devices))
-    out, read = late_rows(first, late_blocks, edges, keys, weight, taps, read, out, cut)
+    first = list(range(half))
+    middle = [offset for offset in range(half, devices) if offset % group_devices == 0]
+    final = [offset for offset in range(half, devices) if offset % group_devices]
+    for wave in (first, middle):
+        out, read = late_rows(wave, late_blocks, edges, keys, weight, taps, read, out, cut)
     values, gated, group_sq = last_read(final, late_blocks, edges, weight, taps, read, newest_output_switch, cut)
     for level in range(group_devices.bit_length() - 1):
         group_sq = group_sq + flip_permute(group_sq, 2**level)

time: 87.6 us -> 79.2 us (0.904)
  waiting for transfers between devices: 16.9 us -> 5.54 us
  starting transfers between devices: 39 us -> 41.6 us
    ppermute x22, waiting for transfers between devices: 16.9 us -> 5.54 us  [flip_permute(): return lax.ppermute(value, 'sp', pairs)]
    ppermute x22, starting transfers between devices: 39 us -> 41.6 us  [flip_permute(): return lax.ppermute(value, 'sp', pairs)]
    pallas_call x1 -> x2, Pallas kernels: 2.62 us -> 4.13 us  [late_rows(): pl.pallas_call(lambda *refs: late_kernel(cut, offsets, *refs), grid=(len(...]
  transfers between devices with their start and end apart: 22 -> 22, of which waited for: 4 -> 4; matrix products, arithmetic and copies ran while one was open for 0% -> 0% of each run, Pallas kernels for 29% -> 33%
where the time goes in v4:
time: 79.2 us; the launch traced here: 79 us
  starting transfers between devices  41.6 us (53%)
  Pallas kernels  30.4 us (38%)
  waiting for transfers between devices  5.54 us (7%)
  between operations  0.82 us (1%)
    ppermute x22, starting transfers between devices, flip_permute(): return lax.ppermute(value, 'sp', pairs)  41.6 us
    pallas_call x1, Pallas kernels, early_values(): pl.pallas_call(early_value_kernel, grid=(steps,), in_specs=[whole((cut, m...  7.12 us
    pallas_call x1, Pallas kernels, early_rows(): pl.pallas_call(lambda *refs: early_kernel(cut, *refs), grid=(sources,), i...  5.8 us
    pallas_call x1, Pallas kernels, late_values(): pl.pallas_call(late_value_kernel, grid=(width // tile,), in_specs=[pl.Blo...  5.58 us
    ppermute x22, waiting for transfers between devices, flip_permute(): return lax.ppermute(value, 'sp', pairs)  5.54 us
    pallas_call x2, Pallas kernels, late_rows(): pl.pallas_call(lambda *refs: late_kernel(cut, offsets, *refs), grid=(len(...  4.13 us
    pallas_call x1, Pallas kernels, key_blocks(): pl.pallas_call(lambda *refs: key_block_kernel(group_devices, *refs), grid...  3.56 us
    pallas_call x1, Pallas kernels, key_read(): pl.pallas_call(lambda *refs: key_read_kernel(group_devices, *refs), in_sp...  2.6 us
  transfers between devices with their start and end apart: 22, of which 4 were waited for; matrix products, arithmetic and copies ran while one was open for 0% of the time, Pallas kernels for 33%

profile of v4, /device:TPU:0, one launch (start us, length us, event | category | flops | bytes accessed | tf_op | source)
XLA Modules:
  0.0 79.0 jit_solution(5575740238918849222)
XLA Ops:
  0.6 3.6 %key_blocks.1 = (bf16[512,128]{1,0:T(8,128)(2,1)S(1)}, bf16[512,128]{1,0:T(8,128)(2,1)S(1)}, bf16[512,128]{1,0:T(8,128)(2,1)S(1)}, bf16[512,128]{1,0:T(8,128)(2,1)S(1)}) custom-call(bf16[1024,2048]{1,0:T(8,128)(2,1)} %bitcast.7, bf16[1024,2048]{1,0:T(8,128)(2,1)} %bitcast.8, bf16[2048,256]{1,0:T(8,128)(2,1)} %refs_2_.1), custom_call_target="tpu_custom_call" | custom-call | flops 1073741824 | bytes 4194304 | tf_op jit(solution)/shard_map/key_blocks/pallas_call | solution.py:81
  4.2 3.1 %collective-permute-start.9 = (bf16[512,128]{1,0:T(8,128)(2,1)S(1)}, bf16[512,128]{1,0:T(8,128)(2,1)S(1)}, u32[]{:S(2)}, u32[]{:S(2)}) collective-permute-start(bf16[512,128]{1,0:T(8,128)(2,1)S(1)} %get-tuple-element.46), channel_id=1, source_target_pairs={{0,4},{2,6},{4,0},{6,2},{8,12},{10,14},{12,8},{14,10},{1,5},{3,7},... | collective-permute-start | bytes 393224 | tf_op jit(solution)/shard_map/ppermute | solution.py:48
  7.3 2.6 %collective-permute-start.10 = (bf16[512,128]{1,0:T(8,128)(2,1)S(1)}, bf16[512,128]{1,0:T(8,128)(2,1)S(1)}, u32[]{:S(2)}, u32[]{:S(2)}) collective-permute-start(bf16[512,128]{1,0:T(8,128)(2,1)S(1)} %get-tuple-element.47), channel_id=1, source_target_pairs={{0,8},{2,10},{4,12},{6,14},{8,0},{10,2},{12,4},{14,6},{1,9},{3,11}... | collective-permute-start | bytes 393224 | tf_op jit(solution)/shard_map/ppermute | solution.py:48
  9.9 1.7 %collective-permute-start.12 = (bf16[512,128]{1,0:T(8,128)(2,1)S(1)}, bf16[512,128]{1,0:T(8,128)(2,1)S(1)}, u32[]{:S(2)}, u32[]{:S(2)}) collective-permute-start(bf16[512,128]{1,0:T(8,128)(2,1)S(1)} %get-tuple-element.35._.refs_0_), channel_id=1, source_target_pairs={{0,2},{2,0},{4,6},{6,4},{8,10},{10,8},{12,14},{14,12},{1,3},{3,1},... | collective-permute-start | bytes 393224 | tf_op jit(solution)/shard_map/ppermute | solution.py:48
  11.6 7.1 %early_values.1 = (bf16[536,128]{1,0:T(8,128)(2,1)S(1)}, bf16[536,128]{1,0:T(8,128)(2,1)S(1)}, bf16[536,128]{1,0:T(8,128)(2,1)S(1)}, bf16[536,128]{1,0:T(8,128)(...) custom-call(bf16[1024,2048]{1,0:T(8,128)(2,1)} %bitcast.9, ...), custom_call_target="tpu_custom_call" | custom-call | flops 2147483648 | bytes 8388608 | tf_op jit(solution)/shard_map/early_values/pallas_call | solution.py:150
  19.1 0.9 %collective-permute-start.3 = (bf16[536,128]{1,0:T(8,128)(2,1)S(1)}, bf16[536,128]{1,0:T(8,128)(2,1)S(1)}, u32[]{:S(2)}, u32[]{:S(2)}) collective-permute-start(bf16[536,128]{1,0:T(8,128)(2,1)S(1)} %get-tuple-element.40), channel_id=1, source_target_pairs={{0,4},{2,6},{4,0},{6,2},{8,12},{10,14},{12,8},{14,10},{1,5},{3,7},... | collective-permute-start | bytes 411656 | tf_op jit(solution)/shard_map/ppermute | solution.py:48
  20.2 1.5 %collective-permute-start.13 = (bf16[512,128]{1,0:T(8,128)(2,1)S(1)}, bf16[512,128]{1,0:T(8,128)(2,1)S(1)}, u32[]{:S(2)}, u32[]{:S(2)}) collective-permute-start(bf16[512,128]{1,0:T(8,128)(2,1)S(1)} %collective-permute-done.9.refs_1_), channel_id=1, source_target_pairs={{0,2},{2,0},{4,6},{6,4},{8,10},{10,8},{12,14},{14,12},{1,3},{3,1},... | collective-permute-start | bytes 393224 | tf_op jit(solution)/shard_map/ppermute | solution.py:48
  21.7 0.5 collective-permute-start.14
  22.2 1.5 %collective-permute-start.15 = (bf16[512,128]{1,0:T(8,128)(2,1)S(1)}, bf16[512,128]{1,0:T(8,128)(2,1)S(1)}, u32[]{:S(2)}, u32[]{:S(2)}) collective-permute-start(bf16[512,128]{1,0:T(8,128)(2,1)S(1)} %collective-permute-done.11.refs_3_), channel_id=1, source_target_pairs={{0,2},{2,0},{4,6},{6,4},{8,10},{10,8},{12,14},{14,12},{1,3},{3,1},... | collective-permute-start | bytes 393224 | tf_op jit(solution)/shard_map/ppermute | solution.py:48
  23.8 1.9 %collective-permute-done.2.refs_1_ = bf16[536,128]{1,0:T(8,128)(2,1)S(1)} collective-permute-done((bf16[536,128]{1,0:T(8,128)(2,1)S(1)}, bf16[536,128]{1,0:T(8,128)(2,1)S(1)}, u32[]{:S(2)}, u32[]{:S(2)}) %collective-permute-start.2) | collective-permute-done | bytes 137248 | tf_op jit(solution)/shard_map/ppermute | solution.py:48
  25.8 4.0 %collective-permute-start.5 = (bf16[536,128]{1,0:T(8,128)(2,1)S(1)}, bf16[536,128]{1,0:T(8,128)(2,1)S(1)}, u32[]{:S(2)}, u32[]{:S(2)}) collective-permute-start(bf16[536,128]{1,0:T(8,128)(2,1)S(1)} %get-tuple-element.42), channel_id=1, source_target_pairs={{0,8},{2,10},{4,12},{6,14},{8,0},{10,2},{12,4},{14,6},{1,9},{3,11}... | collective-permute-start | bytes 411656 | tf_op jit(solution)/shard_map/ppermute | solution.py:48
  29.8 5.4 %collective-permute-start.6 = (bf16[536,128]{1,0:T(8,128)(2,1)S(1)}, bf16[536,128]{1,0:T(8,128)(2,1)S(1)}, u32[]{:S(2)}, u32[]{:S(2)}) collective-permute-start(bf16[536,128]{1,0:T(8,128)(2,1)S(1)} %get-tuple-element.43), channel_id=1, source_target_pairs={{0,10},{2,8},{4,14},{6,12},{8,2},{10,0},{12,6},{14,4},{1,11},{3,9}... | collective-permute-start | bytes 411656 | tf_op jit(solution)/shard_map/ppermute | solution.py:48
  35.3 1.9 %collective-permute-start.7 = (bf16[536,128]{1,0:T(8,128)(2,1)S(1)}, bf16[536,128]{1,0:T(8,128)(2,1)S(1)}, u32[]{:S(2)}, u32[]{:S(2)}) collective-permute-start(bf16[536,128]{1,0:T(8,128)(2,1)S(1)} %get-tuple-element.44), channel_id=1, source_target_pairs={{0,12},{2,14},{4,8},{6,10},{8,4},{10,6},{12,0},{14,2},{1,13},{3,15... | collective-permute-start | bytes 411656 | tf_op jit(solution)/shard_map/ppermute | solution.py:48
  37.2 1.9 %collective-permute-start.8 = (bf16[536,128]{1,0:T(8,128)(2,1)S(1)}, bf16[536,128]{1,0:T(8,128)(2,1)S(1)}, u32[]{:S(2)}, u32[]{:S(2)}) collective-permute-start(bf16[536,128]{1,0:T(8,128)(2,1)S(1)} %get-tuple-element.45), channel_id=1, source_target_pairs={{0,14},{2,12},{4,10},{6,8},{8,6},{10,4},{12,2},{14,0},{1,15},{3,13... | collective-permute-start | bytes 411656 | tf_op jit(solution)/shard_map/ppermute | solution.py:48
  39.0 5.6 %late_values.1 = (bf16[512,128]{1,0:T(8,128)(2,1)S(1)}, bf16[512,128]{1,0:T(8,128)(2,1)S(1)}, bf16[512,128]{1,0:T(8,128)(2,1)S(1)}, bf16[512,128]{1,0:T(8,128)(2...) custom-call(bf16[1024,2048]{1,0:T(8,128)(2,1)} %bitcast.13, ...), custom_call_target="tpu_custom_call" | custom-call | flops 2147483648 | bytes 6291456 | tf_op jit(solution)/shard_map/late_values/pallas_call | solution.py:196
  44.6 2.6 %key_read.1 = (bf16[8,1024,128]{2,1,0:T(8,128)(2,1)S(1)}, f32[8,8,128]{2,1,0:T(8,128)S(1)}) custom-call(bf16[512,128]{1,0:T(8,128)(2,1)S(1)} %get-tuple-element.35._.refs_0_, bf16[512,128]{1,0:T(8,128)(2,1)S(1)} %collective-permute-done.9.refs_1_, bf16[512,128]{1,0:T(8,128)(2,1)S(1)} %collective-permute-done.10.refs_2_, ...), custom_call_target="tpu_custom_call" | custom-call | flops 1000000000 | bytes 4000000 | tf_op jit(solution)/shard_map/key_read/pallas_call | solution.py:273
  47.3 0.9 %collective-permute-start.16 = (bf16[512,128]{1,0:T(8,128)(2,1)S(1)}, bf16[512,128]{1,0:T(8,128)(2,1)S(1)}, u32[]{:S(2)}, u32[]{:S(2)}) collective-permute-start(bf16[512,128]{1,0:T(8,128)(2,1)S(1)} %get-tuple-element.53), channel_id=1, source_target_pairs={{0,8},{2,10},{4,12},{6,14},{8,0},{10,2},{12,4},{14,6},{1,9},{3,11}... | collective-permute-start | bytes 393224 | tf_op jit(solution)/shard_map/ppermute | solution.py:48
  48.2 1.6 %collective-permute-start.17 = (bf16[512,128]{1,0:T(8,128)(2,1)S(1)}, bf16[512,128]{1,0:T(8,128)(2,1)S(1)}, u32[]{:S(2)}, u32[]{:S(2)}) collective-permute-start(bf16[512,128]{1,0:T(8,128)(2,1)S(1)} %get-tuple-element.54), channel_id=1, source_target_pairs={{0,12},{2,14},{4,8},{6,10},{8,4},{10,6},{12,0},{14,2},{1,13},{3,15... | collective-permute-start | bytes 393224 | tf_op jit(solution)/shard_map/ppermute | solution.py:48
  49.8 2.7 %collective-permute-start.18 = (bf16[512,128]{1,0:T(8,128)(2,1)S(1)}, bf16[512,128]{1,0:T(8,128)(2,1)S(1)}, u32[]{:S(2)}, u32[]{:S(2)}) collective-permute-start(bf16[512,128]{1,0:T(8,128)(2,1)S(1)} %get-tuple-element.56), channel_id=1, source_target_pairs={{0,2},{2,0},{4,6},{6,4},{8,10},{10,8},{12,14},{14,12},{1,3},{3,1},... | collective-permute-start | bytes 393224 | tf_op jit(solution)/shard_map/ppermute | solution.py:48
  52.6 0.5 collective-permute-start.19
  53.1 6.1 %collective-permute-start.20 = (bf16[512,128]{1,0:T(8,128)(2,1)S(1)}, bf16[512,128]{1,0:T(8,128)(2,1)S(1)}, u32[]{:S(2)}, u32[]{:S(2)}) collective-permute-start(bf16[512,128]{1,0:T(8,128)(2,1)S(1)} %get-tuple-element.58), channel_id=1, source_target_pairs={{0,6},{2,4},{4,2},{6,0},{8,14},{10,12},{12,10},{14,8},{1,7},{3,5},... | collective-permute-start | bytes 393224 | tf_op jit(solution)/shard_map/ppermute | solution.py:48
  59.2 5.8 %early_rows.1 = (bf16[8,2048,128]{2,1,0:T(8,128)(2,1)}, f32[32,128]{1,0:T(8,128)S(1)}, bf16[8,32,128]{2,1,0:T(8,128)(2,1)S(1)}, f32[8,4,8,128]{3,2,1,0:T(8,128)S(1)}) custom-call(bf16[536,128]{1,0:T(8,128)(2,1)S(1)} %get-tuple-element.36._.refs_0_, bf16[536,128]{1,0:T(8,128)(2,1)S(1)} %collective-permute-done.2.refs_1_, ...), custom_call_target="tpu_custom_call" | custom-call | flops 2000000000 | bytes 6000000 | tf_op jit(solution)/shard_map/early_rows/pallas_call | solution.py:424
  65.0 1.1 %collective-permute-start = (bf16[512,128]{1,0:T(8,128)(2,1)S(1)}, bf16[512,128]{1,0:T(8,128)(2,1)S(1)}, u32[]{:S(2)}, u32[]{:S(2)}) collective-permute-start(bf16[512,128]{1,0:T(8,128)(2,1)S(1)} %get-tuple-element.37), channel_id=1, source_target_pairs={{0,10},{2,8},{4,14},{6,12},{8,2},{10,0},{12,6},{14,4},{1,11},{3,9}... | collective-permute-start | bytes 393224 | tf_op jit(solution)/shard_map/ppermute | solution.py:48
  66.1 2.3 %collective-permute-start.1 = (bf16[512,128]{1,0:T(8,128)(2,1)S(1)}, bf16[512,128]{1,0:T(8,128)(2,1)S(1)}, u32[]{:S(2)}, u32[]{:S(2)}) collective-permute-start(bf16[512,128]{1,0:T(8,128)(2,1)S(1)} %get-tuple-element.38), channel_id=1, source_target_pairs={{0,14},{2,12},{4,10},{6,8},{8,6},{10,4},{12,2},{14,0},{1,15},{3,13... | collective-permute-start | bytes 393224 | tf_op jit(solution)/shard_map/ppermute | solution.py:48
  68.4 2.6 %late_rows.2 = (bf16[8,2048,128]{2,1,0:T(8,128)(2,1)}, f32[32,128]{1,0:T(8,128)S(1)}) custom-call(bf16[512,128]{1,0:T(8,128)(2,1)S(1)} %get-tuple-element.55.refs_0_, bf16[512,128]{1,0:T(8,128)(2,1)S(1)} %collective-permute-done.18.refs_1_, bf16[512,128]{1,0:T(8,128)(2,1)S(1)} %collective-permute-done.19.refs_2_, ...), custom_call_target="tpu_custom_call", output_to_operand_aliasing={{0}: (9, {})} | custom-call | flops 1000000000 | bytes 2000000 | tf_op jit(solution)/shard_map/late_rows/pallas_call | solution.py:499
  71.0 1.5 %late_rows.3 = (bf16[8,2048,128]{2,1,0:T(8,128)(2,1)}, f32[32,128]{1,0:T(8,128)S(1)}) custom-call(bf16[512,128]{1,0:T(8,128)(2,1)S(1)} %collective-permute-done.16.refs_0_, bf16[512,128]{1,0:T(8,128)(2,1)S(1)} %collective-permute-done.17.refs_1_, bf16[8,32,128]{2,1,0:T(8,128)(2,1)S(1)} %get-tuple-element.51.refs_4_.refs_2_, ...), custom_call_target="tpu_custom_call", output_to_operand_aliasing={{0}: (7, {})} | custom-call | flops 1000000000 | bytes 2000000 | tf_op jit(solution)/shard_map/late_rows/pallas_call | solution.py:499
  72.5 1.6 %collective-permute-done.refs_0_ = bf16[512,128]{1,0:T(8,128)(2,1)S(1)} collective-permute-done((bf16[512,128]{1,0:T(8,128)(2,1)S(1)}, bf16[512,128]{1,0:T(8,128)(2,1)S(1)}, u32[]{:S(2)}, u32[]{:S(2)}) %collective-permute-start) | collective-permute-done | bytes 131104 | tf_op jit(solution)/shard_map/ppermute | solution.py:48
  74.1 0.7 last_read.1
  74.8 0.8 %collective-permute-start.21 = (f32[1,128]{1,0:T(1,128)S(1)}, f32[1,128]{1,0:T(1,128)S(1)}, u32[]{:S(2)}, u32[]{:S(2)}) collective-permute-start(f32[1,128]{1,0:T(1,128)S(1)} %get-tuple-element.67), channel_id=1, source_target_pairs={{0,2},{2,0},{4,6},{6,4},{8,10},{10,8},{12,14},{14,12},{1,3},{3,1},... | collective-permute-start | bytes 1544 | tf_op jit(solution)/shard_map/ppermute | solution.py:48
  75.6 1.0 %last_rows.1 = bf16[8,2048,128]{2,1,0:T(8,128)(2,1)} custom-call(bf16[2,512,128]{2,1,0:T(8,128)(2,1)S(1)} %get-tuple-element.64.refs_0_, bf16[8,1024,128]{2,1,0:T(8,128)(2,1)S(1)} %get-tuple-element.49.refs_8_.refs_5_.refs_3_.refs_1_, bf16[8,2048,128]{2,1,0:T(8,128)(2,1)} %get-tuple-element.65.refs_2_), custom_call_target="tpu_custom_call", output_to_operand_aliasing={{}: (2, {})} | custom-call | flops 1000000000 | bytes 2000000 | tf_op jit(solution)/shard_map/last_rows/pallas_call | solution.py:566
  76.6 1.8 %collective-permute-done.21 = f32[1,128]{1,0:T(1,128)S(1)} collective-permute-done((f32[1,128]{1,0:T(1,128)S(1)}, f32[1,128]{1,0:T(1,128)S(1)}, u32[]{:S(2)}, u32[]{:S(2)}) %collective-permute-start.21) | collective-permute-done | bytes 544 | tf_op jit(solution)/shard_map/ppermute | solution.py:48
  78.5 0.5 fusion
  (39 shorter events, 0.8 us)
Async XLA Ops:
  4.2 14.9 %collective-permute-start.9 = (bf16[512,128]{1,0:T(8,128)(2,1)S(1)}, bf16[512,128]{1,0:T(8,128)(2,1)S(1)}, u32[]{:S(2)}, u32[]{:S(2)}) collective-permute-start(bf16[512,128]{1,0:T(8,128)(2,1)S(1)} %get-tuple-element.46), channel_id=1, source_target_pairs={{0,4},{2,6},{4,0},{6,2},{8,12},{10,14},{12,8},{14,10},{1,5},{3,7},... | collective-permute-start | bytes 393224 | tf_op jit(solution)/shard_map/ppermute | solution.py:48
  7.3 12.9 %collective-permute-start.10 = (bf16[512,128]{1,0:T(8,128)(2,1)S(1)}, bf16[512,128]{1,0:T(8,128)(2,1)S(1)}, u32[]{:S(2)}, u32[]{:S(2)}) collective-permute-start(bf16[512,128]{1,0:T(8,128)(2,1)S(1)} %get-tuple-element.47), channel_id=1, source_target_pairs={{0,8},{2,10},{4,12},{6,14},{8,0},{10,2},{12,4},{14,6},{1,9},{3,11}... | collective-permute-start | bytes 393224 | tf_op jit(solution)/shard_map/ppermute | solution.py:48
  9.9 11.8 %collective-permute-start.11 = (bf16[512,128]{1,0:T(8,128)(2,1)S(1)}, bf16[512,128]{1,0:T(8,128)(2,1)S(1)}, u32[]{:S(2)}, u32[]{:S(2)}) collective-permute-start(bf16[512,128]{1,0:T(8,128)(2,1)S(1)} %get-tuple-element.48), channel_id=1, source_target_pairs={{0,12},{2,14},{4,8},{6,10},{8,4},{10,6},{12,0},{14,2},{1,13},{3,15... | collective-permute-start | bytes 393224 | tf_op jit(solution)/shard_map/ppermute | solution.py:48
  9.9 12.3 %collective-permute-start.12 = (bf16[512,128]{1,0:T(8,128)(2,1)S(1)}, bf16[512,128]{1,0:T(8,128)(2,1)S(1)}, u32[]{:S(2)}, u32[]{:S(2)}) collective-permute-start(bf16[512,128]{1,0:T(8,128)(2,1)S(1)} %get-tuple-element.35._.refs_0_), channel_id=1, source_target_pairs={{0,2},{2,0},{4,6},{6,4},{8,10},{10,8},{12,14},{14,12},{1,3},{3,1},... | collective-permute-start | bytes 393224 | tf_op jit(solution)/shard_map/ppermute | solution.py:48
  18.8 6.9 %collective-permute-start.2 = (bf16[536,128]{1,0:T(8,128)(2,1)S(1)}, bf16[536,128]{1,0:T(8,128)(2,1)S(1)}, u32[]{:S(2)}, u32[]{:S(2)}) collective-permute-start(bf16[536,128]{1,0:T(8,128)(2,1)S(1)} %get-tuple-element.39), channel_id=1, source_target_pairs={{0,2},{2,0},{4,6},{6,4},{8,10},{10,8},{12,14},{14,12},{1,3},{3,1},... | collective-permute-start | bytes 411656 | tf_op jit(solution)/shard_map/ppermute | solution.py:48
  19.1 6.7 %collective-permute-start.3 = (bf16[536,128]{1,0:T(8,128)(2,1)S(1)}, bf16[536,128]{1,0:T(8,128)(2,1)S(1)}, u32[]{:S(2)}, u32[]{:S(2)}) collective-permute-start(bf16[536,128]{1,0:T(8,128)(2,1)S(1)} %get-tuple-element.40), channel_id=1, source_target_pairs={{0,4},{2,6},{4,0},{6,2},{8,12},{10,14},{12,8},{14,10},{1,5},{3,7},... | collective-permute-start | bytes 411656 | tf_op jit(solution)/shard_map/ppermute | solution.py:48
  20.2 9.7 %collective-permute-start.13 = (bf16[512,128]{1,0:T(8,128)(2,1)S(1)}, bf16[512,128]{1,0:T(8,128)(2,1)S(1)}, u32[]{:S(2)}, u32[]{:S(2)}) collective-permute-start(bf16[512,128]{1,0:T(8,128)(2,1)S(1)} %collective-permute-done.9.refs_1_), channel_id=1, source_target_pairs={{0,2},{2,0},{4,6},{6,4},{8,10},{10,8},{12,14},{14,12},{1,3},{3,1},... | collective-permute-start | bytes 393224 | tf_op jit(solution)/shard_map/ppermute | solution.py:48
  21.7 13.5 %collective-permute-start.14 = (bf16[512,128]{1,0:T(8,128)(2,1)S(1)}, bf16[512,128]{1,0:T(8,128)(2,1)S(1)}, u32[]{:S(2)}, u32[]{:S(2)}) collective-permute-start(bf16[512,128]{1,0:T(8,128)(2,1)S(1)} %collective-permute-done.10.refs_2_), channel_id=1, source_target_pairs={{0,2},{2,0},{4,6},{6,4},{8,10},{10,8},{12,14},{14,12},{1,3},{3,1},... | collective-permute-start | bytes 393224 | tf_op jit(solution)/shard_map/ppermute | solution.py:48
  22.2 14.9 %collective-permute-start.15 = (bf16[512,128]{1,0:T(8,128)(2,1)S(1)}, bf16[512,128]{1,0:T(8,128)(2,1)S(1)}, u32[]{:S(2)}, u32[]{:S(2)}) collective-permute-start(bf16[512,128]{1,0:T(8,128)(2,1)S(1)} %collective-permute-done.11.refs_3_), channel_id=1, source_target_pairs={{0,2},{2,0},{4,6},{6,4},{8,10},{10,8},{12,14},{14,12},{1,3},{3,1},... | collective-permute-start | bytes 393224 | tf_op jit(solution)/shard_map/ppermute | solution.py:48
  25.7 21.6 %collective-permute-start.4 = (bf16[536,128]{1,0:T(8,128)(2,1)S(1)}, bf16[536,128]{1,0:T(8,128)(2,1)S(1)}, u32[]{:S(2)}, u32[]{:S(2)}) collective-permute-start(bf16[536,128]{1,0:T(8,128)(2,1)S(1)} %get-tuple-element.41), channel_id=1, source_target_pairs={{0,6},{2,4},{4,2},{6,0},{8,14},{10,12},{12,10},{14,8},{1,7},{3,5},... | collective-permute-start | bytes 411656 | tf_op jit(solution)/shard_map/ppermute | solution.py:48
  25.8 22.3 %collective-permute-start.5 = (bf16[536,128]{1,0:T(8,128)(2,1)S(1)}, bf16[536,128]{1,0:T(8,128)(2,1)S(1)}, u32[]{:S(2)}, u32[]{:S(2)}) collective-permute-start(bf16[536,128]{1,0:T(8,128)(2,1)S(1)} %get-tuple-element.42), channel_id=1, source_target_pairs={{0,8},{2,10},{4,12},{6,14},{8,0},{10,2},{12,4},{14,6},{1,9},{3,11}... | collective-permute-start | bytes 411656 | tf_op jit(solution)/shard_map/ppermute | solution.py:48
  29.8 20.0 %collective-permute-start.6 = (bf16[536,128]{1,0:T(8,128)(2,1)S(1)}, bf16[536,128]{1,0:T(8,128)(2,1)S(1)}, u32[]{:S(2)}, u32[]{:S(2)}) collective-permute-start(bf16[536,128]{1,0:T(8,128)(2,1)S(1)} %get-tuple-element.43), channel_id=1, source_target_pairs={{0,10},{2,8},{4,14},{6,12},{8,2},{10,0},{12,6},{14,4},{1,11},{3,9}... | collective-permute-start | bytes 411656 | tf_op jit(solution)/shard_map/ppermute | solution.py:48
  35.3 17.3 %collective-permute-start.7 = (bf16[536,128]{1,0:T(8,128)(2,1)S(1)}, bf16[536,128]{1,0:T(8,128)(2,1)S(1)}, u32[]{:S(2)}, u32[]{:S(2)}) collective-permute-start(bf16[536,128]{1,0:T(8,128)(2,1)S(1)} %get-tuple-element.44), channel_id=1, source_target_pairs={{0,12},{2,14},{4,8},{6,10},{8,4},{10,6},{12,0},{14,2},{1,13},{3,15... | collective-permute-start | bytes 411656 | tf_op jit(solution)/shard_map/ppermute | solution.py:48
  37.2 15.9 %collective-permute-start.8 = (bf16[536,128]{1,0:T(8,128)(2,1)S(1)}, bf16[536,128]{1,0:T(8,128)(2,1)S(1)}, u32[]{:S(2)}, u32[]{:S(2)}) collective-permute-start(bf16[536,128]{1,0:T(8,128)(2,1)S(1)} %get-tuple-element.45), channel_id=1, source_target_pairs={{0,14},{2,12},{4,10},{6,8},{8,6},{10,4},{12,2},{14,0},{1,15},{3,13... | collective-permute-start | bytes 411656 | tf_op jit(solution)/shard_map/ppermute | solution.py:48
  39.0 5.6 %copy-start.2 = (f32[5,4,64]{2,1,0:T(4,128)S(1)}, f32[5,4,64]{2,1,0:T(4,128)}, u32[]{:S(2)}) copy-start(f32[5,4,64]{2,1,0:T(4,128)} %refs_8_.1) | copy-start | bytes 15364
  39.0 5.6 %copy-start.3 = (bf16[1,4,64]{2,1,0:T(4,128)(2,1)S(1)}, bf16[1,4,64]{2,1,0:T(4,128)(2,1)}, u32[]{:S(2)}) copy-start(bf16[1,4,64]{2,1,0:T(4,128)(2,1)} %refs_9_.1) | copy-start | bytes 1540
  39.0 20.1 %copy-start = (f32[5,2,64]{2,1,0:T(2,128)S(1)}, f32[5,2,64]{2,1,0:T(2,128)}, u32[]{:S(2)}) copy-start(f32[5,2,64]{2,1,0:T(2,128)} %refs_4_.1) | copy-start | bytes 7684
  39.0 20.1 %copy-start.1 = (f32[1,2,8192]{2,1,0:T(2,128)S(1)}, f32[1,2,8192]{2,1,0:T(2,128)}, u32[]{:S(2)}) copy-start(f32[1,2,8192]{2,1,0:T(2,128)} %refs_11_.1) | copy-start | bytes 196612
  39.0 20.1 %copy-start.4 = (f32[2]{0:T(128)S(1)}, f32[2]{0:T(128)}, u32[]{:S(2)}) copy-start(f32[2]{0:T(128)} %refs_12_.1) | copy-start | bytes 28
  39.0 20.1 %copy-start.5 = (f32[2]{0:T(128)S(1)}, f32[2]{0:T(128)}, u32[]{:S(2)}) copy-start(f32[2]{0:T(128)} %refs_13_.1) | copy-start | bytes 28
  47.3 23.7 %collective-permute-start.16 = (bf16[512,128]{1,0:T(8,128)(2,1)S(1)}, bf16[512,128]{1,0:T(8,128)(2,1)S(1)}, u32[]{:S(2)}, u32[]{:S(2)}) collective-permute-start(bf16[512,128]{1,0:T(8,128)(2,1)S(1)} %get-tuple-element.53), channel_id=1, source_target_pairs={{0,8},{2,10},{4,12},{6,14},{8,0},{10,2},{12,4},{14,6},{1,9},{3,11}... | collective-permute-start | bytes 393224 | tf_op jit(solution)/shard_map/ppermute | solution.py:48
  48.2 22.8 %collective-permute-start.17 = (bf16[512,128]{1,0:T(8,128)(2,1)S(1)}, bf16[512,128]{1,0:T(8,128)(2,1)S(1)}, u32[]{:S(2)}, u32[]{:S(2)}) collective-permute-start(bf16[512,128]{1,0:T(8,128)(2,1)S(1)} %get-tuple-element.54), channel_id=1, source_target_pairs={{0,12},{2,14},{4,8},{6,10},{8,4},{10,6},{12,0},{14,2},{1,13},{3,15... | collective-permute-start | bytes 393224 | tf_op jit(solution)/shard_map/ppermute | solution.py:48
  49.8 15.1 %collective-permute-start.18 = (bf16[512,128]{1,0:T(8,128)(2,1)S(1)}, bf16[512,128]{1,0:T(8,128)(2,1)S(1)}, u32[]{:S(2)}, u32[]{:S(2)}) collective-permute-start(bf16[512,128]{1,0:T(8,128)(2,1)S(1)} %get-tuple-element.56), channel_id=1, source_target_pairs={{0,2},{2,0},{4,6},{6,4},{8,10},{10,8},{12,14},{14,12},{1,3},{3,1},... | collective-permute-start | bytes 393224 | tf_op jit(solution)/shard_map/ppermute | solution.py:48
  52.6 13.6 %collective-permute-start.19 = (bf16[512,128]{1,0:T(8,128)(2,1)S(1)}, bf16[512,128]{1,0:T(8,128)(2,1)S(1)}, u32[]{:S(2)}, u32[]{:S(2)}) collective-permute-start(bf16[512,128]{1,0:T(8,128)(2,1)S(1)} %get-tuple-element.57), channel_id=1, source_target_pairs={{0,4},{2,6},{4,0},{6,2},{8,12},{10,14},{12,8},{14,10},{1,5},{3,7},... | collective-permute-start | bytes 393224 | tf_op jit(solution)/shard_map/ppermute | solution.py:48
  53.1 15.3 %collective-permute-start.20 = (bf16[512,128]{1,0:T(8,128)(2,1)S(1)}, bf16[512,128]{1,0:T(8,128)(2,1)S(1)}, u32[]{:S(2)}, u32[]{:S(2)}) collective-permute-start(bf16[512,128]{1,0:T(8,128)(2,1)S(1)} %get-tuple-element.58), channel_id=1, source_target_pairs={{0,6},{2,4},{4,2},{6,0},{8,14},{10,12},{12,10},{14,8},{1,7},{3,5},... | collective-permute-start | bytes 393224 | tf_op jit(solution)/shard_map/ppermute | solution.py:48
  65.0 9.2 %collective-permute-start = (bf16[512,128]{1,0:T(8,128)(2,1)S(1)}, bf16[512,128]{1,0:T(8,128)(2,1)S(1)}, u32[]{:S(2)}, u32[]{:S(2)}) collective-permute-start(bf16[512,128]{1,0:T(8,128)(2,1)S(1)} %get-tuple-element.37), channel_id=1, source_target_pairs={{0,10},{2,8},{4,14},{6,12},{8,2},{10,0},{12,6},{14,4},{1,11},{3,9}... | collective-permute-start | bytes 393224 | tf_op jit(solution)/shard_map/ppermute | solution.py:48
  66.1 8.0 %collective-permute-start.1 = (bf16[512,128]{1,0:T(8,128)(2,1)S(1)}, bf16[512,128]{1,0:T(8,128)(2,1)S(1)}, u32[]{:S(2)}, u32[]{:S(2)}) collective-permute-start(bf16[512,128]{1,0:T(8,128)(2,1)S(1)} %get-tuple-element.38), channel_id=1, source_target_pairs={{0,14},{2,12},{4,10},{6,8},{8,6},{10,4},{12,2},{14,0},{1,15},{3,13... | collective-permute-start | bytes 393224 | tf_op jit(solution)/shard_map/ppermute | solution.py:48
  71.0 3.2 %copy-start.6 = (bf16[1,2,64]{2,1,0:T(2,128)(2,1)S(1)}, bf16[1,2,64]{2,1,0:T(2,128)(2,1)}, u32[]{:S(2)}) copy-start(bf16[1,2,64]{2,1,0:T(2,128)(2,1)} %refs_6_.1) | copy-start | bytes 772
  74.8 3.6 %collective-permute-start.21 = (f32[1,128]{1,0:T(1,128)S(1)}, f32[1,128]{1,0:T(1,128)S(1)}, u32[]{:S(2)}, u32[]{:S(2)}) collective-permute-start(f32[1,128]{1,0:T(1,128)S(1)} %get-tuple-element.67), channel_id=1, source_target_pairs={{0,2},{2,0},{4,6},{6,4},{8,10},{10,8},{12,14},{14,12},{1,3},{3,1},... | collective-permute-start | bytes 1544 | tf_op jit(solution)/shard_map/ppermute | solution.py:48
  75.6 2.9 %copy-start.7 = (f32[2,64]{1,0:T(2,128)S(1)}, f32[2,64]{1,0:T(2,128)}, u32[]{:S(2)}) copy-start(f32[2,64]{1,0:T(2,128)} %param.23) | copy-start | bytes 1540

commit v5 on v4

--- a/solution.py
+++ b/solution.py
@@ -513,7 +513,9 @@
 def last_read_kernel(cut, offsets, *refs):
     count = len(offsets)
     blocks = refs[:count]
-    edges_ref, weight_ref, taps_ref, read_ref, gate_ref, values_ref, gated_ref, square_ref, line, total = refs[count:]
+    edges_ref, weight_ref, taps_ref, read_ref, gate_ref, scale_ref, values_ref, gated_ref, square_ref, line, total = refs[
+        count:
+    ]
     total[...] = read_ref[...]
     for index, offset in enumerate(offsets):
         part = line.at[index]
@@ -528,15 +530,15 @@
     read = jnp.sum(jnp.where(mine, total[...], 0.0), axis=0, keepdims=True)
     read = jnp.concatenate([read[:, h * HEAD : (h + 1) * HEAD] for h in range(heads)], axis=0)
     gated = read * silu(gate_ref[0].astype(F32))
-    gated_ref[...] = gated
+    gated_ref[...] = gated * scale_ref[...]
     square = jnp.sum(jnp.sum(gated * gated, axis=1, keepdims=True), axis=0, keepdims=True)
     square_ref[...] = jnp.broadcast_to(square, square_ref.shape)
 
 
-def last_read(offsets, late, edges, weight, taps, read, gate, cut):
+def last_read(offsets, late, edges, weight, taps, read, gate, scale, cut):
     rows, share = late[0].shape
     vmem = pl.BlockSpec(memory_space=pltpu.VMEM)
-    inputs = [late[k] for k in offsets] + [edges, weight, taps, read, gate]
+    inputs = [late[k] for k in offsets] + [edges, weight, taps, read, gate, scale]
     return pl.pallas_call(
         lambda *refs: last_read_kernel(cut, offsets, *refs),
         in_specs=[vmem] * len(inputs),
@@ -633,11 +635,11 @@
     final = [offset for offset in range(half, devices) if offset % group_devices]
     for wave in (first, middle):
         out, read = late_rows(wave, late_blocks, edges, keys, weight, taps, read, out, cut)
-    values, gated, group_sq = last_read(final, late_blocks, edges, weight, taps, read, newest_output_switch, cut)
+    values, gated, group_sq = last_read(final, late_blocks, edges, weight, taps, read, newest_output_switch, cluster_scaling_coefficients, cut)
     for level in range(group_devices.bit_length() - 1):
         group_sq = group_sq + flip_permute(group_sq, 2**level)
     out = last_rows(final, values, keys, out, cut)
-    scaled = gated * lax.rsqrt(group_sq[0, 0] / (repeats * HEAD) + EPS) * cluster_scaling_coefficients
+    scaled = gated * lax.rsqrt(group_sq[0, 0] / (repeats * HEAD) + EPS)
     store = out.reshape(1, devices * span, heads, HEAD + STATE)
     return store, scaled.astype(BF16).reshape(1, heads, HEAD)
 

time: 79.2 us -> 79.2 us (level)
  no operation moved by 1% of the time
where the time goes in v5:
time: 79.2 us; the launch traced here: 79 us
  starting transfers between devices  41.6 us (53%)
  Pallas kernels  30.4 us (38%)
  waiting for transfers between devices  5.55 us (7%)
  between operations  0.82 us (1%)
    ppermute x22, starting transfers between devices, flip_permute(): return lax.ppermute(value, 'sp', pairs)  41.6 us
    pallas_call x1, Pallas kernels, early_values(): pl.pallas_call(early_value_kernel, grid=(steps,), in_specs=[whole((cut, m...  7.12 us
    pallas_call x1, Pallas kernels, early_rows(): pl.pallas_call(lambda *refs: early_kernel(cut, *refs), grid=(sources,), i...  5.8 us
    pallas_call x1, Pallas kernels, late_values(): pl.pallas_call(late_value_kernel, grid=(width // tile,), in_specs=[pl.Blo...  5.58 us
    ppermute x22, waiting for transfers between devices, flip_permute(): return lax.ppermute(value, 'sp', pairs)  5.55 us
    pallas_call x2, Pallas kernels, late_rows(): pl.pallas_call(lambda *refs: late_kernel(cut, offsets, *refs), grid=(len(...  4.13 us
    pallas_call x1, Pallas kernels, key_blocks(): pl.pallas_call(lambda *refs: key_block_kernel(group_devices, *refs), grid...  3.56 us
    pallas_call x1, Pallas kernels, key_read(): pl.pallas_call(lambda *refs: key_read_kernel(group_devices, *refs), in_sp...  2.6 us
  transfers between devices with their start and end apart: 22, of which 4 were waited for; matrix products, arithmetic and copies ran while one was open for 0% of the time, Pallas kernels for 33%

profile of v5, /device:TPU:0, one launch (start us, length us, event | category | flops | bytes accessed | tf_op | source)
XLA Modules:
  0.0 79.0 jit_solution(2331361212544505881)
XLA Ops:
  0.6 3.6 %key_blocks.1 = (bf16[512,128]{1,0:T(8,128)(2,1)S(1)}, bf16[512,128]{1,0:T(8,128)(2,1)S(1)}, bf16[512,128]{1,0:T(8,128)(2,1)S(1)}, bf16[512,128]{1,0:T(8,128)(2,1)S(1)}) custom-call(bf16[1024,2048]{1,0:T(8,128)(2,1)} %bitcast.7, bf16[1024,2048]{1,0:T(8,128)(2,1)} %bitcast.8, bf16[2048,256]{1,0:T(8,128)(2,1)} %refs_2_.1), custom_call_target="tpu_custom_call" | custom-call | flops 1073741824 | bytes 4194304 | tf_op jit(solution)/shard_map/key_blocks/pallas_call | solution.py:81
  4.2 3.1 %collective-permute-start.9 = (bf16[512,128]{1,0:T(8,128)(2,1)S(1)}, bf16[512,128]{1,0:T(8,128)(2,1)S(1)}, u32[]{:S(2)}, u32[]{:S(2)}) collective-permute-start(bf16[512,128]{1,0:T(8,128)(2,1)S(1)} %get-tuple-element.46), channel_id=1, source_target_pairs={{0,4},{2,6},{4,0},{6,2},{8,12},{10,14},{12,8},{14,10},{1,5},{3,7},... | collective-permute-start | bytes 393224 | tf_op jit(solution)/shard_map/ppermute | solution.py:48
  7.3 2.6 %collective-permute-start.10 = (bf16[512,128]{1,0:T(8,128)(2,1)S(1)}, bf16[512,128]{1,0:T(8,128)(2,1)S(1)}, u32[]{:S(2)}, u32[]{:S(2)}) collective-permute-start(bf16[512,128]{1,0:T(8,128)(2,1)S(1)} %get-tuple-element.47), channel_id=1, source_target_pairs={{0,8},{2,10},{4,12},{6,14},{8,0},{10,2},{12,4},{14,6},{1,9},{3,11}... | collective-permute-start | bytes 393224 | tf_op jit(solution)/shard_map/ppermute | solution.py:48
  9.9 1.7 %collective-permute-start.12 = (bf16[512,128]{1,0:T(8,128)(2,1)S(1)}, bf16[512,128]{1,0:T(8,128)(2,1)S(1)}, u32[]{:S(2)}, u32[]{:S(2)}) collective-permute-start(bf16[512,128]{1,0:T(8,128)(2,1)S(1)} %get-tuple-element.35._.refs_0_), channel_id=1, source_target_pairs={{0,2},{2,0},{4,6},{6,4},{8,10},{10,8},{12,14},{14,12},{1,3},{3,1},... | collective-permute-start | bytes 393224 | tf_op jit(solution)/shard_map/ppermute | solution.py:48
  11.6 7.1 %early_values.1 = (bf16[536,128]{1,0:T(8,128)(2,1)S(1)}, bf16[536,128]{1,0:T(8,128)(2,1)S(1)}, bf16[536,128]{1,0:T(8,128)(2,1)S(1)}, bf16[536,128]{1,0:T(8,128)(...) custom-call(bf16[1024,2048]{1,0:T(8,128)(2,1)} %bitcast.9, ...), custom_call_target="tpu_custom_call" | custom-call | flops 2147483648 | bytes 8388608 | tf_op jit(solution)/shard_map/early_values/pallas_call | solution.py:150
  19.1 0.9 %collective-permute-start.3 = (bf16[536,128]{1,0:T(8,128)(2,1)S(1)}, bf16[536,128]{1,0:T(8,128)(2,1)S(1)}, u32[]{:S(2)}, u32[]{:S(2)}) collective-permute-start(bf16[536,128]{1,0:T(8,128)(2,1)S(1)} %get-tuple-element.40), channel_id=1, source_target_pairs={{0,4},{2,6},{4,0},{6,2},{8,12},{10,14},{12,8},{14,10},{1,5},{3,7},... | collective-permute-start | bytes 411656 | tf_op jit(solution)/shard_map/ppermute | solution.py:48
  20.2 1.5 %collective-permute-start.13 = (bf16[512,128]{1,0:T(8,128)(2,1)S(1)}, bf16[512,128]{1,0:T(8,128)(2,1)S(1)}, u32[]{:S(2)}, u32[]{:S(2)}) collective-permute-start(bf16[512,128]{1,0:T(8,128)(2,1)S(1)} %collective-permute-done.9.refs_1_), channel_id=1, source_target_pairs={{0,2},{2,0},{4,6},{6,4},{8,10},{10,8},{12,14},{14,12},{1,3},{3,1},... | collective-permute-start | bytes 393224 | tf_op jit(solution)/shard_map/ppermute | solution.py:48
  21.7 0.5 collective-permute-start.14
  22.2 1.5 %collective-permute-start.15 = (bf16[512,128]{1,0:T(8,128)(2,1)S(1)}, bf16[512,128]{1,0:T(8,128)(2,1)S(1)}, u32[]{:S(2)}, u32[]{:S(2)}) collective-permute-start(bf16[512,128]{1,0:T(8,128)(2,1)S(1)} %collective-permute-done.11.refs_3_), channel_id=1, source_target_pairs={{0,2},{2,0},{4,6},{6,4},{8,10},{10,8},{12,14},{14,12},{1,3},{3,1},... | collective-permute-start | bytes 393224 | tf_op jit(solution)/shard_map/ppermute | solution.py:48
  23.8 1.9 %collective-permute-done.2.refs_1_ = bf16[536,128]{1,0:T(8,128)(2,1)S(1)} collective-permute-done((bf16[536,128]{1,0:T(8,128)(2,1)S(1)}, bf16[536,128]{1,0:T(8,128)(2,1)S(1)}, u32[]{:S(2)}, u32[]{:S(2)}) %collective-permute-start.2) | collective-permute-done | bytes 137248 | tf_op jit(solution)/shard_map/ppermute | solution.py:48
  25.8 4.0 %collective-permute-start.5 = (bf16[536,128]{1,0:T(8,128)(2,1)S(1)}, bf16[536,128]{1,0:T(8,128)(2,1)S(1)}, u32[]{:S(2)}, u32[]{:S(2)}) collective-permute-start(bf16[536,128]{1,0:T(8,128)(2,1)S(1)} %get-tuple-element.42), channel_id=1, source_target_pairs={{0,8},{2,10},{4,12},{6,14},{8,0},{10,2},{12,4},{14,6},{1,9},{3,11}... | collective-permute-start | bytes 411656 | tf_op jit(solution)/shard_map/ppermute | solution.py:48
  29.8 5.4 %collective-permute-start.6 = (bf16[536,128]{1,0:T(8,128)(2,1)S(1)}, bf16[536,128]{1,0:T(8,128)(2,1)S(1)}, u32[]{:S(2)}, u32[]{:S(2)}) collective-permute-start(bf16[536,128]{1,0:T(8,128)(2,1)S(1)} %get-tuple-element.43), channel_id=1, source_target_pairs={{0,10},{2,8},{4,14},{6,12},{8,2},{10,0},{12,6},{14,4},{1,11},{3,9}... | collective-permute-start | bytes 411656 | tf_op jit(solution)/shard_map/ppermute | solution.py:48
  35.3 1.9 %collective-permute-start.7 = (bf16[536,128]{1,0:T(8,128)(2,1)S(1)}, bf16[536,128]{1,0:T(8,128)(2,1)S(1)}, u32[]{:S(2)}, u32[]{:S(2)}) collective-permute-start(bf16[536,128]{1,0:T(8,128)(2,1)S(1)} %get-tuple-element.44), channel_id=1, source_target_pairs={{0,12},{2,14},{4,8},{6,10},{8,4},{10,6},{12,0},{14,2},{1,13},{3,15... | collective-permute-start | bytes 411656 | tf_op jit(solution)/shard_map/ppermute | solution.py:48
  37.2 1.9 %collective-permute-start.8 = (bf16[536,128]{1,0:T(8,128)(2,1)S(1)}, bf16[536,128]{1,0:T(8,128)(2,1)S(1)}, u32[]{:S(2)}, u32[]{:S(2)}) collective-permute-start(bf16[536,128]{1,0:T(8,128)(2,1)S(1)} %get-tuple-element.45), channel_id=1, source_target_pairs={{0,14},{2,12},{4,10},{6,8},{8,6},{10,4},{12,2},{14,0},{1,15},{3,13... | collective-permute-start | bytes 411656 | tf_op jit(solution)/shard_map/ppermute | solution.py:48
  39.0 5.6 %late_values.1 = (bf16[512,128]{1,0:T(8,128)(2,1)S(1)}, bf16[512,128]{1,0:T(8,128)(2,1)S(1)}, bf16[512,128]{1,0:T(8,128)(2,1)S(1)}, bf16[512,128]{1,0:T(8,128)(2...) custom-call(bf16[1024,2048]{1,0:T(8,128)(2,1)} %bitcast.13, ...), custom_call_target="tpu_custom_call" | custom-call | flops 2147483648 | bytes 6291456 | tf_op jit(solution)/shard_map/late_values/pallas_call | solution.py:196
  44.6 2.6 %key_read.1 = (bf16[8,1024,128]{2,1,0:T(8,128)(2,1)S(1)}, f32[8,8,128]{2,1,0:T(8,128)S(1)}) custom-call(bf16[512,128]{1,0:T(8,128)(2,1)S(1)} %get-tuple-element.35._.refs_0_, bf16[512,128]{1,0:T(8,128)(2,1)S(1)} %collective-permute-done.9.refs_1_, bf16[512,128]{1,0:T(8,128)(2,1)S(1)} %collective-permute-done.10.refs_2_, ...), custom_call_target="tpu_custom_call" | custom-call | flops 1000000000 | bytes 4000000 | tf_op jit(solution)/shard_map/key_read/pallas_call | solution.py:273
  47.3 0.9 %collective-permute-start.16 = (bf16[512,128]{1,0:T(8,128)(2,1)S(1)}, bf16[512,128]{1,0:T(8,128)(2,1)S(1)}, u32[]{:S(2)}, u32[]{:S(2)}) collective-permute-start(bf16[512,128]{1,0:T(8,128)(2,1)S(1)} %get-tuple-element.53), channel_id=1, source_target_pairs={{0,8},{2,10},{4,12},{6,14},{8,0},{10,2},{12,4},{14,6},{1,9},{3,11}... | collective-permute-start | bytes 393224 | tf_op jit(solution)/shard_map/ppermute | solution.py:48
  48.2 1.6 %collective-permute-start.17 = (bf16[512,128]{1,0:T(8,128)(2,1)S(1)}, bf16[512,128]{1,0:T(8,128)(2,1)S(1)}, u32[]{:S(2)}, u32[]{:S(2)}) collective-permute-start(bf16[512,128]{1,0:T(8,128)(2,1)S(1)} %get-tuple-element.54), channel_id=1, source_target_pairs={{0,12},{2,14},{4,8},{6,10},{8,4},{10,6},{12,0},{14,2},{1,13},{3,15... | collective-permute-start | bytes 393224 | tf_op jit(solution)/shard_map/ppermute | solution.py:48
  49.8 2.7 %collective-permute-start.18 = (bf16[512,128]{1,0:T(8,128)(2,1)S(1)}, bf16[512,128]{1,0:T(8,128)(2,1)S(1)}, u32[]{:S(2)}, u32[]{:S(2)}) collective-permute-start(bf16[512,128]{1,0:T(8,128)(2,1)S(1)} %get-tuple-element.56), channel_id=1, source_target_pairs={{0,2},{2,0},{4,6},{6,4},{8,10},{10,8},{12,14},{14,12},{1,3},{3,1},... | collective-permute-start | bytes 393224 | tf_op jit(solution)/shard_map/ppermute | solution.py:48
  52.6 0.5 collective-permute-start.19
  53.1 6.1 %collective-permute-start.20 = (bf16[512,128]{1,0:T(8,128)(2,1)S(1)}, bf16[512,128]{1,0:T(8,128)(2,1)S(1)}, u32[]{:S(2)}, u32[]{:S(2)}) collective-permute-start(bf16[512,128]{1,0:T(8,128)(2,1)S(1)} %get-tuple-element.58), channel_id=1, source_target_pairs={{0,6},{2,4},{4,2},{6,0},{8,14},{10,12},{12,10},{14,8},{1,7},{3,5},... | collective-permute-start | bytes 393224 | tf_op jit(solution)/shard_map/ppermute | solution.py:48
  59.2 5.8 %early_rows.1 = (bf16[8,2048,128]{2,1,0:T(8,128)(2,1)}, f32[32,128]{1,0:T(8,128)S(1)}, bf16[8,32,128]{2,1,0:T(8,128)(2,1)S(1)}, f32[8,4,8,128]{3,2,1,0:T(8,128)S(1)}) custom-call(bf16[536,128]{1,0:T(8,128)(2,1)S(1)} %get-tuple-element.36._.refs_0_, bf16[536,128]{1,0:T(8,128)(2,1)S(1)} %collective-permute-done.2.refs_1_, ...), custom_call_target="tpu_custom_call" | custom-call | flops 2000000000 | bytes 6000000 | tf_op jit(solution)/shard_map/early_rows/pallas_call | solution.py:424
  65.0 1.1 %collective-permute-start = (bf16[512,128]{1,0:T(8,128)(2,1)S(1)}, bf16[512,128]{1,0:T(8,128)(2,1)S(1)}, u32[]{:S(2)}, u32[]{:S(2)}) collective-permute-start(bf16[512,128]{1,0:T(8,128)(2,1)S(1)} %get-tuple-element.37), channel_id=1, source_target_pairs={{0,10},{2,8},{4,14},{6,12},{8,2},{10,0},{12,6},{14,4},{1,11},{3,9}... | collective-permute-start | bytes 393224 | tf_op jit(solution)/shard_map/ppermute | solution.py:48
  66.1 2.3 %collective-permute-start.1 = (bf16[512,128]{1,0:T(8,128)(2,1)S(1)}, bf16[512,128]{1,0:T(8,128)(2,1)S(1)}, u32[]{:S(2)}, u32[]{:S(2)}) collective-permute-start(bf16[512,128]{1,0:T(8,128)(2,1)S(1)} %get-tuple-element.38), channel_id=1, source_target_pairs={{0,14},{2,12},{4,10},{6,8},{8,6},{10,4},{12,2},{14,0},{1,15},{3,13... | collective-permute-start | bytes 393224 | tf_op jit(solution)/shard_map/ppermute | solution.py:48
  68.4 2.6 %late_rows.2 = (bf16[8,2048,128]{2,1,0:T(8,128)(2,1)}, f32[32,128]{1,0:T(8,128)S(1)}) custom-call(bf16[512,128]{1,0:T(8,128)(2,1)S(1)} %get-tuple-element.55.refs_0_, bf16[512,128]{1,0:T(8,128)(2,1)S(1)} %collective-permute-done.18.refs_1_, bf16[512,128]{1,0:T(8,128)(2,1)S(1)} %collective-permute-done.19.refs_2_, ...), custom_call_target="tpu_custom_call", output_to_operand_aliasing={{0}: (9, {})} | custom-call | flops 1000000000 | bytes 2000000 | tf_op jit(solution)/shard_map/late_rows/pallas_call | solution.py:499
  71.0 1.5 %late_rows.3 = (bf16[8,2048,128]{2,1,0:T(8,128)(2,1)}, f32[32,128]{1,0:T(8,128)S(1)}) custom-call(bf16[512,128]{1,0:T(8,128)(2,1)S(1)} %collective-permute-done.16.refs_0_, bf16[512,128]{1,0:T(8,128)(2,1)S(1)} %collective-permute-done.17.refs_1_, bf16[8,32,128]{2,1,0:T(8,128)(2,1)S(1)} %get-tuple-element.51.refs_4_.refs_2_, ...), custom_call_target="tpu_custom_call", output_to_operand_aliasing={{0}: (7, {})} | custom-call | flops 1000000000 | bytes 2000000 | tf_op jit(solution)/shard_map/late_rows/pallas_call | solution.py:499
  72.5 1.6 %collective-permute-done.refs_0_ = bf16[512,128]{1,0:T(8,128)(2,1)S(1)} collective-permute-done((bf16[512,128]{1,0:T(8,128)(2,1)S(1)}, bf16[512,128]{1,0:T(8,128)(2,1)S(1)}, u32[]{:S(2)}, u32[]{:S(2)}) %collective-permute-start) | collective-permute-done | bytes 131104 | tf_op jit(solution)/shard_map/ppermute | solution.py:48
  74.1 0.7 last_read.1
  74.8 0.8 %collective-permute-start.21 = (f32[1,128]{1,0:T(1,128)S(1)}, f32[1,128]{1,0:T(1,128)S(1)}, u32[]{:S(2)}, u32[]{:S(2)}) collective-permute-start(f32[1,128]{1,0:T(1,128)S(1)} %get-tuple-element.67), channel_id=1, source_target_pairs={{0,2},{2,0},{4,6},{6,4},{8,10},{10,8},{12,14},{14,12},{1,3},{3,1},... | collective-permute-start | bytes 1544 | tf_op jit(solution)/shard_map/ppermute | solution.py:48
  75.6 1.0 %last_rows.1 = bf16[8,2048,128]{2,1,0:T(8,128)(2,1)} custom-call(bf16[2,512,128]{2,1,0:T(8,128)(2,1)S(1)} %get-tuple-element.64.refs_0_, bf16[8,1024,128]{2,1,0:T(8,128)(2,1)S(1)} %get-tuple-element.49.refs_8_.refs_5_.refs_3_.refs_1_, bf16[8,2048,128]{2,1,0:T(8,128)(2,1)} %get-tuple-element.65.refs_2_), custom_call_target="tpu_custom_call", output_to_operand_aliasing={{}: (2, {})} | custom-call | flops 1000000000 | bytes 2000000 | tf_op jit(solution)/shard_map/last_rows/pallas_call | solution.py:568
  76.6 1.8 %collective-permute-done.21 = f32[1,128]{1,0:T(1,128)S(1)} collective-permute-done((f32[1,128]{1,0:T(1,128)S(1)}, f32[1,128]{1,0:T(1,128)S(1)}, u32[]{:S(2)}, u32[]{:S(2)}) %collective-permute-start.21) | collective-permute-done | bytes 544 | tf_op jit(solution)/shard_map/ppermute | solution.py:48
  78.5 0.5 fusion
  (39 shorter events, 0.8 us)
Async XLA Ops:
  4.2 14.9 %collective-permute-start.9 = (bf16[512,128]{1,0:T(8,128)(2,1)S(1)}, bf16[512,128]{1,0:T(8,128)(2,1)S(1)}, u32[]{:S(2)}, u32[]{:S(2)}) collective-permute-start(bf16[512,128]{1,0:T(8,128)(2,1)S(1)} %get-tuple-element.46), channel_id=1, source_target_pairs={{0,4},{2,6},{4,0},{6,2},{8,12},{10,14},{12,8},{14,10},{1,5},{3,7},... | collective-permute-start | bytes 393224 | tf_op jit(solution)/shard_map/ppermute | solution.py:48
  7.3 12.9 %collective-permute-start.10 = (bf16[512,128]{1,0:T(8,128)(2,1)S(1)}, bf16[512,128]{1,0:T(8,128)(2,1)S(1)}, u32[]{:S(2)}, u32[]{:S(2)}) collective-permute-start(bf16[512,128]{1,0:T(8,128)(2,1)S(1)} %get-tuple-element.47), channel_id=1, source_target_pairs={{0,8},{2,10},{4,12},{6,14},{8,0},{10,2},{12,4},{14,6},{1,9},{3,11}... | collective-permute-start | bytes 393224 | tf_op jit(solution)/shard_map/ppermute | solution.py:48
  9.9 11.8 %collective-permute-start.11 = (bf16[512,128]{1,0:T(8,128)(2,1)S(1)}, bf16[512,128]{1,0:T(8,128)(2,1)S(1)}, u32[]{:S(2)}, u32[]{:S(2)}) collective-permute-start(bf16[512,128]{1,0:T(8,128)(2,1)S(1)} %get-tuple-element.48), channel_id=1, source_target_pairs={{0,12},{2,14},{4,8},{6,10},{8,4},{10,6},{12,0},{14,2},{1,13},{3,15... | collective-permute-start | bytes 393224 | tf_op jit(solution)/shard_map/ppermute | solution.py:48
  9.9 12.3 %collective-permute-start.12 = (bf16[512,128]{1,0:T(8,128)(2,1)S(1)}, bf16[512,128]{1,0:T(8,128)(2,1)S(1)}, u32[]{:S(2)}, u32[]{:S(2)}) collective-permute-start(bf16[512,128]{1,0:T(8,128)(2,1)S(1)} %get-tuple-element.35._.refs_0_), channel_id=1, source_target_pairs={{0,2},{2,0},{4,6},{6,4},{8,10},{10,8},{12,14},{14,12},{1,3},{3,1},... | collective-permute-start | bytes 393224 | tf_op jit(solution)/shard_map/ppermute | solution.py:48
  18.8 6.9 %collective-permute-start.2 = (bf16[536,128]{1,0:T(8,128)(2,1)S(1)}, bf16[536,128]{1,0:T(8,128)(2,1)S(1)}, u32[]{:S(2)}, u32[]{:S(2)}) collective-permute-start(bf16[536,128]{1,0:T(8,128)(2,1)S(1)} %get-tuple-element.39), channel_id=1, source_target_pairs={{0,2},{2,0},{4,6},{6,4},{8,10},{10,8},{12,14},{14,12},{1,3},{3,1},... | collective-permute-start | bytes 411656 | tf_op jit(solution)/shard_map/ppermute | solution.py:48
  19.1 6.7 %collective-permute-start.3 = (bf16[536,128]{1,0:T(8,128)(2,1)S(1)}, bf16[536,128]{1,0:T(8,128)(2,1)S(1)}, u32[]{:S(2)}, u32[]{:S(2)}) collective-permute-start(bf16[536,128]{1,0:T(8,128)(2,1)S(1)} %get-tuple-element.40), channel_id=1, source_target_pairs={{0,4},{2,6},{4,0},{6,2},{8,12},{10,14},{12,8},{14,10},{1,5},{3,7},... | collective-permute-start | bytes 411656 | tf_op jit(solution)/shard_map/ppermute | solution.py:48
  20.2 9.7 %collective-permute-start.13 = (bf16[512,128]{1,0:T(8,128)(2,1)S(1)}, bf16[512,128]{1,0:T(8,128)(2,1)S(1)}, u32[]{:S(2)}, u32[]{:S(2)}) collective-permute-start(bf16[512,128]{1,0:T(8,128)(2,1)S(1)} %collective-permute-done.9.refs_1_), channel_id=1, source_target_pairs={{0,2},{2,0},{4,6},{6,4},{8,10},{10,8},{12,14},{14,12},{1,3},{3,1},... | collective-permute-start | bytes 393224 | tf_op jit(solution)/shard_map/ppermute | solution.py:48
  21.7 13.5 %collective-permute-start.14 = (bf16[512,128]{1,0:T(8,128)(2,1)S(1)}, bf16[512,128]{1,0:T(8,128)(2,1)S(1)}, u32[]{:S(2)}, u32[]{:S(2)}) collective-permute-start(bf16[512,128]{1,0:T(8,128)(2,1)S(1)} %collective-permute-done.10.refs_2_), channel_id=1, source_target_pairs={{0,2},{2,0},{4,6},{6,4},{8,10},{10,8},{12,14},{14,12},{1,3},{3,1},... | collective-permute-start | bytes 393224 | tf_op jit(solution)/shard_map/ppermute | solution.py:48
  22.2 14.9 %collective-permute-start.15 = (bf16[512,128]{1,0:T(8,128)(2,1)S(1)}, bf16[512,128]{1,0:T(8,128)(2,1)S(1)}, u32[]{:S(2)}, u32[]{:S(2)}) collective-permute-start(bf16[512,128]{1,0:T(8,128)(2,1)S(1)} %collective-permute-done.11.refs_3_), channel_id=1, source_target_pairs={{0,2},{2,0},{4,6},{6,4},{8,10},{10,8},{12,14},{14,12},{1,3},{3,1},... | collective-permute-start | bytes 393224 | tf_op jit(solution)/shard_map/ppermute | solution.py:48
  25.7 21.6 %collective-permute-start.4 = (bf16[536,128]{1,0:T(8,128)(2,1)S(1)}, bf16[536,128]{1,0:T(8,128)(2,1)S(1)}, u32[]{:S(2)}, u32[]{:S(2)}) collective-permute-start(bf16[536,128]{1,0:T(8,128)(2,1)S(1)} %get-tuple-element.41), channel_id=1, source_target_pairs={{0,6},{2,4},{4,2},{6,0},{8,14},{10,12},{12,10},{14,8},{1,7},{3,5},... | collective-permute-start | bytes 411656 | tf_op jit(solution)/shard_map/ppermute | solution.py:48
  25.8 22.3 %collective-permute-start.5 = (bf16[536,128]{1,0:T(8,128)(2,1)S(1)}, bf16[536,128]{1,0:T(8,128)(2,1)S(1)}, u32[]{:S(2)}, u32[]{:S(2)}) collective-permute-start(bf16[536,128]{1,0:T(8,128)(2,1)S(1)} %get-tuple-element.42), channel_id=1, source_target_pairs={{0,8},{2,10},{4,12},{6,14},{8,0},{10,2},{12,4},{14,6},{1,9},{3,11}... | collective-permute-start | bytes 411656 | tf_op jit(solution)/shard_map/ppermute | solution.py:48
  29.8 20.0 %collective-permute-start.6 = (bf16[536,128]{1,0:T(8,128)(2,1)S(1)}, bf16[536,128]{1,0:T(8,128)(2,1)S(1)}, u32[]{:S(2)}, u32[]{:S(2)}) collective-permute-start(bf16[536,128]{1,0:T(8,128)(2,1)S(1)} %get-tuple-element.43), channel_id=1, source_target_pairs={{0,10},{2,8},{4,14},{6,12},{8,2},{10,0},{12,6},{14,4},{1,11},{3,9}... | collective-permute-start | bytes 411656 | tf_op jit(solution)/shard_map/ppermute | solution.py:48
  35.3 17.3 %collective-permute-start.7 = (bf16[536,128]{1,0:T(8,128)(2,1)S(1)}, bf16[536,128]{1,0:T(8,128)(2,1)S(1)}, u32[]{:S(2)}, u32[]{:S(2)}) collective-permute-start(bf16[536,128]{1,0:T(8,128)(2,1)S(1)} %get-tuple-element.44), channel_id=1, source_target_pairs={{0,12},{2,14},{4,8},{6,10},{8,4},{10,6},{12,0},{14,2},{1,13},{3,15... | collective-permute-start | bytes 411656 | tf_op jit(solution)/shard_map/ppermute | solution.py:48
  37.2 15.9 %collective-permute-start.8 = (bf16[536,128]{1,0:T(8,128)(2,1)S(1)}, bf16[536,128]{1,0:T(8,128)(2,1)S(1)}, u32[]{:S(2)}, u32[]{:S(2)}) collective-permute-start(bf16[536,128]{1,0:T(8,128)(2,1)S(1)} %get-tuple-element.45), channel_id=1, source_target_pairs={{0,14},{2,12},{4,10},{6,8},{8,6},{10,4},{12,2},{14,0},{1,15},{3,13... | collective-permute-start | bytes 411656 | tf_op jit(solution)/shard_map/ppermute | solution.py:48
  39.0 5.6 %copy-start.2 = (f32[5,4,64]{2,1,0:T(4,128)S(1)}, f32[5,4,64]{2,1,0:T(4,128)}, u32[]{:S(2)}) copy-start(f32[5,4,64]{2,1,0:T(4,128)} %refs_8_.1) | copy-start | bytes 15364
  39.0 5.6 %copy-start.3 = (bf16[1,4,64]{2,1,0:T(4,128)(2,1)S(1)}, bf16[1,4,64]{2,1,0:T(4,128)(2,1)}, u32[]{:S(2)}) copy-start(bf16[1,4,64]{2,1,0:T(4,128)(2,1)} %refs_9_.1) | copy-start | bytes 1540
  39.0 20.1 %copy-start = (f32[5,2,64]{2,1,0:T(2,128)S(1)}, f32[5,2,64]{2,1,0:T(2,128)}, u32[]{:S(2)}) copy-start(f32[5,2,64]{2,1,0:T(2,128)} %refs_4_.1) | copy-start | bytes 7684
  39.0 20.1 %copy-start.1 = (f32[1,2,8192]{2,1,0:T(2,128)S(1)}, f32[1,2,8192]{2,1,0:T(2,128)}, u32[]{:S(2)}) copy-start(f32[1,2,8192]{2,1,0:T(2,128)} %refs_11_.1) | copy-start | bytes 196612
  39.0 20.1 %copy-start.5 = (f32[2]{0:T(128)S(1)}, f32[2]{0:T(128)}, u32[]{:S(2)}) copy-start(f32[2]{0:T(128)} %refs_12_.1) | copy-start | bytes 28
  39.0 20.1 %copy-start.6 = (f32[2]{0:T(128)S(1)}, f32[2]{0:T(128)}, u32[]{:S(2)}) copy-start(f32[2]{0:T(128)} %refs_13_.1) | copy-start | bytes 28
  47.3 23.7 %collective-permute-start.16 = (bf16[512,128]{1,0:T(8,128)(2,1)S(1)}, bf16[512,128]{1,0:T(8,128)(2,1)S(1)}, u32[]{:S(2)}, u32[]{:S(2)}) collective-permute-start(bf16[512,128]{1,0:T(8,128)(2,1)S(1)} %get-tuple-element.53), channel_id=1, source_target_pairs={{0,8},{2,10},{4,12},{6,14},{8,0},{10,2},{12,4},{14,6},{1,9},{3,11}... | collective-permute-start | bytes 393224 | tf_op jit(solution)/shard_map/ppermute | solution.py:48
  48.2 22.8 %collective-permute-start.17 = (bf16[512,128]{1,0:T(8,128)(2,1)S(1)}, bf16[512,128]{1,0:T(8,128)(2,1)S(1)}, u32[]{:S(2)}, u32[]{:S(2)}) collective-permute-start(bf16[512,128]{1,0:T(8,128)(2,1)S(1)} %get-tuple-element.54), channel_id=1, source_target_pairs={{0,12},{2,14},{4,8},{6,10},{8,4},{10,6},{12,0},{14,2},{1,13},{3,15... | collective-permute-start | bytes 393224 | tf_op jit(solution)/shard_map/ppermute | solution.py:48
  49.8 15.1 %collective-permute-start.18 = (bf16[512,128]{1,0:T(8,128)(2,1)S(1)}, bf16[512,128]{1,0:T(8,128)(2,1)S(1)}, u32[]{:S(2)}, u32[]{:S(2)}) collective-permute-start(bf16[512,128]{1,0:T(8,128)(2,1)S(1)} %get-tuple-element.56), channel_id=1, source_target_pairs={{0,2},{2,0},{4,6},{6,4},{8,10},{10,8},{12,14},{14,12},{1,3},{3,1},... | collective-permute-start | bytes 393224 | tf_op jit(solution)/shard_map/ppermute | solution.py:48
  52.6 13.6 %collective-permute-start.19 = (bf16[512,128]{1,0:T(8,128)(2,1)S(1)}, bf16[512,128]{1,0:T(8,128)(2,1)S(1)}, u32[]{:S(2)}, u32[]{:S(2)}) collective-permute-start(bf16[512,128]{1,0:T(8,128)(2,1)S(1)} %get-tuple-element.57), channel_id=1, source_target_pairs={{0,4},{2,6},{4,0},{6,2},{8,12},{10,14},{12,8},{14,10},{1,5},{3,7},... | collective-permute-start | bytes 393224 | tf_op jit(solution)/shard_map/ppermute | solution.py:48
  53.1 15.3 %collective-permute-start.20 = (bf16[512,128]{1,0:T(8,128)(2,1)S(1)}, bf16[512,128]{1,0:T(8,128)(2,1)S(1)}, u32[]{:S(2)}, u32[]{:S(2)}) collective-permute-start(bf16[512,128]{1,0:T(8,128)(2,1)S(1)} %get-tuple-element.58), channel_id=1, source_target_pairs={{0,6},{2,4},{4,2},{6,0},{8,14},{10,12},{12,10},{14,8},{1,7},{3,5},... | collective-permute-start | bytes 393224 | tf_op jit(solution)/shard_map/ppermute | solution.py:48
  65.0 9.2 %collective-permute-start = (bf16[512,128]{1,0:T(8,128)(2,1)S(1)}, bf16[512,128]{1,0:T(8,128)(2,1)S(1)}, u32[]{:S(2)}, u32[]{:S(2)}) collective-permute-start(bf16[512,128]{1,0:T(8,128)(2,1)S(1)} %get-tuple-element.37), channel_id=1, source_target_pairs={{0,10},{2,8},{4,14},{6,12},{8,2},{10,0},{12,6},{14,4},{1,11},{3,9}... | collective-permute-start | bytes 393224 | tf_op jit(solution)/shard_map/ppermute | solution.py:48
  66.1 8.0 %collective-permute-start.1 = (bf16[512,128]{1,0:T(8,128)(2,1)S(1)}, bf16[512,128]{1,0:T(8,128)(2,1)S(1)}, u32[]{:S(2)}, u32[]{:S(2)}) collective-permute-start(bf16[512,128]{1,0:T(8,128)(2,1)S(1)} %get-tuple-element.38), channel_id=1, source_target_pairs={{0,14},{2,12},{4,10},{6,8},{8,6},{10,4},{12,2},{14,0},{1,15},{3,13... | collective-permute-start | bytes 393224 | tf_op jit(solution)/shard_map/ppermute | solution.py:48
  71.0 3.2 %copy-start.4 = (f32[2,64]{1,0:T(2,128)S(1)}, f32[2,64]{1,0:T(2,128)}, u32[]{:S(2)}) copy-start(f32[2,64]{1,0:T(2,128)} %refs_7_.3) | copy-start | bytes 1540
  71.0 3.2 %copy-start.7 = (bf16[1,2,64]{2,1,0:T(2,128)(2,1)S(1)}, bf16[1,2,64]{2,1,0:T(2,128)(2,1)}, u32[]{:S(2)}) copy-start(bf16[1,2,64]{2,1,0:T(2,128)(2,1)} %refs_6_.1) | copy-start | bytes 772
  74.8 3.6 %collective-permute-start.21 = (f32[1,128]{1,0:T(1,128)S(1)}, f32[1,128]{1,0:T(1,128)S(1)}, u32[]{:S(2)}, u32[]{:S(2)}) collective-permute-start(f32[1,128]{1,0:T(1,128)S(1)} %get-tuple-element.67), channel_id=1, source_target_pairs={{0,2},{2,0},{4,6},{6,4},{8,10},{10,8},{12,14},{14,12},{1,3},{3,1},... | collective-permute-start | bytes 1544 | tf_op jit(solution)/shard_map/ppermute | solution.py:48
